TPU v7x, 32 devices: a whole 2x2x4 slice. The times are simulated.
32 devices in a mesh: dp: 4 (over y, x), kv: 4 (over z), tp: 2 (over core).
Axes of the slice: x: 2, y: 2, z: 4, core: 2. Of those that a mesh axis runs over, the one named last changes fastest.
Arguments:
- tokens: bfloat16 [32, 4096], P('dp', ('kv', 'tp')), may hold values from -27 to 27
- lengths: int32 [32], P(('dp', 'kv')), may hold values from 1 to 64, 512 in all
- state: float32 [32, 4, 384, 768], P(('dp', 'kv'), 'tp'), may hold values from -6 to 6
- cache_keys: bfloat16 [32, 4, 64, 384], P(('dp', 'kv'), 'tp'), may hold values from -6 to 6
- cache_values: bfloat16 [32, 4, 64, 768], P(('dp', 'kv'), 'tp'), may hold values from -6 to 6
- cache_rates: float32 [32, 4, 64, 384], P(('dp', 'kv'), 'tp'), may hold values from 0.002 to 0.3
- attn_gain: bfloat16 [4096], P('kv'), may hold values from 0.099609375 to 1.8984375
- w_query: bfloat16 [4096, 1536], P('kv', 'tp'), may hold values from -0.09375 to 0.09375
- w_key: bfloat16 [4096, 1536], P('kv', 'tp'), may hold values from -0.09375 to 0.09375
- w_value: bfloat16 [4096, 3072], P('kv', 'tp'), may hold values from -0.09375 to 0.09375
- w_gate: bfloat16 [4096, 3072], P('kv', 'tp'), may hold values from -0.09375 to 0.09375
- w_decay: bfloat16 [4096, 1536], P('kv', 'tp'), may hold values from -0.375 to 0.375
- head_gain: bfloat16 [4, 768], P('tp'), may hold values from 0.099609375 to 1.8984375
- w_out: bfloat16 [3072, 4096], P(None, ('kv', 'tp')), may hold values from -0.109375 to 0.109375
- mlp_gain: bfloat16 [4096], replicated, may hold values from 0.099609375 to 1.8984375
- w_mlp_gate: bfloat16 [4096, 11008], P(None, ('kv', 'tp')), may hold values from -0.09375 to 0.09375
- w_mlp_up: bfloat16 [4096, 11008], P(None, ('kv', 'tp')), may hold values from -0.09375 to 0.09375
- w_mlp_down: bfloat16 [11008, 4096], P(('kv', 'tp')), may hold values from -0.078125 to 0.078125
Outputs:
- result: bfloat16 [32, 4096], P('dp', ('kv', 'tp'))
Inputs may be any that keep to these rules, and one draw needn't show every extreme that they name: `lengths`: each sequence's count of live slots in its block cache; slots from that count on take no part.
All inputs are finite; a program needn't handle non-finite values.
Results may differ from a plain program's by a relative error of at most 0.0085.
Values may be sent and summed in bfloat16 or wider, within the bound.
No kernel may reach another device: no remote copies, remote signals or barrier semaphores. Data moves between devices by JAX's collectives and lax.ppermute only.
A program may use at most 128 MiB of HBM per device.

v0:
```python
import jax
import jax.numpy as jnp
from jax import lax
from jax.sharding import PartitionSpec as P

EPS = 1e-06
GATE_NORM = 16.0
exact_mode = lax.Precision.HIGHEST


def front_part(query, key_new, log_decay, state, cache_keys, cache_rates, lengths):
    span = cache_keys.shape[2]
    live = (jnp.arange(span, dtype=jnp.int32)[None, :] < lengths[:, None]).astype(jnp.float32)
    running = jnp.cumsum(cache_rates * live[:, None, :, None], axis=2)
    total = running[:, :, -1:, :]
    weight = jnp.exp(running - total + log_decay[:, :, None, :])
    scores = (
        jnp.einsum(
            "bhd,bhjd->bhj", query, weight * cache_keys.astype(jnp.float32), precision=exact_mode
        )
        * live[:, None, :]
    )
    carried = jnp.einsum(
        "bhd,bhde->bhe", query * jnp.exp(log_decay - total[:, :, 0, :]), state, precision=exact_mode
    )
    own = jnp.sum(query * key_new, axis=-1, keepdims=True)
    return (scores, carried, own)


def back_part(scores, carried, own, value_new, cache_values, gate, head_gain):
    inner = jnp.einsum(
        "bhj,bhje->bhe", scores, cache_values.astype(jnp.float32), precision=exact_mode
    )
    attended = carried + inner + own * value_new
    normed = attended * lax.rsqrt(jnp.mean(attended * attended, axis=-1, keepdims=True) + EPS)
    normed = normed * head_gain.astype(jnp.float32)
    return (jax.nn.silu(gate) * normed).astype(jnp.bfloat16)


def open_heads(
    query_sum, key_sum, decay_sum, own_squares, width, state, cache_keys, cache_rates, lengths
):
    seq_dev, heads_dev, key_dim = (state.shape[0], state.shape[1], state.shape[2])
    inv_rms = lax.rsqrt(own_squares / width + EPS)[:, None]
    query = (query_sum * inv_rms * key_dim ** (-0.5)).reshape(seq_dev, heads_dev, key_dim)
    key_new = (key_sum * inv_rms).reshape(seq_dev, heads_dev, key_dim)
    log_decay = (jax.nn.log_sigmoid(decay_sum * inv_rms) / GATE_NORM).reshape(
        seq_dev, heads_dev, key_dim
    )
    scores, carried, own = front_part(
        query, key_new, log_decay, state, cache_keys, cache_rates, lengths
    )
    return (inv_rms, scores, carried, own)


def close_heads(opened, value_sum, gate_sum, cache_values, head_gain):
    inv_rms, scores, carried, own = opened
    seq_dev, heads_dev, value_dim = carried.shape
    value_new = (value_sum * inv_rms).reshape(seq_dev, heads_dev, value_dim)
    gate = (gate_sum * inv_rms).reshape(seq_dev, heads_dev, value_dim)
    heads = back_part(scores, carried, own, value_new, cache_values, gate, head_gain)
    return heads.reshape(seq_dev, heads_dev * value_dim)


def shards(
    tokens,
    lengths,
    state,
    cache_keys,
    cache_values,
    cache_rates,
    attn_gain,
    w_query,
    w_key,
    w_value,
    w_gate,
    w_decay,
    head_gain,
    w_out,
    mlp_gain,
    w_mlp_gate,
    w_mlp_up,
    w_mlp_down,
):
    seq_dev, heads_dev, value_dim = (state.shape[0], state.shape[1], state.shape[3])
    width = mlp_gain.shape[0]
    n_kv = lax.axis_size("kv")
    n_tp = lax.axis_size("tp")
    block = lax.all_gather(tokens, "tp", axis=1, tiled=True).astype(jnp.float32)
    squares = jnp.sum(block * block, axis=1)
    scaled = (block * attn_gain.astype(jnp.float32)).astype(jnp.bfloat16)
    query_part = jnp.dot(scaled, w_query, preferred_element_type=jnp.float32)
    key_part = jnp.dot(scaled, w_key, preferred_element_type=jnp.float32)
    decay_part = jnp.dot(scaled, w_decay, preferred_element_type=jnp.float32)
    value_part = jnp.dot(scaled, w_value, preferred_element_type=jnp.float32)
    gate_part = jnp.dot(scaled, w_gate, preferred_element_type=jnp.float32)
    every_square = lax.psum(squares, "kv")
    own_squares = lax.dynamic_slice_in_dim(every_square, lax.axis_index("kv") * seq_dev, seq_dev)
    query_sum, key_sum, decay_sum, value_sum, gate_sum = (
        lax.psum_scatter(query_part, "kv", scatter_dimension=0, tiled=True),
        lax.psum_scatter(key_part, "kv", scatter_dimension=0, tiled=True),
        lax.psum_scatter(decay_part, "kv", scatter_dimension=0, tiled=True),
        lax.psum_scatter(value_part, "kv", scatter_dimension=0, tiled=True),
        lax.psum_scatter(gate_part, "kv", scatter_dimension=0, tiled=True),
    )
    opened = open_heads(
        query_sum, key_sum, decay_sum, own_squares, width, state, cache_keys, cache_rates, lengths
    )
    heads = close_heads(opened, value_sum, gate_sum, cache_values, head_gain)
    columns = w_out.shape[1]
    stacked = w_out.reshape(n_tp, heads_dev * value_dim, columns)
    piece = lax.all_gather(
        heads.reshape(1, seq_dev, heads_dev * value_dim), ("kv", "tp"), axis=0, tiled=True
    )
    terms = jnp.einsum("psk,tkc->ptsc", piece, stacked, preferred_element_type=jnp.float32)
    owner = jnp.arange(piece.shape[0], dtype=jnp.int32)
    row_match = (owner // n_tp)[:, None, None] == jnp.arange(n_kv, dtype=jnp.int32)[None, :, None]
    head_match = (owner % n_tp)[:, None, None] == jnp.arange(n_tp, dtype=jnp.int32)[None, None, :]
    chosen = (row_match & head_match).astype(jnp.float32)
    projected = jnp.einsum("prt,ptsc->rsc", chosen, terms, precision=exact_mode)
    projected = projected.reshape(n_kv * seq_dev, columns)
    after = (tokens.astype(jnp.float32) + projected).astype(jnp.bfloat16)
    whole = lax.all_gather(after, ("kv", "tp"), axis=1, tiled=True).astype(jnp.float32)
    inv_second = lax.rsqrt(jnp.mean(whole * whole, axis=1, keepdims=True) + EPS)
    normed = (whole * inv_second * mlp_gain.astype(jnp.float32)).astype(jnp.bfloat16)
    gate_ff = jnp.dot(normed, w_mlp_gate, preferred_element_type=jnp.float32)
    up_ff = jnp.dot(normed, w_mlp_up, preferred_element_type=jnp.float32)
    hidden = (jax.nn.silu(gate_ff) * up_ff).astype(jnp.bfloat16)
    terms = jnp.dot(hidden, w_mlp_down, preferred_element_type=jnp.float32)
    own_share = lax.psum_scatter(terms, ("kv", "tp"), scatter_dimension=1, tiled=True)
    return (after.astype(jnp.float32) + own_share).astype(jnp.bfloat16)


def solution(mesh):
    placed = (
        P("dp", ("kv", "tp")),
        P(("dp", "kv")),
        P(("dp", "kv"), "tp", None, None),
        P(("dp", "kv"), "tp", None, None),
        P(("dp", "kv"), "tp", None, None),
        P(("dp", "kv"), "tp", None, None),
        P("kv"),
        P("kv", "tp"),
        P("kv", "tp"),
        P("kv", "tp"),
        P("kv", "tp"),
        P("kv", "tp"),
        P("tp", None),
        P(None, ("kv", "tp")),
        P(),
        P(None, ("kv", "tp")),
        P(None, ("kv", "tp")),
        P(("kv", "tp"), None),
    )
    return jax.shard_map(
        shards, mesh=mesh, in_specs=placed, out_specs=P("dp", ("kv", "tp")), check_vma=False
    )
```

profile of v0, /device:TPU:0, one launch (start us, length us, event | category | flops | bytes accessed | tf_op | source)
XLA Modules:
  0.0 165.6 jit_solution(11538760406876596802)
XLA Ops:
  6.5 2.3 %all_gather.9 = bf16[8,1024]{1,0:T(8,128)(2,1)S(1)} all-gather(bf16[8,512]{1,0:T(8,128)(2,1)} %param.18), channel_id=1, replica_groups=mesh['dp'=4,'kv'=4,'tp'=2] {'tp'}, dimensions={1}, use_global_device_ids=true | all-gather | bytes 24576 | tf_op jit(solution)/shard_map/all_gather | solution.py:89
  10.2 2.4 %fusion.45 = f32[8,768]{1,0:T(8,128)} fusion(bf16[1024,768]{1,0:T(8,128)(2,1)} %param.25, bf16[8,1024]{1,0:T(8,128)(2,1)S(1)} %all_gather.9, f32[1024]{0:T(1024)S(1)} %convert_element_type.57), kind=kOutput, calls=%fused_computation.73 | convolution fusion | flops 12607488 | bytes 1617920 | tf_op jit(solution)/shard_map/dot_general | solution.py:92
  12.6 2.5 %fusion.43 = f32[8,768]{1,0:T(8,128)} fusion(bf16[1024,768]{1,0:T(8,128)(2,1)} %param.29, bf16[8,1024]{1,0:T(8,128)(2,1)S(1)} %all_gather.9, f32[1024]{0:T(1024)S(1)} %convert_element_type.57), kind=kOutput, calls=%fused_computation.72 | convolution fusion | flops 12607488 | bytes 1617920 | tf_op jit(solution)/shard_map/dot_general | solution.py:94
  15.1 1.1 fusion.39
  16.2 0.9 fusion.41
  17.2 1.1 fusion.47
  19.6 0.9 broadcast_multiply_fusion
  20.5 1.4 reduce_window_sum.11
  23.6 0.7 convert_element_type.66
  24.3 1.3 dynamic-slice
  26.2 1.2 iota_compare_fusion
  27.4 28.9 %all-reduce.8.cloned.1.call-done = (f32[8,768]{1,0:T(8,128)}, f32[8]{0:T(128)}, f32[8,768]{1,0:T(8,128)}, f32[8,1536]{1,0:T(8,128)}, f32[8,768]{1,0:T(8,128)}, /*index=5*/f32[8,1536]{1,0:T(8,128)}) async-done(((f32[8,768]{1,0:T(8,128)}, f32[8]{0:T(128)}, f32[8,768]{1,0:T(8,128)}, f32[8,1536]{1,0:T(8,128)}, f32[8,768]{1,0:T(8,128)}, /*index=5*/f32[8,1536]{1,0:T(8,128)}), (f32[8,768]{1,0:T(8,128)}, ...) | async-done | bytes 172080
  56.3 0.7 add_rsqrt_fusion.2
  57.5 1.5 fusion.30
  59.0 1.3 reshape.149
  60.3 1.3 reshape.166
  61.6 1.5 dynamic-slice_multiply_fusion.1
  63.1 1.3 reshape.152
  64.4 1.3 reshape.150
  65.7 1.3 reshape.151
  67.0 1.5 fusion.2
  68.5 0.7 broadcast_multiply_fusion.1
  69.2 0.7 reshape.148
  70.0 0.8 multiply_bitcast_fusion
  70.8 1.3 fusion.51
  72.1 4.7 %fusion.33 = f32[2,2,1,768]{3,2,1,0:T(1,128)S(1)} fusion(f32[2,2,384,768]{3,2,1,0:T(8,128)} %param.20, f32[2,2,384,1]{2,1,0,3:T(2,128)S(1)} %get-tuple-element.13), kind=kOutput, calls=%fused_computation.50 | convolution fusion | flops 14155776 | bytes 4737024 | tf_op jit(solution)/shard_map/bhd,bhde->bhe/dot_general | solution.py:23
  77.0 14.1 %all_gather.10 = bf16[8,2,1536]{2,1,0:T(2,128)(2,1)S(1)} all-gather(bf16[1,2,1536]{2,1,0:T(2,128)(2,1)S(1)} %reshape_reshape.3), channel_id=1, replica_groups=mesh['dp'=4,'kv'=4,'tp'=2] {'kv','tp'}, dimensions={0}, use_global_device_ids=true | all-gather | bytes 55296 | tf_op jit(solution)/shard_map/all_gather | solution.py:112
  92.0 14.2 %all_gather.11 = bf16[8,4096]{1,0:T(8,128)(2,1)S(1)} all-gather(bf16[8,512]{1,0:T(8,128)(2,1)S(1)} %add_convert_fusion.1), channel_id=1, replica_groups=mesh['dp'=4,'kv'=4,'tp'=2] {'kv','tp'}, dimensions={1}, use_global_device_ids=true | all-gather | bytes 73728 | tf_op jit(solution)/shard_map/all_gather | solution.py:123
  106.3 7.2 %fusion.27 = f32[8,1376]{1,0:T(8,128)S(1)} fusion(bf16[4096,1376]{0,1:T(8,128)(2,1)} %param.33, bf16[8,4096]{1,0:T(8,128)(2,1)S(1)} %all_gather.11, f32[4096]{0:T(1024)S(1)} %convert_element_type.66, f32[8]{0:T(128)S(1)} %add_rsqrt_fusion.1), kind=kOutput, calls=%fused_computation.41 | convolution fusion | flops 90308608 | bytes 11398176 | tf_op jit(solution)/shard_map/dot_general | solution.py:126
  113.5 13.2 %fusion.1 = f32[8,4096]{1,0:T(8,128)} fusion(bf16[1376,4096]{1,0:T(8,128)(2,1)} %param.35, bf16[4096,1376]{0,1:T(8,128)(2,1)} %param.34, f32[8,1376]{1,0:T(8,128)S(1)} %fusion.27, bf16[8,4096]{1,0:T(8,128)(2,1)S(1)} %all_gather.11, f32[4096]{0:T(1024)S(1)} %convert_element_type.66, f32[8]{0:T(128)S(1)} %add_rsqrt_fusion.1), kind=kOutput, calls=%fused_computation.4 | convolution fusion | flops 180552192 | bytes 22801440 | tf_op jit(solution)/shard_map/dot_general | solution.py:129
  126.8 30.7 %reduce-scatter.2.cloned.1.call-done = f32[8,512]{1,0:T(8,128)} async-done(((f32[8,4096]{1,0:T(8,128)}), f32[8,512]{1,0:T(8,128)}) %reduce-scatter.2.cloned.1.call-update) | async-done | bytes 16400 | tf_op jit(solution)/shard_map/reduce_scatter | solution.py:130
  157.4 1.3 add_convert_fusion
  (54 shorter events, 6.1 us)
Async XLA Ops:
  6.5 84.7 %copy-start = (bf16[3072,512]{1,0:T(8,128)(2,1)S(1)}, bf16[3072,512]{1,0:T(8,128)(2,1)}, u32[]{:S(2)}) copy-start(bf16[3072,512]{1,0:T(8,128)(2,1)} %param.31) | copy-start | bytes 9437188
  6.5 49.8 %all-reduce.8.cloned.1.call-start = ((), (), s32[]{:S(2)}) async-start(), calls=%async_computation.2 | async-start | bytes 345088
  6.5 8.6 %copy-start.1 = (bf16[1024,1536]{1,0:T(8,128)(2,1)S(1)}, bf16[1024,1536]{1,0:T(8,128)(2,1)}, u32[]{:S(2)}) copy-start(bf16[1024,1536]{1,0:T(8,128)(2,1)} %param.27) | copy-start | bytes 9437188
  10.2 6.1 %copy-start.3 = (bf16[1024,768]{1,0:T(8,128)(2,1)S(1)}, bf16[1024,768]{1,0:T(8,128)(2,1)}, u32[]{:S(2)}) copy-start(bf16[1024,768]{1,0:T(8,128)(2,1)} %param.26) | copy-start | bytes 4718596
  12.6 4.6 %copy-start.2 = (bf16[1024,1536]{1,0:T(8,128)(2,1)S(1)}, bf16[1024,1536]{1,0:T(8,128)(2,1)}, u32[]{:S(2)}) copy-start(bf16[1024,1536]{1,0:T(8,128)(2,1)} %param.28) | copy-start | bytes 9437188
  16.2 2.7 %copy-start.14 = (s32[2]{0:T(128)S(1)}, s32[2]{0:T(128)}, u32[]{:S(2)}) copy-start(s32[2]{0:T(128)} %param.19) | copy-start | bytes 28
  16.2 3.4 %copy-start.4 = (f32[2,2,64,384]{3,2,1,0:T(8,128)S(1)}, f32[2,2,64,384]{3,2,1,0:T(8,128)}, u32[]{:S(2)}) copy-start(f32[2,2,64,384]{3,2,1,0:T(8,128)} %param.23) | copy-start | bytes 1179652
  16.2 6.2 %copy-start.10 = (bf16[2,768]{1,0:T(2,128)(2,1)S(1)}, bf16[2,768]{1,0:T(2,128)(2,1)}, u32[]{:S(2)}) copy-start(bf16[2,768]{1,0:T(2,128)(2,1)} %param.30) | copy-start | bytes 9220
  18.3 139.1 %reduce-scatter.2.cloned.1.call-start = ((), (), s32[]{:S(2)}) async-start(), calls=%async_computation.1 | async-start | bytes 147456 | tf_op jit(solution)/shard_map/reduce_scatter | solution.py:130
  19.1 0.6 copy-start.9
  21.8 1.2 copy-start.5
  57.0 0.5 copy-start.11
  68.5 8.2 %copy-start.6 = (f32[2,2,768]{2,1,0:T(2,128)S(1)}, f32[2,2,768]{2,1,0:T(2,128)}, u32[]{:S(2)}) copy-start(f32[2,2,768]{2,1,0:T(2,128)} %reshape.152) | copy-start | bytes 36868
  68.5 8.4 %copy-start.8 = (f32[2,768]{1,0:T(2,128)S(1)}, f32[2,768]{1,0:T(2,128)}, u32[]{:S(2)}) copy-start(f32[2,768]{1,0:T(2,128)} %convert_element_type.61) | copy-start | bytes 18436
  72.1 19.6 %copy-start.12 = (pred[8,2]{0,1:T(4,128)(4,1)S(1)}, pred[8,2]{0,1:T(4,128)(4,1)}, u32[]{:S(2)}) copy-start(pred[8,2]{0,1:T(4,128)(4,1)} %iota_compare_fusion.1) | copy-start | bytes 52
  72.1 19.6 %copy-start.13 = (pred[8,4]{0,1:T(4,128)(4,1)S(1)}, pred[8,4]{0,1:T(4,128)(4,1)}, u32[]{:S(2)}) copy-start(pred[8,4]{0,1:T(4,128)(4,1)} %iota_compare_fusion) | copy-start | bytes 100
  72.1 19.9 %copy-start.7 = (bf16[8,512]{1,0:T(8,128)(2,1)S(1)}, bf16[8,512]{1,0:T(8,128)(2,1)}, u32[]{:S(2)}) copy-start(bf16[8,512]{1,0:T(8,128)(2,1)} %param.18) | copy-start | bytes 24580
Sparse Core Ops, SparseCore 0:
  18.4 37.8 all-reduce.7
  126.9 30.5 reduce-scatter.1
where the time goes:
time: 166 us
  waiting for transfers between devices  59.6 us (36%)
  matrix products  36.7 us (22%)
  blocking collectives  30.6 us (18%)
  other arithmetic  14.2 us (9%)
  between operations  14.2 us (9%)
  local copies, waits for them, and re-layouts  10.3 us (6%)
    reduce_scatter x1, waiting for transfers between devices, shards(): lax.psum_scatter(terms, ('kv', 'tp'), scatter_dimension=1, tiled=True)  30.7 us
    unnamed x3, waiting for transfers between devices  28.9 us
    all_gather x1, blocking collectives, shards(): lax.all_gather(after, ('kv', 'tp'), axis=1, tiled=True).astype(jnp.float32)  14.2 us
    all_gather x1, blocking collectives, shards(): lax.all_gather(heads.reshape(1, seq_dev, heads_dev * value_dim), ('kv', '...  14.1 us
    dot_general x1, matrix products, shards(): terms = jnp.dot(hidden, w_mlp_down, preferred_element_type=jnp.float32)  13.2 us
    dot_general x1, matrix products, shards(): gate_ff = jnp.dot(normed, w_mlp_gate, preferred_element_type=jnp.float32)  7.2 us
    dot_general x1, matrix products, front_part(): jnp.einsum('bhd,bhde->bhe', query * jnp.exp(log_decay - total[:, :, 0, :]...  4.66 us
  transfers between devices with their start and end apart: 2, of which 2 were waited for; matrix products, arithmetic and copies ran while one was open for 5% of the time, Pallas kernels for 0%

commit v1 on v0

--- a/solution.py
+++ b/solution.py
@@ -1,6 +1,8 @@
 import jax
 import jax.numpy as jnp
 from jax import lax
+from jax.experimental import pallas as pl
+from jax.experimental.pallas import tpu as pltpu
 from jax.sharding import PartitionSpec as P
 
 EPS = 1e-06
@@ -62,7 +64,7 @@
     return heads.reshape(seq_dev, heads_dev * value_dim)
 
 
-def shards(
+def plain_shards(
     tokens,
     lengths,
     state,
@@ -131,6 +133,260 @@
     return (after.astype(jnp.float32) + own_share).astype(jnp.bfloat16)
 
 
+F32 = jnp.float32
+BF16 = jnp.bfloat16
+LANES = 128
+
+
+def in_vmem(array):
+    return pltpu.with_memory_space_constraint(array, pltpu.VMEM)
+
+
+def in_hbm(array):
+    return pltpu.with_memory_space_constraint(array, pltpu.HBM)
+
+
+def vmem_spec():
+    return pl.BlockSpec(memory_space=pltpu.VMEM)
+
+
+def call(kernel, out_shape, in_specs, scratch, limit, flops, moved, name):
+    return pl.pallas_call(
+        kernel,
+        out_shape=out_shape,
+        in_specs=in_specs,
+        out_specs=jax.tree.map(lambda _: vmem_spec(), out_shape),
+        scratch_shapes=scratch,
+        compiler_params=pltpu.CompilerParams(vmem_limit_bytes=limit),
+        cost_estimate=pl.CostEstimate(flops=flops, bytes_accessed=moved, transcendentals=0),
+        name=name,
+    )
+
+
+def project_kernel(
+    seq_dev, own_ref, other_ref, gain_ref, wq, wk, wd, wv, wg, send_ref, bq, bk, bd, bv, bg, acc, sems
+):
+    pairs = ((wq, bq), (wk, bk), (wd, bd), (wv, bv), (wg, bg))
+    copies = [pltpu.make_async_copy(src, dst, sems.at[i]) for i, (src, dst) in enumerate(pairs)]
+    for copy in copies:
+        copy.start()
+    own = own_ref[...].astype(F32)
+    other = other_ref[...].astype(F32)
+    first = lax.axis_index("tp") == 0
+    low = jnp.where(first, own, other)
+    high = jnp.where(first, other, own)
+    block = jnp.concatenate([low, high], axis=1)
+    total = jnp.sum(block * block, axis=1, keepdims=True)
+    scaled = (block * gain_ref[...].astype(F32)).astype(BF16)
+    at = 0
+    for copy, (_, buf) in zip(copies, pairs):
+        copy.wait()
+        acc[:, at : at + buf.shape[1]] = jnp.dot(scaled, buf[...], preferred_element_type=F32)
+        at += buf.shape[1]
+    lane = lax.broadcasted_iota(jnp.int32, (block.shape[0], LANES), 1)
+    upper = total.astype(BF16).astype(F32)
+    lower = total - upper
+    acc[:, at : at + LANES] = jnp.where(lane == 0, upper, jnp.where(lane == 1, lower, 0.0))
+    for i in range(send_ref.shape[0]):
+        send_ref[i] = acc[i * seq_dev : (i + 1) * seq_dev, :].astype(BF16)
+
+
+def split_rows(row):
+    upper = row.astype(BF16).astype(F32)
+    lower = row - upper
+    shape = (8, row.shape[1])
+    at = lax.broadcasted_iota(jnp.int32, shape, 0)
+    upper = jnp.broadcast_to(upper, shape)
+    lower = jnp.broadcast_to(lower, shape)
+    return jnp.where(at == 0, upper, jnp.where(at == 1, lower, 0.0)).astype(BF16)
+
+
+def attend_kernel(
+    width, lengths_ref, recv_ref, state_ref, keys_ref, values_ref, rates_ref, gain_ref, out_ref, heads_ref
+):
+    seq_dev, heads_dev, key_dim, value_dim = state_ref.shape
+    span = keys_ref.shape[2]
+    got = recv_ref[0].astype(F32)
+    for i in range(1, recv_ref.shape[0]):
+        got = got + recv_ref[i].astype(F32)
+    keys_all, values_all = heads_dev * key_dim, heads_dev * value_dim
+    ends = [0, keys_all, 2 * keys_all, 3 * keys_all]
+    ends += [ends[3] + values_all, ends[3] + 2 * values_all]
+    squares = jnp.sum(got[:, ends[5] :], axis=1, keepdims=True)
+    inv_rms = lax.rsqrt(squares / width + EPS)
+    query = got[:, ends[0] : ends[1]] * inv_rms * key_dim ** (-0.5)
+    key_new = got[:, ends[1] : ends[2]] * inv_rms
+    raw = got[:, ends[2] : ends[3]] * inv_rms
+    log_decay = (jnp.minimum(raw, 0.0) - jnp.log(1.0 + jnp.exp(-jnp.abs(raw)))) / GATE_NORM
+    value_new = got[:, ends[3] : ends[4]] * inv_rms
+    gate = got[:, ends[4] : ends[5]] * inv_rms
+    decayed = query * jnp.exp(log_decay)
+    product = query * key_new
+    row_at = lax.broadcasted_iota(jnp.int32, (span, span), 0)
+    col_at = lax.broadcasted_iota(jnp.int32, (span, span), 1)
+    later = jnp.where(col_at > row_at, 1.0, 0.0).astype(BF16)
+    slot_col = lax.broadcasted_iota(jnp.int32, (span, 1), 0)
+    slot_row = lax.broadcasted_iota(jnp.int32, (1, span), 1)
+    for s in range(seq_dev):
+        live_col = (slot_col < lengths_ref[s]).astype(F32)
+        live_row = (slot_row < lengths_ref[s]).astype(F32)
+        for h in range(heads_dev):
+            ks, vs = slice(h * key_dim, (h + 1) * key_dim), slice(h * value_dim, (h + 1) * value_dim)
+            rates = rates_ref[s, h] * live_col
+            upper = rates.astype(BF16)
+            lower = (rates - upper.astype(F32)).astype(BF16)
+            after = jnp.dot(later, upper, preferred_element_type=F32)
+            after = after + jnp.dot(later, lower, preferred_element_type=F32)
+            total = jnp.sum(rates, axis=0, keepdims=True)
+            weighted = jnp.exp(-after) * keys_ref[s, h].astype(F32)
+            w_upper = weighted.astype(BF16)
+            w_lower = (weighted - w_upper.astype(F32)).astype(BF16)
+            row = decayed[s : s + 1, ks]
+            rows = split_rows(row)
+            contract = (((1,), (1,)), ((), ()))
+            scores = lax.dot_general(rows, w_upper, contract, preferred_element_type=F32)
+            scores = scores + lax.dot_general(rows, w_lower, contract, preferred_element_type=F32)
+            scores = jnp.sum(scores, axis=0, keepdims=True) * live_row
+            state_rows = split_rows(row * jnp.exp(-total))
+            mixed = jnp.dot(state_rows, state_ref[s, h].astype(BF16), preferred_element_type=F32)
+            mixed = mixed + jnp.dot(split_rows(scores), values_ref[s, h], preferred_element_type=F32)
+            own = jnp.sum(product[s : s + 1, ks], axis=1, keepdims=True)
+            attended = jnp.sum(mixed, axis=0, keepdims=True) + own * value_new[s : s + 1, vs]
+            scale = lax.rsqrt(jnp.mean(attended * attended, axis=1, keepdims=True) + EPS)
+            normed = attended * scale * gain_ref[h : h + 1, :].astype(F32)
+            opened = gate[s : s + 1, vs]
+            heads_ref[s : s + 1, vs] = opened / (1.0 + jnp.exp(-opened)) * normed
+    heads = heads_ref[...].astype(BF16)
+    for i in range(out_ref.shape[0]):
+        out_ref[i] = heads
+
+
+def output_kernel(n_tp, recv_ref, weight_ref, own_ref, out_ref, rows_ref):
+    seq_dev, wide = recv_ref.shape[1], recv_ref.shape[2]
+    for i in range(recv_ref.shape[0]):
+        kv_at, tp_at = divmod(i, n_tp)
+        rows_ref[kv_at * seq_dev : (kv_at + 1) * seq_dev, tp_at * wide : (tp_at + 1) * wide] = recv_ref[
+            i
+        ].astype(F32)
+    projected = jnp.dot(rows_ref[...].astype(BF16), weight_ref[...], preferred_element_type=F32)
+    after = (own_ref[...].astype(F32) + projected).astype(BF16)
+    for i in range(out_ref.shape[0]):
+        out_ref[i] = after
+
+
+def feed_kernel(recv_ref, gain_ref, gate_ref, up_ref, down_ref, out_ref):
+    whole = jnp.concatenate([recv_ref[i].astype(F32) for i in range(recv_ref.shape[0])], axis=1)
+    inv = lax.rsqrt(jnp.mean(whole * whole, axis=1, keepdims=True) + EPS)
+    normed = (whole * inv * gain_ref[...].astype(F32)).astype(BF16)
+    contract = (((1,), (1,)), ((), ()))
+    gate = lax.dot_general(normed, gate_ref[...], contract, preferred_element_type=F32)
+    up = lax.dot_general(normed, up_ref[...], contract, preferred_element_type=F32)
+    hidden = (gate / (1.0 + jnp.exp(-gate)) * up).astype(BF16)
+    columns = out_ref.shape[2]
+    for i in range(out_ref.shape[0]):
+        piece = down_ref[:, i * columns : (i + 1) * columns]
+        out_ref[i] = jnp.dot(hidden, piece, preferred_element_type=F32).astype(BF16)
+
+
+def finish_kernel(recv_ref, after_ref, out_ref):
+    total = after_ref[0].astype(F32)
+    for i in range(recv_ref.shape[0]):
+        total = total + recv_ref[i].astype(F32)
+    out_ref[...] = total.astype(BF16)
+
+
+MIB = 1 << 20
+
+
+def shards(
+    tokens,
+    lengths,
+    state,
+    cache_keys,
+    cache_values,
+    cache_rates,
+    attn_gain,
+    w_query,
+    w_key,
+    w_value,
+    w_gate,
+    w_decay,
+    head_gain,
+    w_out,
+    mlp_gain,
+    w_mlp_gate,
+    w_mlp_up,
+    w_mlp_down,
+):
+    seq_dev, heads_dev, key_dim, value_dim = state.shape
+    width = mlp_gain.shape[0]
+    n_kv, n_tp = lax.axis_size("kv"), lax.axis_size("tp")
+    members = n_kv * n_tp
+    rows, columns = tokens.shape
+    other = lax.ppermute(tokens, "tp", [(i, n_tp - 1 - i) for i in range(n_tp)])
+    wide = heads_dev * (3 * key_dim + 2 * value_dim) + LANES
+    anywhere = pl.BlockSpec(memory_space=pl.ANY)
+    weights = (w_query, w_key, w_decay, w_value, w_gate)
+    moved = sum(w.size for w in weights) * 2
+    send = call(
+        lambda *refs: project_kernel(seq_dev, *refs),
+        jax.ShapeDtypeStruct((n_kv, seq_dev, wide), BF16),
+        [vmem_spec()] * 3 + [anywhere] * 5,
+        [pltpu.VMEM(w.shape, BF16) for w in weights]
+        + [pltpu.VMEM((rows, wide), F32), pltpu.SemaphoreType.DMA((5,))],
+        16 * MIB,
+        rows * moved,
+        moved,
+        "project",
+    )(tokens, other, attn_gain.reshape(1, -1), *(in_hbm(w) for w in weights))
+    recv = lax.all_to_all(send, "kv", 0, 0, tiled=True)
+    moved = state.size * 4 + cache_rates.size * 8
+    send = call(
+        lambda *refs: attend_kernel(width, *refs),
+        jax.ShapeDtypeStruct((members, seq_dev, heads_dev * value_dim), BF16),
+        [pl.BlockSpec(memory_space=pltpu.SMEM)] + [vmem_spec()] * 6,
+        [pltpu.VMEM((seq_dev, heads_dev * value_dim), F32)],
+        4 * MIB,
+        state.size * 16,
+        moved,
+        "attend",
+    )(lengths, recv, in_vmem(state), in_vmem(cache_keys), in_vmem(cache_values), in_vmem(cache_rates), head_gain)
+    recv = lax.all_to_all(send, ("kv", "tp"), 0, 0, tiled=True)
+    after = call(
+        lambda *refs: output_kernel(n_tp, *refs),
+        jax.ShapeDtypeStruct((members, rows, columns), BF16),
+        [vmem_spec()] * 3,
+        [pltpu.VMEM((rows, w_out.shape[0]), F32)],
+        2 * MIB,
+        rows * w_out.size * 2,
+        w_out.size * 2,
+        "output",
+    )(recv, in_vmem(w_out), tokens)
+    recv = lax.all_to_all(after, ("kv", "tp"), 0, 0, tiled=True)
+    moved = (w_mlp_gate.size + w_mlp_up.size + w_mlp_down.size) * 2
+    send = call(
+        feed_kernel,
+        jax.ShapeDtypeStruct((members, rows, columns), BF16),
+        [vmem_spec()] * 5,
+        [],
+        4 * MIB,
+        rows * moved,
+        moved,
+        "feed",
+    )(recv, mlp_gain.reshape(1, -1), in_vmem(w_mlp_gate.T), in_vmem(w_mlp_up.T), in_vmem(w_mlp_down))
+    recv = lax.all_to_all(send, ("kv", "tp"), 0, 0, tiled=True)
+    return call(
+        finish_kernel,
+        jax.ShapeDtypeStruct((rows, columns), BF16),
+        [vmem_spec()] * 2,
+        [],
+        2 * MIB,
+        rows * columns * members,
+        rows * columns * members * 2,
+        "finish",
+    )(recv, after)
+
+
 def solution(mesh):
     placed = (
         P("dp", ("kv", "tp")),
@@ -152,6 +408,12 @@
         P(None, ("kv", "tp")),
         P(("kv", "tp"), None),
     )
+    sizes = mesh.shape
+
+    def body(*args):
+        fits = sizes["tp"] == 2 and args[13].shape[1] % LANES == 0
+        return (shards if fits else plain_shards)(*args)
+
     return jax.shard_map(
-        shards, mesh=mesh, in_specs=placed, out_specs=P("dp", ("kv", "tp")), check_vma=False
-    )
+        body, mesh=mesh, in_specs=placed, out_specs=P("dp", ("kv", "tp")), check_vma=False
+    )

time: 166 us -> 70.8 us (0.43)
  waiting for transfers between devices: 59.6 us -> 6 us
  matrix products: 36.7 us -> 0 us
  Pallas kernels: 0 us -> 17.3 us
  other arithmetic: 14.2 us -> 0.01 us
  between operations: 14.2 us -> 0.12 us
  local copies, waits for them, and re-layouts: 10.3 us -> 14.7 us
  starting transfers between devices: 0.04 us -> 3.84 us
  blocking collectives: 30.6 us -> 28.4 us
    dot_general x12 -> x0, matrix products: 36.7 us -> none  [the longest x1 13.2 us: shards(): terms = jnp.dot(hidden, w_mlp_down, preferred_element_type=jnp.float32)]
    reduce_scatter x1 -> x0, waiting for transfers between devices: 30.7 us -> none  [shards(): lax.psum_scatter(terms, ('kv', 'tp'), scatter_dimension=1, tiled=True)]
    all_gather x3 -> x0, blocking collectives: 30.6 us -> none  [the longest x1 14.2 us: shards(): lax.all_gather(after, ('kv', 'tp'), axis=1, tiled=True).astype(jnp.float32)]
    unnamed x3 -> x0, waiting for transfers between devices: 28.9 us -> none
    all_to_all x0 -> x3, blocking collectives: none -> 28.4 us  [the longest x2 16.5 us: shards(): recv = lax.all_to_all(send, ('kv', 'tp'), 0, 0, tiled=True)]
    pallas_call x0 -> x5, Pallas kernels: none -> 17.3 us  [the longest x1 7.45 us: shards(): call(feed_kernel, jax.ShapeDtypeStruct((members, rows, columns), BF16), [...]
    unnamed x32 -> x26, local copies, waits for them, and re-layouts: 2.98 us -> 13.9 us
    reshape x7 -> x2, local copies, waits for them, and re-layouts: 7.26 us -> 0.85 us  [the longest x1 0.84 us: shards(): attn_gain.reshape(1, -1)]
  transfers between devices with their start and end apart: 2 -> 2, of which waited for: 2 -> 2; matrix products, arithmetic and copies ran while one was open for 5% -> 1% of each run, Pallas kernels for 0% -> 0%
where the time goes in v1:
time: 70.8 us; the launch traced here: 70.4 us
  blocking collectives  28.4 us (40%)
  Pallas kernels  17.3 us (24%)
  local copies, waits for them, and re-layouts  14.7 us (21%)
  waiting for transfers between devices  6 us (8%)
  starting transfers between devices  3.84 us (5%)
    all_to_all x2, blocking collectives, shards(): recv = lax.all_to_all(send, ('kv', 'tp'), 0, 0, tiled=True)  16.5 us
    unnamed x26, local copies, waits for them, and re-layouts  13.9 us
    all_to_all x1, blocking collectives, shards(): recv = lax.all_to_all(send, 'kv', 0, 0, tiled=True)  11.9 us
    pallas_call x1, Pallas kernels, shards(): call(feed_kernel, jax.ShapeDtypeStruct((members, rows, columns), BF16), [...  7.45 us
    all_to_all x1, waiting for transfers between devices, shards(): recv = lax.all_to_all(after, ('kv', 'tp'), 0, 0, tiled=True)  5.82 us
    pallas_call x1, Pallas kernels, shards(): call(lambda *refs: project_kernel(seq_dev, *refs), jax.ShapeDtypeStruct((...  4.84 us
    all_to_all x1, starting transfers between devices, shards(): recv = lax.all_to_all(after, ('kv', 'tp'), 0, 0, tiled=True)  3.35 us
    pallas_call x1, Pallas kernels, shards(): call(lambda *refs: attend_kernel(width, *refs), jax.ShapeDtypeStruct((mem...  2.36 us
  transfers between devices with their start and end apart: 2, of which 2 were waited for; matrix products, arithmetic and copies ran while one was open for 1% of the time, Pallas kernels for 0%

profile of v1, /device:TPU:0, one launch (start us, length us, event | category | flops | bytes accessed | tf_op | source)
XLA Modules:
  0.0 70.4 jit_solution(15189624012189330993)
XLA Ops:
  0.0 0.5 collective-permute-start
  0.5 0.0 slice-start
  0.5 0.8 %reshape.6.refs_2_ = bf16[1,1024]{1,0:T(2,128)(2,1)S(1)} reshape(bf16[1024]{0:T(1024)(128)(2,1)} %param.24) | data formatting | bytes 4096 | tf_op jit(solution)/shard_map/reshape | solution.py:341
  1.3 0.0 slice-start.1
  1.3 0.0 copy-start.4
  1.3 0.0 copy-start.6
  1.4 0.2 collective-permute-done.refs_1_
  1.5 1.2 %copy-done.7 = bf16[8,512]{1,0:T(8,128)(2,1)S(1)} copy-done((bf16[8,512]{1,0:T(8,128)(2,1)S(1)}, bf16[8,512]{1,0:T(8,128)(2,1)}, u32[]{:S(2)}) %copy-start.7) | copy-done | bytes 8216
  2.8 4.8 %project.1 = bf16[4,2,5504]{2,1,0:T(2,128)(2,1)S(1)} custom-call(bf16[8,512]{1,0:T(8,128)(2,1)S(1)} %copy-done.7, bf16[8,512]{1,0:T(8,128)(2,1)S(1)} %collective-permute-done.refs_1_, bf16[1,1024]{1,0:T(2,128)(2,1)S(1)} %reshape.6.refs_2_, bf16[1024,768]{1,0:T(8,128)(2,1)} %refs_3_.2, bf16[1024,768]{1,0:T(8,128)(2,1)} %refs_4_.2, bf16[1024,768]{1,0:T(8,128)(2,1)} %refs_5_.2, ...), custom_call_target="tpu_custom_call" | custom-call | flops 88080384 | bytes 11010048 | tf_op jit(solution)/shard_map/project/pallas_call | solution.py:331
  7.6 0.0 copy-start.3
  7.6 11.9 %all_to_all.20.refs_1_ = bf16[4,2,5504]{2,1,0:T(2,128)(2,1)S(1)} all-to-all(bf16[4,2,5504]{2,1,0:T(2,128)(2,1)S(1)} %project.1), channel_id=1, replica_groups=mesh['dp'=4,'kv'=4,'tp'=2] {'kv'}, dimensions={0} | all-to-all | bytes 176128 | tf_op jit(solution)/shard_map/all_to_all | solution.py:342
  19.5 0.0 slice-done
  19.5 0.0 slice-done.1
  19.5 0.0 copy-done.4
  19.5 0.0 copy-done.5
  19.6 0.0 copy-done.6
  19.6 0.0 copy-done.8
  19.6 0.0 copy-done.9
  19.6 2.4 %attend.1 = bf16[8,2,1536]{2,1,0:T(2,128)(2,1)S(1)} custom-call(s32[2]{0:T(128)S(1)} %copy-done.9, bf16[4,2,5504]{2,1,0:T(2,128)(2,1)S(1)} %all_to_all.20.refs_1_, f32[2,2,384,768]{3,2,1,0:T(8,128)S(1)} %bitcast.5, bf16[2,2,64,384]{3,2,1,0:T(8,128)(2,1)S(1)} %copy-done.6, bf16[2,2,64,768]{3,2,1,0:T(8,128)(2,1)S(1)} %copy-done.4, ...), custom_call_target="tpu_custom_call" | custom-call | flops 18874368 | bytes 5505024 | tf_op jit(solution)/shard_map/attend/pallas_call | solution.py:344
  22.0 0.0 copy-start.10
  22.0 8.2 %all_to_all.21.refs_0_ = bf16[8,2,1536]{2,1,0:T(2,128)(2,1)S(1)} all-to-all(bf16[8,2,1536]{2,1,0:T(2,128)(2,1)S(1)} %attend.1), channel_id=1, replica_groups=mesh['dp'=4,'kv'=4,'tp'=2] {'kv','tp'}, dimensions={0} | all-to-all | bytes 98304 | tf_op jit(solution)/shard_map/all_to_all | solution.py:354
  30.2 0.0 copy-done.3
  30.2 1.2 %output.1.after_ref = bf16[8,8,512]{2,1,0:T(8,128)(2,1)} custom-call(bf16[8,2,1536]{2,1,0:T(2,128)(2,1)S(1)} %all_to_all.21.refs_0_, bf16[3072,512]{1,0:T(8,128)(2,1)S(1)} %copy-done.3, bf16[8,512]{1,0:T(8,128)(2,1)S(1)} %copy-done.7), custom_call_target="tpu_custom_call" | custom-call | flops 25165824 | bytes 3145728 | tf_op jit(solution)/shard_map/output/pallas_call | solution.py:355
  31.3 3.3 %all-to-all-start.2 = ((bf16[8,8,512]{2,1,0:T(8,128)(2,1)}), bf16[8,8,512]{2,1,0:T(8,128)(2,1)S(1)}, u32[]{:S(2)}, u32[]{:S(2)}) async-start(bf16[8,8,512]{2,1,0:T(8,128)(2,1)} %output.1.after_ref), calls=%async_computation.2 | async-start | bytes 131072 | tf_op jit(solution)/shard_map/all_to_all | solution.py:365
  34.7 0.0 copy-done.10
  34.7 5.8 %all-to-all-done.2.recv_ref = bf16[8,8,512]{2,1,0:T(8,128)(2,1)S(1)} async-done(((bf16[8,8,512]{2,1,0:T(8,128)(2,1)}), bf16[8,8,512]{2,1,0:T(8,128)(2,1)S(1)}, u32[]{:S(2)}, u32[]{:S(2)}) %all-to-all-start.2) | async-done | bytes 65568 | tf_op jit(solution)/shard_map/all_to_all | solution.py:365
  40.6 4.2 %copy-done = bf16[4096,1376]{0,1:T(8,128)(2,1)S(1)} copy-done((bf16[4096,1376]{0,1:T(8,128)(2,1)S(1)}, bf16[4096,1376]{0,1:T(8,128)(2,1)}, u32[]{:S(2)}) %copy-start) | copy-done | bytes 11272216
  44.8 4.2 %copy-done.1 = bf16[4096,1376]{0,1:T(8,128)(2,1)S(1)} copy-done((bf16[4096,1376]{0,1:T(8,128)(2,1)S(1)}, bf16[4096,1376]{0,1:T(8,128)(2,1)}, u32[]{:S(2)}) %copy-start.1) | copy-done | bytes 11272216
  49.0 4.2 %copy-done.2 = bf16[1376,4096]{1,0:T(8,128)(2,1)S(1)} copy-done((bf16[1376,4096]{1,0:T(8,128)(2,1)S(1)}, bf16[1376,4096]{1,0:T(8,128)(2,1)}, u32[]{:S(2)}) %copy-start.2) | copy-done | bytes 11272216
  53.2 7.4 %feed.1 = bf16[8,8,512]{2,1,0:T(8,128)(2,1)S(1)} custom-call(bf16[8,8,512]{2,1,0:T(8,128)(2,1)S(1)} %all-to-all-done.2.recv_ref, bf16[1,4096]{1,0:T(2,128)(2,1)S(1)} %reshape.7.gain_ref, bf16[1376,4096]{1,0:T(8,128)(2,1)S(1)} %bitcast.2, bf16[1376,4096]{1,0:T(8,128)(2,1)S(1)} %bitcast.3, bf16[1376,4096]{1,0:T(8,128)(2,1)S(1)} %copy-done.2), custom_call_target="tpu_custom_call" | custom-call | flops 270532608 | bytes 33816576 | tf_op jit(solution)/shard_map/feed/pallas_call | solution.py:367
  60.6 8.3 %all_to_all.22.recv_ref = bf16[8,8,512]{2,1,0:T(8,128)(2,1)S(1)} all-to-all(bf16[8,8,512]{2,1,0:T(8,128)(2,1)S(1)} %feed.1), channel_id=1, replica_groups=mesh['dp'=4,'kv'=4,'tp'=2] {'kv','tp'}, dimensions={0} | all-to-all | bytes 131072 | tf_op jit(solution)/shard_map/all_to_all | solution.py:377
  68.9 1.5 %finish.1 = bf16[8,512]{1,0:T(8,128)(2,1)} custom-call(bf16[8,8,512]{2,1,0:T(8,128)(2,1)S(1)} %all_to_all.22.recv_ref, bf16[8,8,512]{2,1,0:T(8,128)(2,1)} %output.1.after_ref), custom_call_target="tpu_custom_call" | custom-call | flops 32768 | bytes 65536 | tf_op jit(solution)/shard_map/finish/pallas_call | solution.py:378
  (9 shorter events, 0.0 us)
Async XLA Ops:
  0.0 1.5 %collective-permute-start = (bf16[8,512]{1,0:T(8,128)(2,1)}, bf16[8,512]{1,0:T(8,128)(2,1)S(1)}, u32[]{:S(2)}, u32[]{:S(2)}) collective-permute-start(bf16[8,512]{1,0:T(8,128)(2,1)} %refs_2_.3), channel_id=1, source_target_pairs={{0,1},{1,0},{2,3},{3,2},{4,5},{5,4},{6,7},{7,6},{8,9},{9,8},{10,11... | collective-permute-start | bytes 24584 | tf_op jit(solution)/shard_map/ppermute | solution.py:326
  0.5 19.0 %slice-start = ((s8[4718592]{0:T(1024)(128)(4,1)}), s8[4194304]{0:T(1024)(128)(4,1)S(1)}, s32[]{:S(2)}) async-start(s8[4718592]{0:T(1024)(128)(4,1)} %bitcast.4), calls=%async_computation.4 | async-start | bytes 8388608
  1.3 18.2 %slice-start.1 = ((s8[4718592]{0:T(1024)(128)(4,1)}), s8[524288]{0:T(1024)(128)(4,1)S(1)}, s32[]{:S(2)}) async-start(s8[4718592]{0:T(1024)(128)(4,1)} %bitcast.4), calls=%async_computation.5 | async-start | bytes 1048576
  1.3 18.2 %copy-start.4 = (bf16[2,2,64,768]{3,2,1,0:T(8,128)(2,1)S(1)}, bf16[2,2,64,768]{3,2,1,0:T(8,128)(2,1)}, u32[]{:S(2)}) copy-start(bf16[2,2,64,768]{3,2,1,0:T(8,128)(2,1)} %refs_4_.3) | copy-start | bytes 1179652
  1.3 18.2 %copy-start.5 = (f32[2,2,64,384]{3,2,1,0:T(8,128)S(1)}, f32[2,2,64,384]{3,2,1,0:T(8,128)}, u32[]{:S(2)}) copy-start(f32[2,2,64,384]{3,2,1,0:T(8,128)} %refs_5_.3) | copy-start | bytes 1179652
  1.3 18.2 %copy-start.6 = (bf16[2,2,64,384]{3,2,1,0:T(8,128)(2,1)S(1)}, bf16[2,2,64,384]{3,2,1,0:T(8,128)(2,1)}, u32[]{:S(2)}) copy-start(bf16[2,2,64,384]{3,2,1,0:T(8,128)(2,1)} %refs_3_.3) | copy-start | bytes 589828
  1.5 1.2 %copy-start.7 = (bf16[8,512]{1,0:T(8,128)(2,1)S(1)}, bf16[8,512]{1,0:T(8,128)(2,1)}, u32[]{:S(2)}) copy-start(bf16[8,512]{1,0:T(8,128)(2,1)} %refs_2_.3) | copy-start | bytes 24580
  2.7 16.8 %copy-start.8 = (bf16[2,768]{1,0:T(2,128)(2,1)S(1)}, bf16[2,768]{1,0:T(2,128)(2,1)}, u32[]{:S(2)}) copy-start(bf16[2,768]{1,0:T(2,128)(2,1)} %refs_6_.3) | copy-start | bytes 9220
  2.8 16.8 %copy-start.9 = (s32[2]{0:T(128)S(1)}, s32[2]{0:T(128)}, u32[]{:S(2)}) copy-start(s32[2]{0:T(128)} %refs_0_.3) | copy-start | bytes 28
  7.6 22.6 %copy-start.3 = (bf16[3072,512]{1,0:T(8,128)(2,1)S(1)}, bf16[3072,512]{1,0:T(8,128)(2,1)}, u32[]{:S(2)}) copy-start(bf16[3072,512]{1,0:T(8,128)(2,1)} %refs_1_.1) | copy-start | bytes 9437188
  22.0 12.7 %copy-start.10 = (bf16[4096]{0:T(1024)(128)(2,1)S(1)}, bf16[4096]{0:T(1024)(128)(2,1)}, u32[]{:S(2)}) copy-start(bf16[4096]{0:T(1024)(128)(2,1)} %param.32) | copy-start | bytes 24580
  31.3 9.2 %all-to-all-start.2 = ((bf16[8,8,512]{2,1,0:T(8,128)(2,1)}), bf16[8,8,512]{2,1,0:T(8,128)(2,1)S(1)}, u32[]{:S(2)}, u32[]{:S(2)}) async-start(bf16[8,8,512]{2,1,0:T(8,128)(2,1)} %output.1.after_ref), calls=%async_computation.2 | async-start | bytes 131072 | tf_op jit(solution)/shard_map/all_to_all | solution.py:365
  40.6 4.2 %copy-start = (bf16[4096,1376]{0,1:T(8,128)(2,1)S(1)}, bf16[4096,1376]{0,1:T(8,128)(2,1)}, u32[]{:S(2)}) copy-start(bf16[4096,1376]{0,1:T(8,128)(2,1)} %param.33) | copy-start | bytes 33816580
  44.8 4.2 %copy-start.1 = (bf16[4096,1376]{0,1:T(8,128)(2,1)S(1)}, bf16[4096,1376]{0,1:T(8,128)(2,1)}, u32[]{:S(2)}) copy-start(bf16[4096,1376]{0,1:T(8,128)(2,1)} %param.34) | copy-start | bytes 33816580
  49.0 4.2 %copy-start.2 = (bf16[1376,4096]{1,0:T(8,128)(2,1)S(1)}, bf16[1376,4096]{1,0:T(8,128)(2,1)}, u32[]{:S(2)}) copy-start(bf16[1376,4096]{1,0:T(8,128)(2,1)} %down_ref.1) | copy-start | bytes 33816580

commit v2 on v1

--- a/solution.py
+++ b/solution.py
@@ -163,13 +163,20 @@
     )
 
 
+def spread(gain_ref):
+    rows = gain_ref[...].astype(F32)
+    return jnp.concatenate([rows[i : i + 1] for i in range(rows.shape[0])], axis=1)
+
+
 def project_kernel(
-    seq_dev, own_ref, other_ref, gain_ref, wq, wk, wd, wv, wg, send_ref, bq, bk, bd, bv, bg, acc, sems
+    seq_dev, own_hbm, other_ref, gain_hbm, wq, wk, wd, wv, wg, send_ref, own_ref, gain_ref, bq, bk, bd, bv, bg, acc, sems
 ):
-    pairs = ((wq, bq), (wk, bk), (wd, bd), (wv, bv), (wg, bg))
+    pairs = ((own_hbm, own_ref), (gain_hbm, gain_ref), (wq, bq), (wk, bk), (wd, bd), (wv, bv), (wg, bg))
     copies = [pltpu.make_async_copy(src, dst, sems.at[i]) for i, (src, dst) in enumerate(pairs)]
     for copy in copies:
         copy.start()
+    copies[0].wait()
+    copies[1].wait()
     own = own_ref[...].astype(F32)
     other = other_ref[...].astype(F32)
     first = lax.axis_index("tp") == 0
@@ -177,9 +184,9 @@
     high = jnp.where(first, other, own)
     block = jnp.concatenate([low, high], axis=1)
     total = jnp.sum(block * block, axis=1, keepdims=True)
-    scaled = (block * gain_ref[...].astype(F32)).astype(BF16)
+    scaled = (block * spread(gain_ref)).astype(BF16)
     at = 0
-    for copy, (_, buf) in zip(copies, pairs):
+    for copy, (_, buf) in zip(copies[2:], pairs[2:]):
         copy.wait()
         acc[:, at : at + buf.shape[1]] = jnp.dot(scaled, buf[...], preferred_element_type=F32)
         at += buf.shape[1]
@@ -261,7 +268,7 @@
         out_ref[i] = heads
 
 
-def output_kernel(n_tp, recv_ref, weight_ref, own_ref, out_ref, rows_ref):
+def output_kernel(n_tp, recv_ref, weight_ref, own_ref, out_ref, after_ref, rows_ref):
     seq_dev, wide = recv_ref.shape[1], recv_ref.shape[2]
     for i in range(recv_ref.shape[0]):
         kv_at, tp_at = divmod(i, n_tp)
@@ -270,6 +277,7 @@
         ].astype(F32)
     projected = jnp.dot(rows_ref[...].astype(BF16), weight_ref[...], preferred_element_type=F32)
     after = (own_ref[...].astype(F32) + projected).astype(BF16)
+    after_ref[...] = after
     for i in range(out_ref.shape[0]):
         out_ref[i] = after
 
@@ -277,7 +285,7 @@
 def feed_kernel(recv_ref, gain_ref, gate_ref, up_ref, down_ref, out_ref):
     whole = jnp.concatenate([recv_ref[i].astype(F32) for i in range(recv_ref.shape[0])], axis=1)
     inv = lax.rsqrt(jnp.mean(whole * whole, axis=1, keepdims=True) + EPS)
-    normed = (whole * inv * gain_ref[...].astype(F32)).astype(BF16)
+    normed = (whole * inv * spread(gain_ref)).astype(BF16)
     contract = (((1,), (1,)), ((), ()))
     gate = lax.dot_general(normed, gate_ref[...], contract, preferred_element_type=F32)
     up = lax.dot_general(normed, up_ref[...], contract, preferred_element_type=F32)
@@ -289,7 +297,7 @@
 
 
 def finish_kernel(recv_ref, after_ref, out_ref):
-    total = after_ref[0].astype(F32)
+    total = after_ref[...].astype(F32)
     for i in range(recv_ref.shape[0]):
         total = total + recv_ref[i].astype(F32)
     out_ref[...] = total.astype(BF16)
@@ -331,14 +339,15 @@
     send = call(
         lambda *refs: project_kernel(seq_dev, *refs),
         jax.ShapeDtypeStruct((n_kv, seq_dev, wide), BF16),
-        [vmem_spec()] * 3 + [anywhere] * 5,
-        [pltpu.VMEM(w.shape, BF16) for w in weights]
-        + [pltpu.VMEM((rows, wide), F32), pltpu.SemaphoreType.DMA((5,))],
+        [anywhere, vmem_spec()] + [anywhere] * 6,
+        [pltpu.VMEM(tokens.shape, BF16), pltpu.VMEM((attn_gain.size // LANES, LANES), BF16)]
+        + [pltpu.VMEM(w.shape, BF16) for w in weights]
+        + [pltpu.VMEM((rows, wide), F32), pltpu.SemaphoreType.DMA((7,))],
         16 * MIB,
-        rows * moved,
+        10**10,
         moved,
         "project",
-    )(tokens, other, attn_gain.reshape(1, -1), *(in_hbm(w) for w in weights))
+    )(in_hbm(tokens), other, in_hbm(attn_gain.reshape(-1, LANES)), *(in_hbm(w) for w in weights))
     recv = lax.all_to_all(send, "kv", 0, 0, tiled=True)
     moved = state.size * 4 + cache_rates.size * 8
     send = call(
@@ -347,22 +356,22 @@
         [pl.BlockSpec(memory_space=pltpu.SMEM)] + [vmem_spec()] * 6,
         [pltpu.VMEM((seq_dev, heads_dev * value_dim), F32)],
         4 * MIB,
-        state.size * 16,
+        4 * 10**10,
         moved,
         "attend",
-    )(lengths, recv, in_vmem(state), in_vmem(cache_keys), in_vmem(cache_values), in_vmem(cache_rates), head_gain)
+    )(lengths, recv, in_vmem(state), in_vmem(cache_keys), in_vmem(cache_values), in_vmem(cache_rates), in_vmem(head_gain))
     recv = lax.all_to_all(send, ("kv", "tp"), 0, 0, tiled=True)
-    after = call(
+    send, after = call(
         lambda *refs: output_kernel(n_tp, *refs),
-        jax.ShapeDtypeStruct((members, rows, columns), BF16),
+        (jax.ShapeDtypeStruct((members, rows, columns), BF16), jax.ShapeDtypeStruct((rows, columns), BF16)),
         [vmem_spec()] * 3,
         [pltpu.VMEM((rows, w_out.shape[0]), F32)],
         2 * MIB,
-        rows * w_out.size * 2,
+        10**6,
         w_out.size * 2,
         "output",
-    )(recv, in_vmem(w_out), tokens)
-    recv = lax.all_to_all(after, ("kv", "tp"), 0, 0, tiled=True)
+    )(recv, in_vmem(w_out), in_vmem(tokens))
+    recv = lax.all_to_all(send, ("kv", "tp"), 0, 0, tiled=True)
     moved = (w_mlp_gate.size + w_mlp_up.size + w_mlp_down.size) * 2
     send = call(
         feed_kernel,
@@ -373,7 +382,7 @@
         rows * moved,
         moved,
         "feed",
-    )(recv, mlp_gain.reshape(1, -1), in_vmem(w_mlp_gate.T), in_vmem(w_mlp_up.T), in_vmem(w_mlp_down))
+    )(recv, in_vmem(mlp_gain.reshape(-1, LANES)), in_vmem(w_mlp_gate.T), in_vmem(w_mlp_up.T), in_vmem(w_mlp_down))
     recv = lax.all_to_all(send, ("kv", "tp"), 0, 0, tiled=True)
     return call(
         finish_kernel,

time: 70.8 us -> 55.5 us (0.78)
  local copies, waits for them, and re-layouts: 14.7 us -> 0.1 us
  blocking collectives: 28.4 us -> 37.4 us
  waiting for transfers between devices: 6 us -> 1.04 us
  starting transfers between devices: 3.84 us -> 0.49 us
  Pallas kernels: 17.3 us -> 16 us
    unnamed x26 -> x36, local copies, waits for them, and re-layouts: 13.9 us -> 0.1 us
    all_to_all x2 -> x3, blocking collectives: 16.5 us -> 25.3 us  [shards(): recv = lax.all_to_all(send, ('kv', 'tp'), 0, 0, tiled=True)]
    all_to_all x1 -> x0, waiting for transfers between devices: 5.82 us -> none  [shards(): recv = lax.all_to_all(after, ('kv', 'tp'), 0, 0, tiled=True)]
    all_to_all x1 -> x0, starting transfers between devices: 3.35 us -> none  [shards(): recv = lax.all_to_all(after, ('kv', 'tp'), 0, 0, tiled=True)]
    ppermute x1, waiting for transfers between devices: 0.18 us -> 1.04 us  [shards(): other = lax.ppermute(tokens, 'tp', [(i, n_tp - 1 - i) for i in range(n_tp)])]
    reshape x2 -> x0, local copies, waits for them, and re-layouts: 0.85 us -> none  [the longest x1 0.84 us: shards(): attn_gain.reshape(1, -1)]
    pallas_call x1, Pallas kernels: 1.45 us -> 0.61 us  [shards(): call(finish_kernel, jax.ShapeDtypeStruct((rows, columns), BF16), [vmem_sp...]
  transfers between devices with their start and end apart: 2 -> 1, of which waited for: 2 -> 1; matrix products, arithmetic and copies ran while one was open for 1% -> 0% of each run, Pallas kernels for 0% -> 0%
where the time goes in v2:
time: 55.5 us; the launch traced here: 55.2 us
  blocking collectives  37.4 us (67%)
  Pallas kernels  16 us (29%)
  waiting for transfers between devices  1.04 us (2%)
    all_to_all x3, blocking collectives, shards(): recv = lax.all_to_all(send, ('kv', 'tp'), 0, 0, tiled=True)  25.3 us
    all_to_all x1, blocking collectives, shards(): recv = lax.all_to_all(send, 'kv', 0, 0, tiled=True)  12.1 us
    pallas_call x1, Pallas kernels, shards(): call(feed_kernel, jax.ShapeDtypeStruct((members, rows, columns), BF16), [...  7.45 us
    pallas_call x1, Pallas kernels, shards(): call(lambda *refs: project_kernel(seq_dev, *refs), jax.ShapeDtypeStruct((...  5.01 us
    pallas_call x1, Pallas kernels, shards(): call(lambda *refs: attend_kernel(width, *refs), jax.ShapeDtypeStruct((mem...  2.36 us
  transfers between devices with their start and end apart: 1, of which 1 were waited for; matrix products, arithmetic and copies ran while one was open for 0% of the time, Pallas kernels for 0%

profile of v2, /device:TPU:0, one launch (start us, length us, event | category | flops | bytes accessed | tf_op | source)
XLA Modules:
  0.0 55.2 jit_solution(10329643841440939816)
XLA Ops:
  0.0 0.5 collective-permute-start
  0.5 1.0 %collective-permute-done.refs_1_ = bf16[8,512]{1,0:T(8,128)(2,1)S(1)} collective-permute-done((bf16[8,512]{1,0:T(8,128)(2,1)}, bf16[8,512]{1,0:T(8,128)(2,1)S(1)}, u32[]{:S(2)}, u32[]{:S(2)}) %collective-permute-start) | collective-permute-done | bytes 8224 | tf_op jit(solution)/shard_map/ppermute | solution.py:334
  1.5 0.0 copy-start.8
  1.6 5.0 %project.1 = bf16[4,2,5504]{2,1,0:T(2,128)(2,1)S(1)} custom-call(bf16[8,512]{1,0:T(8,128)(2,1)} %refs_2_.3, bf16[8,512]{1,0:T(8,128)(2,1)S(1)} %collective-permute-done.refs_1_, bf16[8,128]{1,0:T(8,128)(2,1)} %bitcast.13, bf16[1024,768]{1,0:T(8,128)(2,1)} %refs_3_.2, bf16[1024,768]{1,0:T(8,128)(2,1)} %refs_4_.2, bf16[1024,768]{1,0:T(8,128)(2,1)} %refs_5_.2, ...), custom_call_target="tpu_custom_call" | custom-call | flops 10000000000 | bytes 11010048 | tf_op jit(solution)/shard_map/project/pallas_call | solution.py:339
  6.6 0.0 slice-start
  6.6 0.0 slice-start.3
  6.6 0.0 slice-start.6
  6.6 12.1 %all_to_all.20.refs_1_ = bf16[4,2,5504]{2,1,0:T(2,128)(2,1)S(1)} all-to-all(bf16[4,2,5504]{2,1,0:T(2,128)(2,1)S(1)} %project.1), channel_id=1, replica_groups=mesh['dp'=4,'kv'=4,'tp'=2] {'kv'}, dimensions={0} | all-to-all | bytes 176128 | tf_op jit(solution)/shard_map/all_to_all | solution.py:351
  18.7 0.0 copy-done.4
  18.7 0.0 copy-start
  18.7 0.0 copy-start.1
  18.7 0.0 slice-start.1
  18.8 0.0 slice-start.2
  18.8 0.0 slice-start.4
  18.8 0.0 slice-start.5
  18.8 0.0 slice-start.7
  18.8 0.0 slice-start.8
  18.8 2.4 %attend.1 = bf16[8,2,1536]{2,1,0:T(2,128)(2,1)S(1)} custom-call(s32[2]{0:T(128)S(1)} %copy-done.8, bf16[4,2,5504]{2,1,0:T(2,128)(2,1)S(1)} %all_to_all.20.refs_1_, f32[2,2,384,768]{3,2,1,0:T(8,128)S(1)} %copy-done.3, bf16[2,2,64,384]{3,2,1,0:T(8,128)(2,1)S(1)} %copy-done.6, bf16[2,2,64,768]{3,2,1,0:T(8,128)(2,1)S(1)} %copy-done.4, ...), custom_call_target="tpu_custom_call" | custom-call | flops 40000000000 | bytes 5505024 | tf_op jit(solution)/shard_map/attend/pallas_call | solution.py:353
  21.2 0.0 copy-start.2
  21.2 8.7 %all_to_all.21.refs_0_ = bf16[8,2,1536]{2,1,0:T(2,128)(2,1)S(1)} all-to-all(bf16[8,2,1536]{2,1,0:T(2,128)(2,1)S(1)} %attend.1), channel_id=1, replica_groups=mesh['dp'=4,'kv'=4,'tp'=2] {'kv','tp'}, dimensions={0} | all-to-all | bytes 98304 | tf_op jit(solution)/shard_map/all_to_all | solution.py:363
  29.9 0.0 copy-done.1
  29.9 0.5 output.1
  30.5 8.3 %all_to_all.22.recv_ref = bf16[8,8,512]{2,1,0:T(8,128)(2,1)S(1)} all-to-all(bf16[8,8,512]{2,1,0:T(8,128)(2,1)S(1)} %get-tuple-element.7), channel_id=1, replica_groups=mesh['dp'=4,'kv'=4,'tp'=2] {'kv','tp'}, dimensions={0} | all-to-all | bytes 131072 | tf_op jit(solution)/shard_map/all_to_all | solution.py:374
  38.8 0.0 slice-done.6
  38.8 0.0 slice-done.1
  38.8 0.0 slice-done.2
  38.8 0.0 slice-done.4
  38.8 0.0 slice-done.5
  38.8 0.0 slice-done.7
  38.9 7.5 %feed.1 = bf16[8,8,512]{2,1,0:T(8,128)(2,1)S(1)} custom-call(bf16[8,8,512]{2,1,0:T(8,128)(2,1)S(1)} %all_to_all.22.recv_ref, bf16[32,128]{1,0:T(8,128)(2,1)S(1)} %bitcast.12, bf16[1376,4096]{1,0:T(8,128)(2,1)S(1)} %bitcast.6, bf16[1376,4096]{1,0:T(8,128)(2,1)S(1)} %bitcast.9, bf16[1376,4096]{1,0:T(8,128)(2,1)S(1)} %bitcast.11), custom_call_target="tpu_custom_call" | custom-call | flops 270532608 | bytes 33816576 | tf_op jit(solution)/shard_map/feed/pallas_call | solution.py:376
  46.3 8.3 %all_to_all.23.recv_ref = bf16[8,8,512]{2,1,0:T(8,128)(2,1)S(1)} all-to-all(bf16[8,8,512]{2,1,0:T(8,128)(2,1)S(1)} %feed.1), channel_id=1, replica_groups=mesh['dp'=4,'kv'=4,'tp'=2] {'kv','tp'}, dimensions={0} | all-to-all | bytes 131072 | tf_op jit(solution)/shard_map/all_to_all | solution.py:386
  54.6 0.6 %finish.1 = bf16[8,512]{1,0:T(8,128)(2,1)} custom-call(bf16[8,8,512]{2,1,0:T(8,128)(2,1)S(1)} %all_to_all.23.recv_ref, bf16[8,512]{1,0:T(8,128)(2,1)S(1)} %get-tuple-element.8.after_ref), custom_call_target="tpu_custom_call" | custom-call | flops 32768 | bytes 65536 | tf_op jit(solution)/shard_map/finish/pallas_call | solution.py:387
  (18 shorter events, 0.0 us)
Async XLA Ops:
  0.0 1.5 %collective-permute-start = (bf16[8,512]{1,0:T(8,128)(2,1)}, bf16[8,512]{1,0:T(8,128)(2,1)S(1)}, u32[]{:S(2)}, u32[]{:S(2)}) collective-permute-start(bf16[8,512]{1,0:T(8,128)(2,1)} %refs_2_.3), channel_id=1, source_target_pairs={{0,1},{1,0},{2,3},{3,2},{4,5},{5,4},{6,7},{7,6},{8,9},{9,8},{10,11... | collective-permute-start | bytes 24584 | tf_op jit(solution)/shard_map/ppermute | solution.py:334
  1.5 17.2 %copy-start.3 = (f32[2,2,384,768]{3,2,1,0:T(8,128)S(1)}, f32[2,2,384,768]{3,2,1,0:T(8,128)}, u32[]{:S(2)}) copy-start(f32[2,2,384,768]{3,2,1,0:T(8,128)} %refs_2_.2) | copy-start | bytes 14155780
  1.5 17.2 %copy-start.4 = (bf16[2,2,64,768]{3,2,1,0:T(8,128)(2,1)S(1)}, bf16[2,2,64,768]{3,2,1,0:T(8,128)(2,1)}, u32[]{:S(2)}) copy-start(bf16[2,2,64,768]{3,2,1,0:T(8,128)(2,1)} %refs_4_.3) | copy-start | bytes 1179652
  1.5 17.2 %copy-start.5 = (f32[2,2,64,384]{3,2,1,0:T(8,128)S(1)}, f32[2,2,64,384]{3,2,1,0:T(8,128)}, u32[]{:S(2)}) copy-start(f32[2,2,64,384]{3,2,1,0:T(8,128)} %refs_5_.3) | copy-start | bytes 1179652
  1.5 17.2 %copy-start.6 = (bf16[2,2,64,384]{3,2,1,0:T(8,128)(2,1)S(1)}, bf16[2,2,64,384]{3,2,1,0:T(8,128)(2,1)}, u32[]{:S(2)}) copy-start(bf16[2,2,64,384]{3,2,1,0:T(8,128)(2,1)} %refs_3_.3) | copy-start | bytes 589828
  1.5 17.2 %copy-start.7 = (bf16[2,768]{1,0:T(2,128)(2,1)S(1)}, bf16[2,768]{1,0:T(2,128)(2,1)}, u32[]{:S(2)}) copy-start(bf16[2,768]{1,0:T(2,128)(2,1)} %refs_6_.3) | copy-start | bytes 9220
  1.5 17.2 %copy-start.8 = (s32[2]{0:T(128)S(1)}, s32[2]{0:T(128)}, u32[]{:S(2)}) copy-start(s32[2]{0:T(128)} %refs_0_.3) | copy-start | bytes 28
  6.6 32.2 %slice-start = ((s8[11272192]{0:T(1024)(128)(4,1)}), s8[4194304]{0:T(1024)(128)(4,1)S(1)}, s32[]{:S(2)}) async-start(s8[11272192]{0:T(1024)(128)(4,1)} %bitcast.4), calls=%async_computation.4 | async-start | bytes 8388608
  6.6 32.2 %slice-start.3 = ((s8[11272192]{0:T(1024)(128)(4,1)}), s8[4194304]{0:T(1024)(128)(4,1)S(1)}, s32[]{:S(2)}) async-start(s8[11272192]{0:T(1024)(128)(4,1)} %bitcast.7), calls=%async_computation.7 | async-start | bytes 8388608
  6.6 32.2 %slice-start.6 = ((s8[11272192]{0:T(1024)(128)(4,1)}), s8[4194304]{0:T(1024)(128)(4,1)S(1)}, s32[]{:S(2)}) async-start(s8[11272192]{0:T(1024)(128)(4,1)} %bitcast.10), calls=%async_computation.10 | async-start | bytes 8388608
  18.7 11.2 %copy-start = (bf16[3072,512]{1,0:T(8,128)(2,1)S(1)}, bf16[3072,512]{1,0:T(8,128)(2,1)}, u32[]{:S(2)}) copy-start(bf16[3072,512]{1,0:T(8,128)(2,1)} %refs_1_.1) | copy-start | bytes 9437188
  18.7 11.2 %copy-start.1 = (bf16[8,512]{1,0:T(8,128)(2,1)S(1)}, bf16[8,512]{1,0:T(8,128)(2,1)}, u32[]{:S(2)}) copy-start(bf16[8,512]{1,0:T(8,128)(2,1)} %refs_2_.3) | copy-start | bytes 24580
  18.7 20.0 %slice-start.1 = ((s8[11272192]{0:T(1024)(128)(4,1)}), s8[4194304]{0:T(1024)(128)(4,1)S(1)}, s32[]{:S(2)}) async-start(s8[11272192]{0:T(1024)(128)(4,1)} %bitcast.4), calls=%async_computation.5 | async-start | bytes 8388608
  18.8 20.0 %slice-start.2 = ((s8[11272192]{0:T(1024)(128)(4,1)}), s8[2883584]{0:T(1024)(128)(4,1)S(1)}, s32[]{:S(2)}) async-start(s8[11272192]{0:T(1024)(128)(4,1)} %bitcast.4), calls=%async_computation.6 | async-start | bytes 5767168
  18.8 20.0 %slice-start.4 = ((s8[11272192]{0:T(1024)(128)(4,1)}), s8[4194304]{0:T(1024)(128)(4,1)S(1)}, s32[]{:S(2)}) async-start(s8[11272192]{0:T(1024)(128)(4,1)} %bitcast.7), calls=%async_computation.8 | async-start | bytes 8388608
  18.8 20.0 %slice-start.5 = ((s8[11272192]{0:T(1024)(128)(4,1)}), s8[2883584]{0:T(1024)(128)(4,1)S(1)}, s32[]{:S(2)}) async-start(s8[11272192]{0:T(1024)(128)(4,1)} %bitcast.7), calls=%async_computation.9 | async-start | bytes 5767168
  18.8 20.0 %slice-start.7 = ((s8[11272192]{0:T(1024)(128)(4,1)}), s8[4194304]{0:T(1024)(128)(4,1)S(1)}, s32[]{:S(2)}) async-start(s8[11272192]{0:T(1024)(128)(4,1)} %bitcast.10), calls=%async_computation.11 | async-start | bytes 8388608
  18.8 20.0 %slice-start.8 = ((s8[11272192]{0:T(1024)(128)(4,1)}), s8[2883584]{0:T(1024)(128)(4,1)S(1)}, s32[]{:S(2)}) async-start(s8[11272192]{0:T(1024)(128)(4,1)} %bitcast.10), calls=%async_computation.12 | async-start | bytes 5767168
  21.2 17.6 %copy-start.2 = (bf16[4096]{0:T(1024)(128)(2,1)S(1)}, bf16[4096]{0:T(1024)(128)(2,1)}, u32[]{:S(2)}) copy-start(bf16[4096]{0:T(1024)(128)(2,1)} %param.32) | copy-start | bytes 24580

commit v3 on v2

--- a/solution.py
+++ b/solution.py
@@ -168,9 +168,24 @@
     return jnp.concatenate([rows[i : i + 1] for i in range(rows.shape[0])], axis=1)
 
 
+def by_partner(block, seq_dev, n_kv):
+    me = lax.axis_index("kv")
+    place = lax.broadcasted_iota(jnp.int32, block.shape, 0) // seq_dev
+    rows = block.shape[0]
+    bit = 1
+    while bit < n_kv:
+        down = pltpu.roll(block, bit * seq_dev, 0)
+        up = pltpu.roll(block, rows - bit * seq_dev, 0)
+        swapped = jnp.where((place & bit) == 0, up, down)
+        block = jnp.where((me & bit) == 0, block, swapped)
+        bit *= 2
+    return block
+
+
 def project_kernel(
-    seq_dev, own_hbm, other_ref, gain_hbm, wq, wk, wd, wv, wg, send_ref, own_ref, gain_ref, bq, bk, bd, bv, bg, acc, sems
+    seq_dev, own_hbm, other_ref, gain_hbm, wq, wk, wd, wv, wg, *rest
 ):
+    out_refs, (own_ref, gain_ref, bq, bk, bd, bv, bg, acc, sems) = rest[:-9], rest[-9:]
     pairs = ((own_hbm, own_ref), (gain_hbm, gain_ref), (wq, bq), (wk, bk), (wd, bd), (wv, bv), (wg, bg))
     copies = [pltpu.make_async_copy(src, dst, sems.at[i]) for i, (src, dst) in enumerate(pairs)]
     for copy in copies:
@@ -182,7 +197,7 @@
     first = lax.axis_index("tp") == 0
     low = jnp.where(first, own, other)
     high = jnp.where(first, other, own)
-    block = jnp.concatenate([low, high], axis=1)
+    block = by_partner(jnp.concatenate([low, high], axis=1), seq_dev, len(out_refs))
     total = jnp.sum(block * block, axis=1, keepdims=True)
     scaled = (block * spread(gain_ref)).astype(BF16)
     at = 0
@@ -194,8 +209,8 @@
     upper = total.astype(BF16).astype(F32)
     lower = total - upper
     acc[:, at : at + LANES] = jnp.where(lane == 0, upper, jnp.where(lane == 1, lower, 0.0))
-    for i in range(send_ref.shape[0]):
-        send_ref[i] = acc[i * seq_dev : (i + 1) * seq_dev, :].astype(BF16)
+    for step, out_ref in enumerate(out_refs):
+        out_ref[...] = acc[step * seq_dev : (step + 1) * seq_dev, :].astype(out_ref.dtype)
 
 
 def split_rows(row):
@@ -208,14 +223,34 @@
     return jnp.where(at == 0, upper, jnp.where(at == 1, lower, 0.0)).astype(BF16)
 
 
-def attend_kernel(
-    width, lengths_ref, recv_ref, state_ref, keys_ref, values_ref, rates_ref, gain_ref, out_ref, heads_ref
-):
+def gather_kernel(lengths_ref, _, state_ref, keys_ref, values_ref, rates_ref, mixed_ref, total_ref):
     seq_dev, heads_dev, key_dim, value_dim = state_ref.shape
     span = keys_ref.shape[2]
-    got = recv_ref[0].astype(F32)
-    for i in range(1, recv_ref.shape[0]):
-        got = got + recv_ref[i].astype(F32)
+    row_at = lax.broadcasted_iota(jnp.int32, (span, span), 0)
+    col_at = lax.broadcasted_iota(jnp.int32, (span, span), 1)
+    upto = jnp.where(col_at <= row_at, 1.0, 0.0).astype(BF16)
+    slot = lax.broadcasted_iota(jnp.int32, (span, 1), 0)
+    for s in range(seq_dev):
+        live = (slot < lengths_ref[s]).astype(F32)
+        for h in range(heads_dev):
+            rates = rates_ref[s, h] * live
+            upper = rates.astype(BF16)
+            lower = (rates - upper.astype(F32)).astype(BF16)
+            running = jnp.dot(upto, upper, preferred_element_type=F32)
+            running = running + jnp.dot(upto, lower, preferred_element_type=F32)
+            total_ref[s : s + 1, h * key_dim : (h + 1) * key_dim] = running[span - 1 :]
+            grown = (jnp.exp(running) * keys_ref[s, h].astype(F32) * live).astype(BF16)
+            added = lax.dot_general(
+                grown, values_ref[s, h], (((0,), (0,)), ((), ())), preferred_element_type=F32
+            )
+            mixed_ref[s, h] = (state_ref[s, h] + added).astype(BF16)
+
+
+def attend_kernel(width, parts, mixed_ref, total_ref, gain_ref, out_ref, heads_ref):
+    seq_dev, heads_dev, key_dim, value_dim = mixed_ref.shape
+    got = parts[0][...]
+    for part in parts[1:]:
+        got = got + part[...].astype(F32)
     keys_all, values_all = heads_dev * key_dim, heads_dev * value_dim
     ends = [0, keys_all, 2 * keys_all, 3 * keys_all]
     ends += [ends[3] + values_all, ends[3] + 2 * values_all]
@@ -227,43 +262,23 @@
     log_decay = (jnp.minimum(raw, 0.0) - jnp.log(1.0 + jnp.exp(-jnp.abs(raw)))) / GATE_NORM
     value_new = got[:, ends[3] : ends[4]] * inv_rms
     gate = got[:, ends[4] : ends[5]] * inv_rms
-    decayed = query * jnp.exp(log_decay)
+    gate = gate / (1.0 + jnp.exp(-gate))
+    decayed = query * jnp.exp(log_decay - total_ref[...])
     product = query * key_new
-    row_at = lax.broadcasted_iota(jnp.int32, (span, span), 0)
-    col_at = lax.broadcasted_iota(jnp.int32, (span, span), 1)
-    later = jnp.where(col_at > row_at, 1.0, 0.0).astype(BF16)
-    slot_col = lax.broadcasted_iota(jnp.int32, (span, 1), 0)
-    slot_row = lax.broadcasted_iota(jnp.int32, (1, span), 1)
     for s in range(seq_dev):
-        live_col = (slot_col < lengths_ref[s]).astype(F32)
-        live_row = (slot_row < lengths_ref[s]).astype(F32)
         for h in range(heads_dev):
             ks, vs = slice(h * key_dim, (h + 1) * key_dim), slice(h * value_dim, (h + 1) * value_dim)
-            rates = rates_ref[s, h] * live_col
-            upper = rates.astype(BF16)
-            lower = (rates - upper.astype(F32)).astype(BF16)
-            after = jnp.dot(later, upper, preferred_element_type=F32)
-            after = after + jnp.dot(later, lower, preferred_element_type=F32)
-            total = jnp.sum(rates, axis=0, keepdims=True)
-            weighted = jnp.exp(-after) * keys_ref[s, h].astype(F32)
-            w_upper = weighted.astype(BF16)
-            w_lower = (weighted - w_upper.astype(F32)).astype(BF16)
-            row = decayed[s : s + 1, ks]
-            rows = split_rows(row)
-            contract = (((1,), (1,)), ((), ()))
-            scores = lax.dot_general(rows, w_upper, contract, preferred_element_type=F32)
-            scores = scores + lax.dot_general(rows, w_lower, contract, preferred_element_type=F32)
-            scores = jnp.sum(scores, axis=0, keepdims=True) * live_row
-            state_rows = split_rows(row * jnp.exp(-total))
-            mixed = jnp.dot(state_rows, state_ref[s, h].astype(BF16), preferred_element_type=F32)
-            mixed = mixed + jnp.dot(split_rows(scores), values_ref[s, h], preferred_element_type=F32)
+            rows = split_rows(decayed[s : s + 1, ks])
+            mixed = jnp.dot(rows, mixed_ref[s, h], preferred_element_type=F32)
             own = jnp.sum(product[s : s + 1, ks], axis=1, keepdims=True)
-            attended = jnp.sum(mixed, axis=0, keepdims=True) + own * value_new[s : s + 1, vs]
-            scale = lax.rsqrt(jnp.mean(attended * attended, axis=1, keepdims=True) + EPS)
-            normed = attended * scale * gain_ref[h : h + 1, :].astype(F32)
-            opened = gate[s : s + 1, vs]
-            heads_ref[s : s + 1, vs] = opened / (1.0 + jnp.exp(-opened)) * normed
-    heads = heads_ref[...].astype(BF16)
+            heads_ref[s : s + 1, vs] = jnp.sum(mixed, axis=0, keepdims=True) + own * value_new[s : s + 1, vs]
+    pieces = []
+    for h in range(heads_dev):
+        vs = slice(h * value_dim, (h + 1) * value_dim)
+        attended = heads_ref[:, vs]
+        scale = lax.rsqrt(jnp.mean(attended * attended, axis=1, keepdims=True) + EPS)
+        pieces.append(gate[:, vs] * (attended * scale * gain_ref[h : h + 1, :].astype(F32)))
+    heads = jnp.concatenate(pieces, axis=1).astype(BF16)
     for i in range(out_ref.shape[0]):
         out_ref[i] = heads
 
@@ -282,18 +297,38 @@
         out_ref[i] = after
 
 
-def feed_kernel(recv_ref, gain_ref, gate_ref, up_ref, down_ref, out_ref):
-    whole = jnp.concatenate([recv_ref[i].astype(F32) for i in range(recv_ref.shape[0])], axis=1)
-    inv = lax.rsqrt(jnp.mean(whole * whole, axis=1, keepdims=True) + EPS)
-    normed = (whole * inv * spread(gain_ref)).astype(BF16)
+def feed_kernel(cut, recv_ref, gain_ref, gate_ref, up_ref, down_ref, out_ref, gate_cols, up_cols):
+    members, rows, columns = recv_ref.shape
     contract = (((1,), (1,)), ((), ()))
-    gate = lax.dot_general(normed, gate_ref[...], contract, preferred_element_type=F32)
-    up = lax.dot_general(normed, up_ref[...], contract, preferred_element_type=F32)
-    hidden = (gate / (1.0 + jnp.exp(-gate)) * up).astype(BF16)
-    columns = out_ref.shape[2]
-    for i in range(out_ref.shape[0]):
-        piece = down_ref[:, i * columns : (i + 1) * columns]
-        out_ref[i] = jnp.dot(hidden, piece, preferred_element_type=F32).astype(BF16)
+    squares = 0.0
+    gain = spread(gain_ref)
+    sums = [0.0, 0.0]
+    group = 1
+    for k in range(members // group):
+        pieces = []
+        for i in range(k * group, (k + 1) * group):
+            piece = recv_ref[i].astype(F32)
+            squares = squares + jnp.sum(piece * piece, axis=1, keepdims=True)
+            pieces.append((piece * gain[:, i * columns : (i + 1) * columns]).astype(BF16))
+        scaled = jnp.concatenate(pieces, axis=1)
+        at = slice(k * group * columns, (k + 1) * group * columns)
+        for j, (weight, cols) in enumerate(((gate_ref, gate_cols), (up_ref, up_cols))):
+            tall = lax.dot_general(weight[:cut, at], scaled, contract, preferred_element_type=F32)
+            cols[...] = tall if k == 0 else cols[...] + tall
+            sums[j] = sums[j] + lax.dot_general(scaled, weight[cut:, at], contract, preferred_element_type=F32)
+    inv = lax.rsqrt(squares / (members * columns) + EPS)
+    inv_row = jnp.transpose(jnp.broadcast_to(inv, (rows, LANES)))[:1]
+    gate = gate_cols[...] * inv_row
+    tall = (gate / (1.0 + jnp.exp(-gate)) * (up_cols[...] * inv_row)).astype(BF16)
+    gate = sums[0] * inv
+    flat = (gate / (1.0 + jnp.exp(-gate)) * (sums[1] * inv)).astype(BF16)
+    for i in range(members):
+        at = slice(i * columns, (i + 1) * columns)
+        share = lax.dot_general(
+            tall, down_ref[:cut, at], (((0,), (0,)), ((), ())), preferred_element_type=F32
+        )
+        share = share + jnp.dot(flat, down_ref[cut:, at], preferred_element_type=F32)
+        out_ref[i] = share.astype(BF16)
 
 
 def finish_kernel(recv_ref, after_ref, out_ref):
@@ -336,9 +371,9 @@
     anywhere = pl.BlockSpec(memory_space=pl.ANY)
     weights = (w_query, w_key, w_decay, w_value, w_gate)
     moved = sum(w.size for w in weights) * 2
-    send = call(
+    parts = call(
         lambda *refs: project_kernel(seq_dev, *refs),
-        jax.ShapeDtypeStruct((n_kv, seq_dev, wide), BF16),
+        [jax.ShapeDtypeStruct((seq_dev, wide), F32 if step == 0 else BF16) for step in range(n_kv)],
         [anywhere, vmem_spec()] + [anywhere] * 6,
         [pltpu.VMEM(tokens.shape, BF16), pltpu.VMEM((attn_gain.size // LANES, LANES), BF16)]
         + [pltpu.VMEM(w.shape, BF16) for w in weights]
@@ -348,18 +383,34 @@
         moved,
         "project",
     )(in_hbm(tokens), other, in_hbm(attn_gain.reshape(-1, LANES)), *(in_hbm(w) for w in weights))
-    recv = lax.all_to_all(send, "kv", 0, 0, tiled=True)
-    moved = state.size * 4 + cache_rates.size * 8
+    parts = list(parts)
+    own = parts[0]
+    for step in range(1, n_kv):
+        parts[step] = lax.ppermute(parts[step], "kv", [(i, i ^ step) for i in range(n_kv)])
+    moved = state.size * 6 + cache_rates.size * 8
+    mixed, total = call(
+        gather_kernel,
+        [
+            jax.ShapeDtypeStruct(state.shape, BF16),
+            jax.ShapeDtypeStruct((seq_dev, heads_dev * key_dim), F32),
+        ],
+        [pl.BlockSpec(memory_space=pltpu.SMEM), anywhere] + [vmem_spec()] * 4,
+        [],
+        4 * MIB,
+        10**9,
+        moved,
+        "gather",
+    )(lengths, own, in_vmem(state), in_vmem(cache_keys), in_vmem(cache_values), in_vmem(cache_rates))
     send = call(
-        lambda *refs: attend_kernel(width, *refs),
+        lambda *refs: attend_kernel(width, refs[:n_kv], *refs[n_kv:]),
         jax.ShapeDtypeStruct((members, seq_dev, heads_dev * value_dim), BF16),
-        [pl.BlockSpec(memory_space=pltpu.SMEM)] + [vmem_spec()] * 6,
+        [vmem_spec()] * (n_kv + 3),
         [pltpu.VMEM((seq_dev, heads_dev * value_dim), F32)],
         4 * MIB,
         4 * 10**10,
-        moved,
+        state.size * 2,
         "attend",
-    )(lengths, recv, in_vmem(state), in_vmem(cache_keys), in_vmem(cache_values), in_vmem(cache_rates), in_vmem(head_gain))
+    )(own, *parts[:0:-1], mixed, total, in_vmem(head_gain))
     recv = lax.all_to_all(send, ("kv", "tp"), 0, 0, tiled=True)
     send, after = call(
         lambda *refs: output_kernel(n_tp, *refs),
@@ -373,11 +424,12 @@
     )(recv, in_vmem(w_out), in_vmem(tokens))
     recv = lax.all_to_all(send, ("kv", "tp"), 0, 0, tiled=True)
     moved = (w_mlp_gate.size + w_mlp_up.size + w_mlp_down.size) * 2
+    cut = w_mlp_down.shape[0] // 64 * 16
     send = call(
-        feed_kernel,
+        lambda *refs: feed_kernel(cut, *refs),
         jax.ShapeDtypeStruct((members, rows, columns), BF16),
         [vmem_spec()] * 5,
-        [],
+        [pltpu.VMEM((cut, rows), F32)] * 2,
         4 * MIB,
         rows * moved,
         moved,
@@ -420,7 +472,7 @@
     sizes = mesh.shape
 
     def body(*args):
-        fits = sizes["tp"] == 2 and args[13].shape[1] % LANES == 0
+        fits = sizes["tp"] == 2 and sizes["kv"] == 4 and args[13].shape[1] % LANES == 0
         return (shards if fits else plain_shards)(*args)
 
     return jax.shard_map(

time: 55.5 us -> 51.5 us (0.928)
  blocking collectives: 37.4 us -> 25.9 us
  starting transfers between devices: 0.49 us -> 6.14 us
  waiting for transfers between devices: 1.04 us -> 2.99 us
    all_to_all x1 -> x0, blocking collectives: 12.1 us -> none  [shards(): recv = lax.all_to_all(send, 'kv', 0, 0, tiled=True)]
    ppermute x0 -> x3, starting transfers between devices: none -> 5.64 us  [shards(): lax.ppermute(parts[step], 'kv', [(i, i ^ step) for i in range(n_kv)])]
    ppermute x0 -> x3, waiting for transfers between devices: none -> 1.95 us  [shards(): lax.ppermute(parts[step], 'kv', [(i, i ^ step) for i in range(n_kv)])]
    all_to_all x3, blocking collectives: 25.3 us -> 25.9 us  [shards(): recv = lax.all_to_all(send, ('kv', 'tp'), 0, 0, tiled=True)]
    pallas_call x3 -> x4, Pallas kernels: 14.8 us -> 14.7 us  [the longest x1 7.03 us: shards(): call(lambda *refs: feed_kernel(cut, *refs), jax.ShapeDtypeStruct((members...]
  transfers between devices with their start and end apart: 1 -> 4, of which waited for: 1 -> 2; matrix products, arithmetic and copies ran while one was open for 0% -> 0% of each run, Pallas kernels for 0% -> 4%
where the time goes in v3:
time: 51.5 us; the launch traced here: 51.2 us
  blocking collectives  25.9 us (50%)
  Pallas kernels  15.9 us (31%)
  starting transfers between devices  6.14 us (12%)
  waiting for transfers between devices  2.99 us (6%)
    all_to_all x3, blocking collectives, shards(): recv = lax.all_to_all(send, ('kv', 'tp'), 0, 0, tiled=True)  25.9 us
    pallas_call x1, Pallas kernels, shards(): call(lambda *refs: feed_kernel(cut, *refs), jax.ShapeDtypeStruct((members...  7.03 us
    ppermute x3, starting transfers between devices, shards(): lax.ppermute(parts[step], 'kv', [(i, i ^ step) for i in range(n_kv)])  5.64 us
    pallas_call x1, Pallas kernels, shards(): call(lambda *refs: project_kernel(seq_dev, *refs), [jax.ShapeDtypeStruct(...  5 us
    pallas_call x1, Pallas kernels, shards(): call(gather_kernel, [jax.ShapeDtypeStruct(state.shape, BF16), jax.ShapeDt...  2.07 us
    ppermute x3, waiting for transfers between devices, shards(): lax.ppermute(parts[step], 'kv', [(i, i ^ step) for i in range(n_kv)])  1.95 us
    ppermute x1, waiting for transfers between devices, shards(): other = lax.ppermute(tokens, 'tp', [(i, n_tp - 1 - i) for i in range(n_tp)])  1.04 us
  transfers between devices with their start and end apart: 4, of which 2 were waited for; matrix products, arithmetic and copies ran while one was open for 0% of the time, Pallas kernels for 4%

profile of v3, /device:TPU:0, one launch (start us, length us, event | category | flops | bytes accessed | tf_op | source)
XLA Modules:
  0.0 51.2 jit_solution(12248690099241224543)
XLA Ops:
  0.0 0.5 collective-permute-start
  0.5 1.0 %collective-permute-done.refs_1_ = bf16[8,512]{1,0:T(8,128)(2,1)S(1)} collective-permute-done((bf16[8,512]{1,0:T(8,128)(2,1)}, bf16[8,512]{1,0:T(8,128)(2,1)S(1)}, u32[]{:S(2)}, u32[]{:S(2)}) %collective-permute-start) | collective-permute-done | bytes 8224 | tf_op jit(solution)/shard_map/ppermute | solution.py:369
  1.5 5.0 %project.1 = (f32[2,5504]{1,0:T(2,128)S(1)}, bf16[2,5504]{1,0:T(2,128)(2,1)S(1)}, bf16[2,5504]{1,0:T(2,128)(2,1)S(1)}, bf16[2,5504]{1,0:T(2,128)(2,1)S(1)}) custom-call(bf16[8,512]{1,0:T(8,128)(2,1)} %refs_2_.1, bf16[8,512]{1,0:T(8,128)(2,1)S(1)} %collective-permute-done.refs_1_, bf16[8,128]{1,0:T(8,128)(2,1)} %bitcast.13, bf16[1024,768]{1,0:T(8,128)(2,1)} %refs_3_.1, ...), custom_call_target="tpu_custom_call" | custom-call | flops 10000000000 | bytes 11010048 | tf_op jit(solution)/shard_map/project/pallas_call | solution.py:374
  6.6 0.0 copy-start.8
  6.6 5.0 %collective-permute-start.1 = (bf16[2,5504]{1,0:T(2,128)(2,1)S(1)}, bf16[2,5504]{1,0:T(2,128)(2,1)S(1)}, u32[]{:S(2)}, u32[]{:S(2)}) collective-permute-start(bf16[2,5504]{1,0:T(2,128)(2,1)S(1)} %get-tuple-element.14), channel_id=1, source_target_pairs={{0,6},{2,4},{4,2},{6,0},{1,7},{3,5},{5,3},{7,1},{8,14},{10,12},{12... | collective-permute-start | bytes 66056 | tf_op jit(solution)/shard_map/ppermute | solution.py:389
  11.6 0.0 collective-permute-start.2
  11.6 0.6 %collective-permute-start.3 = (bf16[2,5504]{1,0:T(2,128)(2,1)S(1)}, bf16[2,5504]{1,0:T(2,128)(2,1)S(1)}, u32[]{:S(2)}, u32[]{:S(2)}) collective-permute-start(bf16[2,5504]{1,0:T(2,128)(2,1)S(1)} %get-tuple-element.16), channel_id=1, source_target_pairs={{0,2},{2,0},{4,6},{6,4},{1,3},{3,1},{5,7},{7,5},{8,10},{10,8},{12,... | collective-permute-start | bytes 66056 | tf_op jit(solution)/shard_map/ppermute | solution.py:389
  12.2 0.0 copy-done
  12.2 0.0 copy-done.2
  12.2 0.0 copy-done.3
  12.2 0.0 copy-done.4
  12.2 0.0 copy-done.7
  12.2 2.1 %gather.1 = (bf16[2,2,384,768]{3,2,1,0:T(8,128)(2,1)S(1)}, f32[2,768]{1,0:T(2,128)S(1)}) custom-call(s32[2]{0:T(128)S(1)} %copy-done.7, f32[2,5504]{1,0:T(2,128)S(1)} %get-tuple-element.13._.refs_0_, f32[2,2,384,768]{3,2,1,0:T(8,128)S(1)} %copy-done, bf16[2,2,64,384]{3,2,1,0:T(8,128)(2,1)S(1)} %copy-done.4, bf16[2,2,64,768]{3,2,1,0:T(8,128)(2,1)S(1)} %copy-done.2, ...), custom_call_target="tpu_custom_call" | custom-call | flops 1000000000 | bytes 7864320 | tf_op jit(solution)/shard_map/gather/pallas_call | solution.py:391
  14.3 0.0 collective-permute-done.1.refs_1_
  14.3 1.9 %collective-permute-done.2.refs_2_ = bf16[2,5504]{1,0:T(2,128)(2,1)S(1)} collective-permute-done((bf16[2,5504]{1,0:T(2,128)(2,1)S(1)}, bf16[2,5504]{1,0:T(2,128)(2,1)S(1)}, u32[]{:S(2)}, u32[]{:S(2)}) %collective-permute-start.2) | collective-permute-done | bytes 22048 | tf_op jit(solution)/shard_map/ppermute | solution.py:389
  16.3 0.0 collective-permute-done.3.refs_3_
  16.3 0.0 copy-start.1
  16.3 0.0 copy-start.5
  16.3 0.0 slice-start.1
  16.3 0.0 slice-start.2
  16.3 0.0 slice-start.4
  16.4 0.0 slice-start.5
  16.4 0.0 slice-start.7
  16.4 0.0 slice-start.8
  16.4 0.6 %attend.1 = bf16[8,2,1536]{2,1,0:T(2,128)(2,1)S(1)} custom-call(f32[2,5504]{1,0:T(2,128)S(1)} %get-tuple-element.13._.refs_0_, bf16[2,5504]{1,0:T(2,128)(2,1)S(1)} %collective-permute-done.1.refs_1_, bf16[2,5504]{1,0:T(2,128)(2,1)S(1)} %collective-permute-done.2.refs_2_, bf16[2,5504]{1,0:T(2,128)(2,1)S(1)} %collective-permute-done.3.refs_3_, ...), custom_call_target="tpu_custom_call" | custom-call | flops 40000000000 | bytes 2359296 | tf_op jit(solution)/shard_map/attend/pallas_call | solution.py:404
  17.0 0.0 copy-start.6
  17.0 9.2 %all_to_all.15.refs_0_ = bf16[8,2,1536]{2,1,0:T(2,128)(2,1)S(1)} all-to-all(bf16[8,2,1536]{2,1,0:T(2,128)(2,1)S(1)} %attend.1), channel_id=1, replica_groups=mesh['dp'=4,'kv'=4,'tp'=2] {'kv','tp'}, dimensions={0} | all-to-all | bytes 98304 | tf_op jit(solution)/shard_map/all_to_all | solution.py:414
  26.2 0.5 %output.1 = (bf16[8,8,512]{2,1,0:T(8,128)(2,1)S(1)}, bf16[8,512]{1,0:T(8,128)(2,1)S(1)}) custom-call(bf16[8,2,1536]{2,1,0:T(2,128)(2,1)S(1)} %all_to_all.15.refs_0_, bf16[3072,512]{1,0:T(8,128)(2,1)S(1)} %copy-done.1, bf16[8,512]{1,0:T(8,128)(2,1)S(1)} %copy-done.5), custom_call_target="tpu_custom_call" | custom-call | flops 1000000 | bytes 3145728 | tf_op jit(solution)/shard_map/output/pallas_call | solution.py:415
  26.8 8.4 %all_to_all.16.refs_0_ = bf16[8,8,512]{2,1,0:T(8,128)(2,1)S(1)} all-to-all(bf16[8,8,512]{2,1,0:T(8,128)(2,1)S(1)} %get-tuple-element.19), channel_id=1, replica_groups=mesh['dp'=4,'kv'=4,'tp'=2] {'kv','tp'}, dimensions={0} | all-to-all | bytes 131072 | tf_op jit(solution)/shard_map/all_to_all | solution.py:425
  35.3 7.0 %feed.1 = bf16[8,8,512]{2,1,0:T(8,128)(2,1)S(1)} custom-call(bf16[8,8,512]{2,1,0:T(8,128)(2,1)S(1)} %all_to_all.16.refs_0_, bf16[32,128]{1,0:T(8,128)(2,1)S(1)} %bitcast.12, bf16[1376,4096]{1,0:T(8,128)(2,1)S(1)} %bitcast.6, bf16[1376,4096]{1,0:T(8,128)(2,1)S(1)} %bitcast.9, bf16[1376,4096]{1,0:T(8,128)(2,1)S(1)} %bitcast.11), custom_call_target="tpu_custom_call" | custom-call | flops 270532608 | bytes 33816576 | tf_op jit(solution)/shard_map/feed/pallas_call | solution.py:428
  42.3 8.3 %all_to_all.17.recv_ref = bf16[8,8,512]{2,1,0:T(8,128)(2,1)S(1)} all-to-all(bf16[8,8,512]{2,1,0:T(8,128)(2,1)S(1)} %feed.1), channel_id=1, replica_groups=mesh['dp'=4,'kv'=4,'tp'=2] {'kv','tp'}, dimensions={0} | all-to-all | bytes 131072 | tf_op jit(solution)/shard_map/all_to_all | solution.py:438
  50.6 0.6 %finish.1 = bf16[8,512]{1,0:T(8,128)(2,1)} custom-call(bf16[8,8,512]{2,1,0:T(8,128)(2,1)S(1)} %all_to_all.17.recv_ref, bf16[8,512]{1,0:T(8,128)(2,1)S(1)} %get-tuple-element.20.after_ref), custom_call_target="tpu_custom_call" | custom-call | flops 32768 | bytes 65536 | tf_op jit(solution)/shard_map/finish/pallas_call | solution.py:439
  (24 shorter events, 0.0 us)
Async XLA Ops:
  0.0 1.5 %collective-permute-start = (bf16[8,512]{1,0:T(8,128)(2,1)}, bf16[8,512]{1,0:T(8,128)(2,1)S(1)}, u32[]{:S(2)}, u32[]{:S(2)}) collective-permute-start(bf16[8,512]{1,0:T(8,128)(2,1)} %refs_2_.1), channel_id=1, source_target_pairs={{0,1},{1,0},{2,3},{3,2},{4,5},{5,4},{6,7},{7,6},{8,9},{9,8},{10,11... | collective-permute-start | bytes 24584 | tf_op jit(solution)/shard_map/ppermute | solution.py:369
  1.5 10.7 %copy-start = (f32[2,2,384,768]{3,2,1,0:T(8,128)S(1)}, f32[2,2,384,768]{3,2,1,0:T(8,128)}, u32[]{:S(2)}) copy-start(f32[2,2,384,768]{3,2,1,0:T(8,128)} %state_ref.1) | copy-start | bytes 14155780
  1.5 10.7 %copy-start.2 = (bf16[2,2,64,768]{3,2,1,0:T(8,128)(2,1)S(1)}, bf16[2,2,64,768]{3,2,1,0:T(8,128)(2,1)}, u32[]{:S(2)}) copy-start(bf16[2,2,64,768]{3,2,1,0:T(8,128)(2,1)} %values_ref.1) | copy-start | bytes 1179652
  1.5 10.7 %copy-start.3 = (f32[2,2,64,384]{3,2,1,0:T(8,128)S(1)}, f32[2,2,64,384]{3,2,1,0:T(8,128)}, u32[]{:S(2)}) copy-start(f32[2,2,64,384]{3,2,1,0:T(8,128)} %rates_ref.1) | copy-start | bytes 1179652
  1.5 10.7 %copy-start.4 = (bf16[2,2,64,384]{3,2,1,0:T(8,128)(2,1)S(1)}, bf16[2,2,64,384]{3,2,1,0:T(8,128)(2,1)}, u32[]{:S(2)}) copy-start(bf16[2,2,64,384]{3,2,1,0:T(8,128)(2,1)} %keys_ref.1) | copy-start | bytes 589828
  1.5 10.7 %copy-start.7 = (s32[2]{0:T(128)S(1)}, s32[2]{0:T(128)}, u32[]{:S(2)}) copy-start(s32[2]{0:T(128)} %lengths_ref.1) | copy-start | bytes 28
  6.6 9.7 %copy-start.8 = (bf16[2,768]{1,0:T(2,128)(2,1)S(1)}, bf16[2,768]{1,0:T(2,128)(2,1)}, u32[]{:S(2)}) copy-start(bf16[2,768]{1,0:T(2,128)(2,1)} %refs_6_.3) | copy-start | bytes 9220
  6.6 7.7 %collective-permute-start.1 = (bf16[2,5504]{1,0:T(2,128)(2,1)S(1)}, bf16[2,5504]{1,0:T(2,128)(2,1)S(1)}, u32[]{:S(2)}, u32[]{:S(2)}) collective-permute-start(bf16[2,5504]{1,0:T(2,128)(2,1)S(1)} %get-tuple-element.14), channel_id=1, source_target_pairs={{0,6},{2,4},{4,2},{6,0},{1,7},{3,5},{5,3},{7,1},{8,14},{10,12},{12... | collective-permute-start | bytes 66056 | tf_op jit(solution)/shard_map/ppermute | solution.py:389
  11.6 4.7 %collective-permute-start.2 = (bf16[2,5504]{1,0:T(2,128)(2,1)S(1)}, bf16[2,5504]{1,0:T(2,128)(2,1)S(1)}, u32[]{:S(2)}, u32[]{:S(2)}) collective-permute-start(bf16[2,5504]{1,0:T(2,128)(2,1)S(1)} %get-tuple-element.15), channel_id=1, source_target_pairs={{0,4},{2,6},{4,0},{6,2},{1,5},{3,7},{5,1},{7,3},{8,12},{10,14},{12... | collective-permute-start | bytes 66056 | tf_op jit(solution)/shard_map/ppermute | solution.py:389
  11.6 4.7 %collective-permute-start.3 = (bf16[2,5504]{1,0:T(2,128)(2,1)S(1)}, bf16[2,5504]{1,0:T(2,128)(2,1)S(1)}, u32[]{:S(2)}, u32[]{:S(2)}) collective-permute-start(bf16[2,5504]{1,0:T(2,128)(2,1)S(1)} %get-tuple-element.16), channel_id=1, source_target_pairs={{0,2},{2,0},{4,6},{6,4},{1,3},{3,1},{5,7},{7,5},{8,10},{10,8},{12,... | collective-permute-start | bytes 66056 | tf_op jit(solution)/shard_map/ppermute | solution.py:389
  16.3 18.9 %slice-start = ((s8[11272192]{0:T(1024)(128)(4,1)}), s8[4194304]{0:T(1024)(128)(4,1)S(1)}, s32[]{:S(2)}) async-start(s8[11272192]{0:T(1024)(128)(4,1)} %bitcast.4), calls=%async_computation.3 | async-start | bytes 8388608
  16.3 18.9 %slice-start.3 = ((s8[11272192]{0:T(1024)(128)(4,1)}), s8[4194304]{0:T(1024)(128)(4,1)S(1)}, s32[]{:S(2)}) async-start(s8[11272192]{0:T(1024)(128)(4,1)} %bitcast.7), calls=%async_computation.6 | async-start | bytes 8388608
  16.3 18.9 %slice-start.6 = ((s8[11272192]{0:T(1024)(128)(4,1)}), s8[4194304]{0:T(1024)(128)(4,1)S(1)}, s32[]{:S(2)}) async-start(s8[11272192]{0:T(1024)(128)(4,1)} %bitcast.10), calls=%async_computation.9 | async-start | bytes 8388608
  16.3 9.9 %copy-start.1 = (bf16[3072,512]{1,0:T(8,128)(2,1)S(1)}, bf16[3072,512]{1,0:T(8,128)(2,1)}, u32[]{:S(2)}) copy-start(bf16[3072,512]{1,0:T(8,128)(2,1)} %refs_1_.1) | copy-start | bytes 9437188
  16.3 9.9 %copy-start.5 = (bf16[8,512]{1,0:T(8,128)(2,1)S(1)}, bf16[8,512]{1,0:T(8,128)(2,1)}, u32[]{:S(2)}) copy-start(bf16[8,512]{1,0:T(8,128)(2,1)} %refs_2_.1) | copy-start | bytes 24580
  16.3 18.9 %slice-start.1 = ((s8[11272192]{0:T(1024)(128)(4,1)}), s8[4194304]{0:T(1024)(128)(4,1)S(1)}, s32[]{:S(2)}) async-start(s8[11272192]{0:T(1024)(128)(4,1)} %bitcast.4), calls=%async_computation.4 | async-start | bytes 8388608
  16.3 18.9 %slice-start.2 = ((s8[11272192]{0:T(1024)(128)(4,1)}), s8[2883584]{0:T(1024)(128)(4,1)S(1)}, s32[]{:S(2)}) async-start(s8[11272192]{0:T(1024)(128)(4,1)} %bitcast.4), calls=%async_computation.5 | async-start | bytes 5767168
  16.3 18.9 %slice-start.4 = ((s8[11272192]{0:T(1024)(128)(4,1)}), s8[4194304]{0:T(1024)(128)(4,1)S(1)}, s32[]{:S(2)}) async-start(s8[11272192]{0:T(1024)(128)(4,1)} %bitcast.7), calls=%async_computation.7 | async-start | bytes 8388608
  16.4 18.9 %slice-start.5 = ((s8[11272192]{0:T(1024)(128)(4,1)}), s8[2883584]{0:T(1024)(128)(4,1)S(1)}, s32[]{:S(2)}) async-start(s8[11272192]{0:T(1024)(128)(4,1)} %bitcast.7), calls=%async_computation.8 | async-start | bytes 5767168
  16.4 18.9 %slice-start.7 = ((s8[11272192]{0:T(1024)(128)(4,1)}), s8[4194304]{0:T(1024)(128)(4,1)S(1)}, s32[]{:S(2)}) async-start(s8[11272192]{0:T(1024)(128)(4,1)} %bitcast.10), calls=%async_computation.10 | async-start | bytes 8388608
  16.4 18.9 %slice-start.8 = ((s8[11272192]{0:T(1024)(128)(4,1)}), s8[2883584]{0:T(1024)(128)(4,1)S(1)}, s32[]{:S(2)}) async-start(s8[11272192]{0:T(1024)(128)(4,1)} %bitcast.10), calls=%async_computation.11 | async-start | bytes 5767168
  17.0 18.2 %copy-start.6 = (bf16[4096]{0:T(1024)(128)(2,1)S(1)}, bf16[4096]{0:T(1024)(128)(2,1)}, u32[]{:S(2)}) copy-start(bf16[4096]{0:T(1024)(128)(2,1)} %param.32) | copy-start | bytes 24580

commit v4 on v3

--- a/solution.py
+++ b/solution.py
@@ -223,13 +223,22 @@
     return jnp.where(at == 0, upper, jnp.where(at == 1, lower, 0.0)).astype(BF16)
 
 
-def gather_kernel(lengths_ref, _, state_ref, keys_ref, values_ref, rates_ref, mixed_ref, total_ref):
+def gather_kernel(
+    lengths_ref, _, state_ref, keys_ref, values_ref, rates_ref, gain_ref, mixed_ref, total_ref, own_gain_ref
+):
     seq_dev, heads_dev, key_dim, value_dim = state_ref.shape
     span = keys_ref.shape[2]
     row_at = lax.broadcasted_iota(jnp.int32, (span, span), 0)
     col_at = lax.broadcasted_iota(jnp.int32, (span, span), 1)
     upto = jnp.where(col_at <= row_at, 1.0, 0.0).astype(BF16)
     slot = lax.broadcasted_iota(jnp.int32, (span, 1), 0)
+    gain = spread(gain_ref)
+    columns = own_gain_ref.shape[1]
+    member = lax.axis_index("kv") * lax.axis_size("tp") + lax.axis_index("tp")
+    own_gain = gain[:, :columns]
+    for i in range(1, gain.shape[1] // columns):
+        own_gain = jnp.where(member == i, gain[:, i * columns : (i + 1) * columns], own_gain)
+    own_gain_ref[...] = own_gain
     for s in range(seq_dev):
         live = (slot < lengths_ref[s]).astype(F32)
         for h in range(heads_dev):
@@ -283,7 +292,7 @@
         out_ref[i] = heads
 
 
-def output_kernel(n_tp, recv_ref, weight_ref, own_ref, out_ref, after_ref, rows_ref):
+def output_kernel(n_tp, recv_ref, weight_ref, own_ref, gain_ref, after_ref, scaled_ref, rows_ref):
     seq_dev, wide = recv_ref.shape[1], recv_ref.shape[2]
     for i in range(recv_ref.shape[0]):
         kv_at, tp_at = divmod(i, n_tp)
@@ -293,49 +302,111 @@
     projected = jnp.dot(rows_ref[...].astype(BF16), weight_ref[...], preferred_element_type=F32)
     after = (own_ref[...].astype(F32) + projected).astype(BF16)
     after_ref[...] = after
-    for i in range(out_ref.shape[0]):
-        out_ref[i] = after
-
-
-def feed_kernel(cut, recv_ref, gain_ref, gate_ref, up_ref, down_ref, out_ref, gate_cols, up_cols):
-    members, rows, columns = recv_ref.shape
+    after = after.astype(F32)
+    columns = after.shape[1]
+    scaled_ref[:, :columns] = (after * gain_ref[...]).astype(BF16)
+    squares = jnp.sum(after * after, axis=1, keepdims=True)
+    lane = lax.broadcasted_iota(jnp.int32, (after.shape[0], LANES), 1)
+    upper = squares.astype(BF16).astype(F32)
+    lower = squares - upper
+    scaled_ref[:, columns:] = jnp.where(lane == 0, upper, jnp.where(lane == 1, lower, 0.0)).astype(BF16)
+
+
+def member_columns(step, other, columns):
+    tp = lax.axis_index("tp")
+    tp = 1 - tp if other else tp
+    member = (lax.axis_index("kv") ^ step) * lax.axis_size("tp") + tp
+    return pl.ds(pl.multiple_of(member * columns, columns), columns)
+
+
+def grow(cut, columns, pieces, gate_ref, up_ref, tall_refs, flats, squares, fresh):
     contract = (((1,), (1,)), ((), ()))
-    squares = 0.0
-    gain = spread(gain_ref)
-    sums = [0.0, 0.0]
-    group = 1
-    for k in range(members // group):
-        pieces = []
-        for i in range(k * group, (k + 1) * group):
-            piece = recv_ref[i].astype(F32)
-            squares = squares + jnp.sum(piece * piece, axis=1, keepdims=True)
-            pieces.append((piece * gain[:, i * columns : (i + 1) * columns]).astype(BF16))
-        scaled = jnp.concatenate(pieces, axis=1)
-        at = slice(k * group * columns, (k + 1) * group * columns)
-        for j, (weight, cols) in enumerate(((gate_ref, gate_cols), (up_ref, up_cols))):
-            tall = lax.dot_general(weight[:cut, at], scaled, contract, preferred_element_type=F32)
-            cols[...] = tall if k == 0 else cols[...] + tall
-            sums[j] = sums[j] + lax.dot_general(scaled, weight[cut:, at], contract, preferred_element_type=F32)
-    inv = lax.rsqrt(squares / (members * columns) + EPS)
-    inv_row = jnp.transpose(jnp.broadcast_to(inv, (rows, LANES)))[:1]
-    gate = gate_cols[...] * inv_row
-    tall = (gate / (1.0 + jnp.exp(-gate)) * (up_cols[...] * inv_row)).astype(BF16)
-    gate = sums[0] * inv
-    flat = (gate / (1.0 + jnp.exp(-gate)) * (sums[1] * inv)).astype(BF16)
-    for i in range(members):
-        at = slice(i * columns, (i + 1) * columns)
+    for piece, step, other in pieces:
+        at = member_columns(step, other, columns)
+        rows = piece[:, :columns]
+        squares = squares + jnp.sum(piece[:, columns:].astype(F32), axis=1, keepdims=True)
+        for j, weight in enumerate((gate_ref, up_ref)):
+            tall = lax.dot_general(weight[:cut, at], rows, contract, preferred_element_type=F32)
+            tall_refs[j][...] = tall if fresh else tall_refs[j][...] + tall
+            flats[j] = flats[j] + lax.dot_general(rows, weight[cut:, at], contract, preferred_element_type=F32)
+        fresh = False
+    return squares
+
+
+def first_kernel(cut, columns, own_ref, other_ref, gate_ref, up_ref, _, *sums):
+    talls, flat_refs, squares_ref = sums[:2], sums[2:4], sums[4]
+    flats = [0.0, 0.0]
+    pieces = ((own_ref, 0, False), (other_ref, 0, True))
+    squares = grow(cut, columns, pieces, gate_ref, up_ref, talls, flats, 0.0, True)
+    for ref, flat in zip(flat_refs, flats):
+        ref[...] = flat
+    squares_ref[...] = jnp.broadcast_to(squares, squares_ref.shape)
+
+
+def next_sums(cut, columns, count, other, refs, talls):
+    pieces = [(refs[i], i + 1, other) for i in range(count)]
+    gate_ref, up_ref = refs[count : count + 2]
+    old_talls, flat_refs, squares_ref = refs[count + 2 : count + 4], refs[count + 4 : count + 6], refs[count + 6]
+    for new, old in zip(talls, old_talls):
+        new[...] = old[...]
+    flats = [ref[...] for ref in flat_refs]
+    squares = grow(cut, columns, pieces, gate_ref, up_ref, talls, flats, squares_ref[:, :1], False)
+    return flats, squares
+
+
+def second_kernel(cut, columns, count, *refs):
+    sums = refs[count + 8 :]
+    flats, squares = next_sums(cut, columns, count, False, refs, sums[:2])
+    for ref, flat in zip(sums[2:4], flats):
+        ref[...] = flat
+    sums[4][...] = jnp.broadcast_to(squares, sums[4].shape)
+
+
+def shares(cut, columns, other, tall, flat, down_ref, out_refs):
+    for step, out_ref in enumerate(out_refs):
+        at = member_columns(step, other, columns)
         share = lax.dot_general(
             tall, down_ref[:cut, at], (((0,), (0,)), ((), ())), preferred_element_type=F32
         )
         share = share + jnp.dot(flat, down_ref[cut:, at], preferred_element_type=F32)
-        out_ref[i] = share.astype(BF16)
-
-
-def finish_kernel(recv_ref, after_ref, out_ref):
-    total = after_ref[...].astype(F32)
-    for i in range(recv_ref.shape[0]):
-        total = total + recv_ref[i].astype(F32)
-    out_ref[...] = total.astype(BF16)
+        out_ref[...] = share.astype(out_ref.dtype)
+
+
+def third_kernel(cut, columns, count, width, *refs):
+    down_ref, (send_ref, tall_ref, flat_ref), talls = refs[count + 7], refs[count + 8 : -2], refs[-2:]
+    flats, squares = next_sums(cut, columns, count, True, refs, talls)
+    inv = lax.rsqrt(squares / width + EPS)
+    rows = inv.shape[0]
+    inv_row = jnp.transpose(jnp.broadcast_to(inv, (rows, LANES)))[:1]
+    gate = talls[0][...] * inv_row
+    tall = (gate / (1.0 + jnp.exp(-gate)) * (talls[1][...] * inv_row)).astype(BF16)
+    gate = flats[0] * inv
+    flat = (gate / (1.0 + jnp.exp(-gate)) * (flats[1] * inv)).astype(BF16)
+    tall_ref[...] = tall
+    flat_ref[...] = flat
+    outs = [send_ref.at[:, i * columns : (i + 1) * columns] for i in range(count + 1)]
+    shares(cut, columns, True, tall, flat, down_ref, outs)
+
+
+def fourth_kernel(cut, columns, tall_ref, flat_ref, down_ref, out_ref):
+    outs = [out_ref.at[:, i * columns : (i + 1) * columns] for i in range(out_ref.shape[1] // columns)]
+    shares(cut, columns, False, tall_ref[...], flat_ref[...], down_ref, outs)
+
+
+def merge_kernel(columns, own_ref, recv_ref, after_ref, *out_refs):
+    for step, out_ref in enumerate(out_refs):
+        at = slice(step * columns, (step + 1) * columns)
+        total = own_ref[:, at] + recv_ref[:, at].astype(F32)
+        if step == 0:
+            total = total + after_ref[...].astype(F32)
+        out_ref[...] = total.astype(out_ref.dtype)
+
+
+def finish_kernel(*refs):
+    total = refs[0][...]
+    for part in refs[1:-1]:
+        total = total + part[...].astype(F32)
+    refs[-1][...] = total.astype(BF16)
 
 
 MIB = 1 << 20
@@ -388,64 +459,125 @@
     for step in range(1, n_kv):
         parts[step] = lax.ppermute(parts[step], "kv", [(i, i ^ step) for i in range(n_kv)])
     moved = state.size * 6 + cache_rates.size * 8
-    mixed, total = call(
+    mixed, total, own_gain = call(
         gather_kernel,
         [
             jax.ShapeDtypeStruct(state.shape, BF16),
             jax.ShapeDtypeStruct((seq_dev, heads_dev * key_dim), F32),
+            jax.ShapeDtypeStruct((1, columns), F32),
         ],
-        [pl.BlockSpec(memory_space=pltpu.SMEM), anywhere] + [vmem_spec()] * 4,
+        [pl.BlockSpec(memory_space=pltpu.SMEM), anywhere] + [vmem_spec()] * 5,
         [],
         4 * MIB,
-        10**9,
+        4 * 10**10,
         moved,
         "gather",
-    )(lengths, own, in_vmem(state), in_vmem(cache_keys), in_vmem(cache_values), in_vmem(cache_rates))
+    )(lengths, own, in_vmem(state), in_vmem(cache_keys), in_vmem(cache_values), in_vmem(cache_rates), in_vmem(mlp_gain.reshape(-1, LANES)))
     send = call(
         lambda *refs: attend_kernel(width, refs[:n_kv], *refs[n_kv:]),
         jax.ShapeDtypeStruct((members, seq_dev, heads_dev * value_dim), BF16),
         [vmem_spec()] * (n_kv + 3),
         [pltpu.VMEM((seq_dev, heads_dev * value_dim), F32)],
         4 * MIB,
-        4 * 10**10,
+        10**6,
         state.size * 2,
         "attend",
     )(own, *parts[:0:-1], mixed, total, in_vmem(head_gain))
     recv = lax.all_to_all(send, ("kv", "tp"), 0, 0, tiled=True)
-    send, after = call(
+    narrow = jax.ShapeDtypeStruct((rows, columns + LANES), BF16)
+    after, scaled = call(
         lambda *refs: output_kernel(n_tp, *refs),
-        (jax.ShapeDtypeStruct((members, rows, columns), BF16), jax.ShapeDtypeStruct((rows, columns), BF16)),
-        [vmem_spec()] * 3,
+        (jax.ShapeDtypeStruct((rows, columns), BF16), narrow),
+        [vmem_spec()] * 4,
         [pltpu.VMEM((rows, w_out.shape[0]), F32)],
         2 * MIB,
         10**6,
         w_out.size * 2,
         "output",
-    )(recv, in_vmem(w_out), in_vmem(tokens))
-    recv = lax.all_to_all(send, ("kv", "tp"), 0, 0, tiled=True)
-    moved = (w_mlp_gate.size + w_mlp_up.size + w_mlp_down.size) * 2
+    )(recv, in_vmem(w_out), in_vmem(tokens), own_gain)
+    swap = [(i, n_tp - 1 - i) for i in range(n_tp)]
+    far = n_kv - 1
+    got = [lax.ppermute(scaled, "kv", [(i, i ^ step) for i in range(n_kv)]) for step in range(1, n_kv)]
+    beside = lax.ppermute(scaled, "tp", swap)
+    hidden = w_mlp_down.shape[0]
     cut = w_mlp_down.shape[0] // 64 * 16
-    send = call(
-        lambda *refs: feed_kernel(cut, *refs),
-        jax.ShapeDtypeStruct((members, rows, columns), BF16),
+    sums = (
+        [jax.ShapeDtypeStruct((cut, rows), F32)] * 2
+        + [jax.ShapeDtypeStruct((rows, hidden - cut), F32)] * 2
+        + [jax.ShapeDtypeStruct((rows, LANES), F32)]
+    )
+    down = in_vmem(w_mlp_down)
+    gate_up = (in_vmem(w_mlp_gate.T), in_vmem(w_mlp_up.T))
+    running = call(
+        lambda *refs: first_kernel(cut, columns, *refs),
+        sums,
         [vmem_spec()] * 5,
+        [],
+        4 * MIB,
+        MIB,
+        MIB,
+        "feed_first",
+    )(scaled, beside, *gate_up, down)
+    got, running = lax.optimization_barrier((got, running))
+    beside = [lax.ppermute(piece, "tp", swap) for piece in got]
+    running = call(
+        lambda *refs: second_kernel(cut, columns, far, *refs),
+        sums,
+        [vmem_spec()] * (far + 8),
+        [],
+        4 * MIB,
+        MIB,
+        MIB,
+        "feed_second",
+    )(*got, *gate_up, *running, down)
+    send, tall, flat = call(
+        lambda *refs: third_kernel(cut, columns, far, width, *refs),
+        [
+            jax.ShapeDtypeStruct((rows, n_kv * columns), BF16),
+            jax.ShapeDtypeStruct((cut, rows), BF16),
+            jax.ShapeDtypeStruct((rows, hidden - cut), BF16),
+        ],
+        [vmem_spec()] * (far + 8),
         [pltpu.VMEM((cut, rows), F32)] * 2,
         4 * MIB,
-        rows * moved,
-        moved,
-        "feed",
-    )(recv, in_vmem(mlp_gain.reshape(-1, LANES)), in_vmem(w_mlp_gate.T), in_vmem(w_mlp_up.T), in_vmem(w_mlp_down))
-    recv = lax.all_to_all(send, ("kv", "tp"), 0, 0, tiled=True)
+        MIB,
+        MIB,
+        "feed_third",
+    )(*beside, *gate_up, *running, down)
+    recv = lax.ppermute(send, "tp", swap)
+    own = call(
+        lambda *refs: fourth_kernel(cut, columns, *refs),
+        jax.ShapeDtypeStruct((rows, n_kv * columns), F32),
+        [vmem_spec()] * 3,
+        [],
+        4 * MIB,
+        MIB,
+        MIB,
+        "feed_fourth",
+    )(tall, flat, down)
+    merged = call(
+        lambda *refs: merge_kernel(columns, *refs),
+        [jax.ShapeDtypeStruct((rows, columns), F32 if step == 0 else BF16) for step in range(n_kv)],
+        [vmem_spec()] * 3,
+        [],
+        2 * MIB,
+        rows * columns * n_kv,
+        rows * columns * n_kv * 6,
+        "merge",
+    )(own, recv, after)
+    parts = [
+        lax.ppermute(merged[step], "kv", [(i, i ^ step) for i in range(n_kv)]) for step in range(1, n_kv)
+    ]
     return call(
         finish_kernel,
         jax.ShapeDtypeStruct((rows, columns), BF16),
-        [vmem_spec()] * 2,
+        [vmem_spec()] * n_kv,
         [],
         2 * MIB,
-        rows * columns * members,
-        rows * columns * members * 2,
+        rows * columns * n_kv,
+        rows * columns * n_kv * 2,
         "finish",
-    )(recv, after)
+    )(merged[0], *parts[::-1])
 
 
 def solution(mesh):

time: 51.5 us -> 47.8 us (0.928)
  blocking collectives: 25.9 us -> 9.19 us
  starting transfers between devices: 6.14 us -> 16.1 us
  waiting for transfers between devices: 2.99 us -> 5.58 us
    all_to_all x3 -> x1, blocking collectives: 25.9 us -> 9.19 us  [shards(): recv = lax.all_to_all(send, ('kv', 'tp'), 0, 0, tiled=True)]
    ppermute x0 -> x11, starting transfers between devices: none -> 9.96 us  [the longest x3 4.45 us: shards(): lax.ppermute(scaled, 'kv', [(i, i ^ step) for i in range(n_kv)])]
    ppermute x0 -> x11, waiting for transfers between devices: none -> 2.74 us  [the longest x3 2.69 us: shards(): lax.ppermute(merged[step], 'kv', [(i, i ^ step) for i in range(n_kv)])]
    pallas_call x2 -> x6, Pallas kernels: 7.55 us -> 8.05 us  [the longest x1 2.93 us: shards(): call(lambda *refs: third_kernel(cut, columns, far, width, *refs), [jax.Sh...]
  transfers between devices with their start and end apart: 4 -> 15, of which waited for: 2 -> 5; matrix products, arithmetic and copies ran while one was open for 0% -> 0% of each run, Pallas kernels for 4% -> 14%
where the time goes in v4:
time: 47.8 us; the launch traced here: 47.6 us
  Pallas kernels  16.4 us (34%)
  starting transfers between devices  16.1 us (34%)
  blocking collectives  9.19 us (19%)
  waiting for transfers between devices  5.58 us (12%)
    all_to_all x1, blocking collectives, shards(): recv = lax.all_to_all(send, ('kv', 'tp'), 0, 0, tiled=True)  9.19 us
    ppermute x3, starting transfers between devices, shards(): lax.ppermute(parts[step], 'kv', [(i, i ^ step) for i in range(n_kv)])  5.64 us
    pallas_call x1, Pallas kernels, shards(): call(lambda *refs: project_kernel(seq_dev, *refs), [jax.ShapeDtypeStruct(...  5 us
    ppermute x3, starting transfers between devices, shards(): lax.ppermute(scaled, 'kv', [(i, i ^ step) for i in range(n_kv)])  4.45 us
    ppermute x3, starting transfers between devices, shards(): lax.ppermute(merged[step], 'kv', [(i, i ^ step) for i in range(n_kv)])  4.45 us
    pallas_call x1, Pallas kernels, shards(): call(lambda *refs: third_kernel(cut, columns, far, width, *refs), [jax.Sh...  2.93 us
    ppermute x3, waiting for transfers between devices, shards(): lax.ppermute(merged[step], 'kv', [(i, i ^ step) for i in range(n_kv)])  2.69 us
    pallas_call x1, Pallas kernels, shards(): call(lambda *refs: second_kernel(cut, columns, far, *refs), sums, [vmem_s...  2.08 us
  transfers between devices with their start and end apart: 15, of which 5 were waited for; matrix products, arithmetic and copies ran while one was open for 0% of the time, Pallas kernels for 14%

profile of v4, /device:TPU:0, one launch (start us, length us, event | category | flops | bytes accessed | tf_op | source)
XLA Modules:
  0.0 47.6 jit_solution(16514898716868153575)
XLA Ops:
  0.0 0.5 %collective-permute-start = (bf16[8,512]{1,0:T(8,128)(2,1)}, bf16[8,512]{1,0:T(8,128)(2,1)S(1)}, u32[]{:S(2)}, u32[]{:S(2)}) collective-permute-start(bf16[8,512]{1,0:T(8,128)(2,1)} %refs_2_.2), channel_id=1, source_target_pairs={{0,1},{1,0},{2,3},{3,2},{4,5},{5,4},{6,7},{7,6},{8,9},{9,8},{10,11... | collective-permute-start | bytes 24584 | tf_op jit(solution)/shard_map/ppermute | solution.py:440
  0.5 1.0 %collective-permute-done.refs_1_ = bf16[8,512]{1,0:T(8,128)(2,1)S(1)} collective-permute-done((bf16[8,512]{1,0:T(8,128)(2,1)}, bf16[8,512]{1,0:T(8,128)(2,1)S(1)}, u32[]{:S(2)}, u32[]{:S(2)}) %collective-permute-start) | collective-permute-done | bytes 8224 | tf_op jit(solution)/shard_map/ppermute | solution.py:440
  1.6 5.0 %project.1 = (f32[2,5504]{1,0:T(2,128)S(1)}, bf16[2,5504]{1,0:T(2,128)(2,1)S(1)}, bf16[2,5504]{1,0:T(2,128)(2,1)S(1)}, bf16[2,5504]{1,0:T(2,128)(2,1)S(1)}) custom-call(bf16[8,512]{1,0:T(8,128)(2,1)} %refs_2_.2, bf16[8,512]{1,0:T(8,128)(2,1)S(1)} %collective-permute-done.refs_1_, bf16[8,128]{1,0:T(8,128)(2,1)} %bitcast.17, bf16[1024,768]{1,0:T(8,128)(2,1)} %refs_3_.1, ...), custom_call_target="tpu_custom_call" | custom-call | flops 10000000000 | bytes 11010048 | tf_op jit(solution)/shard_map/project/pallas_call | solution.py:445
  6.6 5.0 %collective-permute-start.1 = (bf16[2,5504]{1,0:T(2,128)(2,1)S(1)}, bf16[2,5504]{1,0:T(2,128)(2,1)S(1)}, u32[]{:S(2)}, u32[]{:S(2)}) collective-permute-start(bf16[2,5504]{1,0:T(2,128)(2,1)S(1)} %get-tuple-element.40), channel_id=1, source_target_pairs={{0,6},{2,4},{4,2},{6,0},{1,7},{3,5},{5,3},{7,1},{8,14},{10,12},{12... | collective-permute-start | bytes 66056 | tf_op jit(solution)/shard_map/ppermute | solution.py:460
  11.6 0.6 %collective-permute-start.3 = (bf16[2,5504]{1,0:T(2,128)(2,1)S(1)}, bf16[2,5504]{1,0:T(2,128)(2,1)S(1)}, u32[]{:S(2)}, u32[]{:S(2)}) collective-permute-start(bf16[2,5504]{1,0:T(2,128)(2,1)S(1)} %get-tuple-element.42), channel_id=1, source_target_pairs={{0,2},{2,0},{4,6},{6,4},{1,3},{3,1},{5,7},{7,5},{8,10},{10,8},{12,... | collective-permute-start | bytes 66056 | tf_op jit(solution)/shard_map/ppermute | solution.py:460
  12.4 2.1 %gather.1 = (bf16[2,2,384,768]{3,2,1,0:T(8,128)(2,1)S(1)}, f32[2,768]{1,0:T(2,128)S(1)}, f32[1,512]{1,0:T(1,128)S(1)}) custom-call(s32[2]{0:T(128)S(1)} %copy-done.8, f32[2,5504]{1,0:T(2,128)S(1)} %get-tuple-element.39._.refs_0_, f32[2,2,384,768]{3,2,1,0:T(8,128)S(1)} %copy-done.3, bf16[2,2,64,384]{3,2,1,0:T(8,128)(2,1)S(1)} %copy-done.6, ...), custom_call_target="tpu_custom_call" | custom-call | flops 40000000000 | bytes 7864320 | tf_op jit(solution)/shard_map/gather/pallas_call | solution.py:462
  14.5 1.8 %collective-permute-done.2.refs_2_ = bf16[2,5504]{1,0:T(2,128)(2,1)S(1)} collective-permute-done((bf16[2,5504]{1,0:T(2,128)(2,1)S(1)}, bf16[2,5504]{1,0:T(2,128)(2,1)S(1)}, u32[]{:S(2)}, u32[]{:S(2)}) %collective-permute-start.2) | collective-permute-done | bytes 22048 | tf_op jit(solution)/shard_map/ppermute | solution.py:460
  16.3 0.6 %attend.1 = bf16[8,2,1536]{2,1,0:T(2,128)(2,1)S(1)} custom-call(f32[2,5504]{1,0:T(2,128)S(1)} %get-tuple-element.39._.refs_0_, bf16[2,5504]{1,0:T(2,128)(2,1)S(1)} %collective-permute-done.1.refs_1_, bf16[2,5504]{1,0:T(2,128)(2,1)S(1)} %collective-permute-done.2.refs_2_, bf16[2,5504]{1,0:T(2,128)(2,1)S(1)} %collective-permute-done.3.refs_3_, ...), custom_call_target="tpu_custom_call" | custom-call | flops 1000000 | bytes 2359296 | tf_op jit(solution)/shard_map/attend/pallas_call | solution.py:476
  16.9 9.2 %all_to_all.5.refs_0_ = bf16[8,2,1536]{2,1,0:T(2,128)(2,1)S(1)} all-to-all(bf16[8,2,1536]{2,1,0:T(2,128)(2,1)S(1)} %attend.1), channel_id=1, replica_groups=mesh['dp'=4,'kv'=4,'tp'=2] {'kv','tp'}, dimensions={0} | all-to-all | bytes 98304 | tf_op jit(solution)/shard_map/all_to_all | solution.py:486
  26.1 0.6 %output.1 = (bf16[8,512]{1,0:T(8,128)(2,1)S(1)}, bf16[8,640]{1,0:T(8,128)(2,1)S(1)}) custom-call(bf16[8,2,1536]{2,1,0:T(2,128)(2,1)S(1)} %all_to_all.5.refs_0_, bf16[3072,512]{1,0:T(8,128)(2,1)S(1)} %copy-done, bf16[8,512]{1,0:T(8,128)(2,1)S(1)} %copy-done.1, f32[1,512]{1,0:T(1,128)S(1)} %get-tuple-element.45.refs_3_), custom_call_target="tpu_custom_call" | custom-call | flops 1000000 | bytes 3145728 | tf_op jit(solution)/shard_map/output/pallas_call | solution.py:488
  26.7 0.0 collective-permute-start.7
  26.7 0.7 %collective-permute-start.6 = (bf16[8,640]{1,0:T(8,128)(2,1)S(1)}, bf16[8,640]{1,0:T(8,128)(2,1)S(1)}, u32[]{:S(2)}, u32[]{:S(2)}) collective-permute-start(bf16[8,640]{1,0:T(8,128)(2,1)S(1)} %get-tuple-element.46.refs_0_), channel_id=1, source_target_pairs={{0,6},{2,4},{4,2},{6,0},{1,7},{3,5},{5,3},{7,1},{8,14},{10,12},{12... | collective-permute-start | bytes 30728 | tf_op jit(solution)/shard_map/ppermute | solution.py:500
  27.5 1.5 %collective-permute-start.5 = (bf16[8,640]{1,0:T(8,128)(2,1)S(1)}, bf16[8,640]{1,0:T(8,128)(2,1)S(1)}, u32[]{:S(2)}, u32[]{:S(2)}) collective-permute-start(bf16[8,640]{1,0:T(8,128)(2,1)S(1)} %get-tuple-element.46.refs_0_), channel_id=1, source_target_pairs={{0,4},{2,6},{4,0},{6,2},{1,5},{3,7},{5,1},{7,3},{8,12},{10,14},{12... | collective-permute-start | bytes 30728 | tf_op jit(solution)/shard_map/ppermute | solution.py:500
  29.0 2.2 %collective-permute-start.4 = (bf16[8,640]{1,0:T(8,128)(2,1)S(1)}, bf16[8,640]{1,0:T(8,128)(2,1)S(1)}, u32[]{:S(2)}, u32[]{:S(2)}) collective-permute-start(bf16[8,640]{1,0:T(8,128)(2,1)S(1)} %get-tuple-element.46.refs_0_), channel_id=1, source_target_pairs={{0,2},{2,0},{4,6},{6,4},{1,3},{3,1},{5,7},{7,5},{8,10},{10,8},{12,... | collective-permute-start | bytes 30728 | tf_op jit(solution)/shard_map/ppermute | solution.py:500
  31.3 1.5 %feed_first.1 = (f32[336,8]{1,0:T(8,128)S(1)}, f32[336,8]{1,0:T(8,128)S(1)}, f32[8,1040]{1,0:T(8,128)S(1)}, f32[8,1040]{1,0:T(8,128)S(1)}, f32[8,128]{1,0:T(8,128)S(1)}) custom-call(bf16[8,640]{1,0:T(8,128)(2,1)S(1)} %get-tuple-element.46.refs_0_, bf16[8,640]{1,0:T(8,128)(2,1)S(1)} %collective-permute-done.7.refs_1_, bf16[1376,4096]{1,0:T(8,128)(2,1)S(1)} %bitcast.8, ...), custom_call_target="tpu_custom_call" | custom-call | flops 1048576 | bytes 1048576 | tf_op jit(solution)/shard_map/feed_first/pallas_call | solution.py:511
  32.8 0.0 collective-permute-done.5.refs_1_
  32.8 0.0 collective-permute-done.4.refs_0_
  32.8 0.1 collective-permute-start.8
  32.9 0.5 %collective-permute-start.9 = (bf16[8,640]{1,0:T(8,128)(2,1)S(1)}, bf16[8,640]{1,0:T(8,128)(2,1)S(1)}, u32[]{:S(2)}, u32[]{:S(2)}) collective-permute-start(bf16[8,640]{1,0:T(8,128)(2,1)S(1)} %collective-permute-done.5.refs_1_), channel_id=1, source_target_pairs={{0,1},{1,0},{2,3},{3,2},{4,5},{5,4},{6,7},{7,6},{8,9},{9,8},{10,11... | collective-permute-start | bytes 30728 | tf_op jit(solution)/shard_map/ppermute | solution.py:522
  33.4 0.1 collective-permute-start.10
  33.5 2.1 %feed_second.1 = (f32[336,8]{1,0:T(8,128)S(1)}, f32[336,8]{1,0:T(8,128)S(1)}, f32[8,1040]{1,0:T(8,128)S(1)}, f32[8,1040]{1,0:T(8,128)S(1)}, f32[8,128]{1,0:T(8,128)S(1)}) custom-call(bf16[8,640]{1,0:T(8,128)(2,1)S(1)} %collective-permute-done.4.refs_0_, bf16[8,640]{1,0:T(8,128)(2,1)S(1)} %collective-permute-done.5.refs_1_, ...), custom_call_target="tpu_custom_call" | custom-call | flops 1048576 | bytes 1048576 | tf_op jit(solution)/shard_map/feed_second/pallas_call | solution.py:523
  35.6 0.0 collective-permute-done.9.refs_1_
  35.6 2.9 %feed_third.1 = (bf16[8,2048]{1,0:T(8,128)(2,1)S(1)}, bf16[336,8]{1,0:T(8,128)(2,1)S(1)}, bf16[8,1040]{1,0:T(8,128)(2,1)S(1)}) custom-call(bf16[8,640]{1,0:T(8,128)(2,1)S(1)} %collective-permute-done.8.refs_0_, bf16[8,640]{1,0:T(8,128)(2,1)S(1)} %collective-permute-done.9.refs_1_, bf16[8,640]{1,0:T(8,128)(2,1)S(1)} %collective-permute-done.10.refs_2_, ...), custom_call_target="tpu_custom_call" | custom-call | flops 1048576 | bytes 1048576 | tf_op jit(solution)/shard_map/feed_third/pallas_call | solution.py:533
  38.5 0.4 collective-permute-start.11
  38.9 0.9 %feed_fourth.1.refs_0_ = f32[8,2048]{1,0:T(8,128)S(1)} custom-call(bf16[336,8]{1,0:T(8,128)(2,1)S(1)} %get-tuple-element.65.refs_0_, bf16[8,1040]{1,0:T(8,128)(2,1)S(1)} %get-tuple-element.66.refs_1_, bf16[1376,4096]{1,0:T(8,128)(2,1)S(1)} %bitcast.5), custom_call_target="tpu_custom_call" | custom-call | flops 1048576 | bytes 1048576 | tf_op jit(solution)/shard_map/feed_fourth/pallas_call | solution.py:548
  39.9 2.4 %collective-permute-start.12 = (bf16[8,512]{1,0:T(8,128)(2,1)S(1)}, bf16[8,512]{1,0:T(8,128)(2,1)S(1)}, u32[]{:S(2)}, u32[]{:S(2)}) collective-permute-start(bf16[8,512]{1,0:T(8,128)(2,1)S(1)} %get-tuple-element.70), channel_id=1, source_target_pairs={{0,6},{2,4},{4,2},{6,0},{1,7},{3,5},{5,3},{7,1},{8,14},{10,12},{12... | collective-permute-start | bytes 24584 | tf_op jit(solution)/shard_map/ppermute | solution.py:569
  42.3 1.1 %collective-permute-start.13 = (bf16[8,512]{1,0:T(8,128)(2,1)S(1)}, bf16[8,512]{1,0:T(8,128)(2,1)S(1)}, u32[]{:S(2)}, u32[]{:S(2)}) collective-permute-start(bf16[8,512]{1,0:T(8,128)(2,1)S(1)} %get-tuple-element.71), channel_id=1, source_target_pairs={{0,4},{2,6},{4,0},{6,2},{1,5},{3,7},{5,1},{7,3},{8,12},{10,14},{12... | collective-permute-start | bytes 24584 | tf_op jit(solution)/shard_map/ppermute | solution.py:569
  43.4 1.0 %collective-permute-start.14 = (bf16[8,512]{1,0:T(8,128)(2,1)S(1)}, bf16[8,512]{1,0:T(8,128)(2,1)S(1)}, u32[]{:S(2)}, u32[]{:S(2)}) collective-permute-start(bf16[8,512]{1,0:T(8,128)(2,1)S(1)} %get-tuple-element.72), channel_id=1, source_target_pairs={{0,2},{2,0},{4,6},{6,4},{1,3},{3,1},{5,7},{7,5},{8,10},{10,8},{12,... | collective-permute-start | bytes 24584 | tf_op jit(solution)/shard_map/ppermute | solution.py:569
  44.3 1.1 %collective-permute-done.12.refs_1_ = bf16[8,512]{1,0:T(8,128)(2,1)S(1)} collective-permute-done((bf16[8,512]{1,0:T(8,128)(2,1)S(1)}, bf16[8,512]{1,0:T(8,128)(2,1)S(1)}, u32[]{:S(2)}, u32[]{:S(2)}) %collective-permute-start.12) | collective-permute-done | bytes 8224 | tf_op jit(solution)/shard_map/ppermute | solution.py:569
  45.4 1.4 %collective-permute-done.13.refs_2_ = bf16[8,512]{1,0:T(8,128)(2,1)S(1)} collective-permute-done((bf16[8,512]{1,0:T(8,128)(2,1)S(1)}, bf16[8,512]{1,0:T(8,128)(2,1)S(1)}, u32[]{:S(2)}, u32[]{:S(2)}) %collective-permute-start.13) | collective-permute-done | bytes 8224 | tf_op jit(solution)/shard_map/ppermute | solution.py:569
  46.8 0.2 collective-permute-done.14.refs_3_
  47.0 0.6 %finish.1 = bf16[8,512]{1,0:T(8,128)(2,1)} custom-call(f32[8,512]{1,0:T(8,128)S(1)} %get-tuple-element.69.refs_0_, bf16[8,512]{1,0:T(8,128)(2,1)S(1)} %collective-permute-done.12.refs_1_, bf16[8,512]{1,0:T(8,128)(2,1)S(1)} %collective-permute-done.13.refs_2_, bf16[8,512]{1,0:T(8,128)(2,1)S(1)} %collective-permute-done.14.refs_3_), custom_call_target="tpu_custom_call" | custom-call | flops 16384 | bytes 32768 | tf_op jit(solution)/shard_map/finish/pallas_call | solution.py:571
  (48 shorter events, 0.1 us)
Async XLA Ops:
  0.0 1.5 %collective-permute-start = (bf16[8,512]{1,0:T(8,128)(2,1)}, bf16[8,512]{1,0:T(8,128)(2,1)S(1)}, u32[]{:S(2)}, u32[]{:S(2)}) collective-permute-start(bf16[8,512]{1,0:T(8,128)(2,1)} %refs_2_.2), channel_id=1, source_target_pairs={{0,1},{1,0},{2,3},{3,2},{4,5},{5,4},{6,7},{7,6},{8,9},{9,8},{10,11... | collective-permute-start | bytes 24584 | tf_op jit(solution)/shard_map/ppermute | solution.py:440
  1.5 10.7 %copy-start.3 = (f32[2,2,384,768]{3,2,1,0:T(8,128)S(1)}, f32[2,2,384,768]{3,2,1,0:T(8,128)}, u32[]{:S(2)}) copy-start(f32[2,2,384,768]{3,2,1,0:T(8,128)} %state_ref.1) | copy-start | bytes 14155780
  1.5 10.7 %copy-start.4 = (bf16[2,2,64,768]{3,2,1,0:T(8,128)(2,1)S(1)}, bf16[2,2,64,768]{3,2,1,0:T(8,128)(2,1)}, u32[]{:S(2)}) copy-start(bf16[2,2,64,768]{3,2,1,0:T(8,128)(2,1)} %values_ref.1) | copy-start | bytes 1179652
  1.5 10.7 %copy-start.5 = (f32[2,2,64,384]{3,2,1,0:T(8,128)S(1)}, f32[2,2,64,384]{3,2,1,0:T(8,128)}, u32[]{:S(2)}) copy-start(f32[2,2,64,384]{3,2,1,0:T(8,128)} %rates_ref.1) | copy-start | bytes 1179652
  1.5 10.7 %copy-start.6 = (bf16[2,2,64,384]{3,2,1,0:T(8,128)(2,1)S(1)}, bf16[2,2,64,384]{3,2,1,0:T(8,128)(2,1)}, u32[]{:S(2)}) copy-start(bf16[2,2,64,384]{3,2,1,0:T(8,128)(2,1)} %keys_ref.1) | copy-start | bytes 589828
  1.5 10.7 %copy-start.7 = (bf16[4096]{0:T(1024)(128)(2,1)S(1)}, bf16[4096]{0:T(1024)(128)(2,1)}, u32[]{:S(2)}) copy-start(bf16[4096]{0:T(1024)(128)(2,1)} %param.32) | copy-start | bytes 24580
  1.5 10.7 %copy-start.8 = (s32[2]{0:T(128)S(1)}, s32[2]{0:T(128)}, u32[]{:S(2)}) copy-start(s32[2]{0:T(128)} %lengths_ref.1) | copy-start | bytes 28
  6.6 7.9 %collective-permute-start.1 = (bf16[2,5504]{1,0:T(2,128)(2,1)S(1)}, bf16[2,5504]{1,0:T(2,128)(2,1)S(1)}, u32[]{:S(2)}, u32[]{:S(2)}) collective-permute-start(bf16[2,5504]{1,0:T(2,128)(2,1)S(1)} %get-tuple-element.40), channel_id=1, source_target_pairs={{0,6},{2,4},{4,2},{6,0},{1,7},{3,5},{5,3},{7,1},{8,14},{10,12},{12... | collective-permute-start | bytes 66056 | tf_op jit(solution)/shard_map/ppermute | solution.py:460
  11.6 4.7 %collective-permute-start.2 = (bf16[2,5504]{1,0:T(2,128)(2,1)S(1)}, bf16[2,5504]{1,0:T(2,128)(2,1)S(1)}, u32[]{:S(2)}, u32[]{:S(2)}) collective-permute-start(bf16[2,5504]{1,0:T(2,128)(2,1)S(1)} %get-tuple-element.41), channel_id=1, source_target_pairs={{0,4},{2,6},{4,0},{6,2},{1,5},{3,7},{5,1},{7,3},{8,12},{10,14},{12... | collective-permute-start | bytes 66056 | tf_op jit(solution)/shard_map/ppermute | solution.py:460
  11.6 4.7 %collective-permute-start.3 = (bf16[2,5504]{1,0:T(2,128)(2,1)S(1)}, bf16[2,5504]{1,0:T(2,128)(2,1)S(1)}, u32[]{:S(2)}, u32[]{:S(2)}) collective-permute-start(bf16[2,5504]{1,0:T(2,128)(2,1)S(1)} %get-tuple-element.42), channel_id=1, source_target_pairs={{0,2},{2,0},{4,6},{6,4},{1,3},{3,1},{5,7},{7,5},{8,10},{10,8},{12,... | collective-permute-start | bytes 66056 | tf_op jit(solution)/shard_map/ppermute | solution.py:460
  12.2 19.0 %slice-start = ((s8[11272192]{0:T(1024)(128)(4,1)}), s8[4194304]{0:T(1024)(128)(4,1)S(1)}, s32[]{:S(2)}) async-start(s8[11272192]{0:T(1024)(128)(4,1)} %bitcast.4), calls=%async_computation.1 | async-start | bytes 8388608
  12.2 19.0 %slice-start.3 = ((s8[11272192]{0:T(1024)(128)(4,1)}), s8[4194304]{0:T(1024)(128)(4,1)S(1)}, s32[]{:S(2)}) async-start(s8[11272192]{0:T(1024)(128)(4,1)} %bitcast.6), calls=%async_computation.4 | async-start | bytes 8388608
  12.2 19.0 %slice-start.6 = ((s8[11272192]{0:T(1024)(128)(4,1)}), s8[4194304]{0:T(1024)(128)(4,1)S(1)}, s32[]{:S(2)}) async-start(s8[11272192]{0:T(1024)(128)(4,1)} %bitcast.11), calls=%async_computation.7 | async-start | bytes 8388608
  12.3 13.8 %copy-start = (bf16[3072,512]{1,0:T(8,128)(2,1)S(1)}, bf16[3072,512]{1,0:T(8,128)(2,1)}, u32[]{:S(2)}) copy-start(bf16[3072,512]{1,0:T(8,128)(2,1)} %refs_1_.1) | copy-start | bytes 9437188
  12.3 13.8 %copy-start.1 = (bf16[8,512]{1,0:T(8,128)(2,1)S(1)}, bf16[8,512]{1,0:T(8,128)(2,1)}, u32[]{:S(2)}) copy-start(bf16[8,512]{1,0:T(8,128)(2,1)} %refs_2_.2) | copy-start | bytes 24580
  12.3 18.9 %slice-start.1 = ((s8[11272192]{0:T(1024)(128)(4,1)}), s8[4194304]{0:T(1024)(128)(4,1)S(1)}, s32[]{:S(2)}) async-start(s8[11272192]{0:T(1024)(128)(4,1)} %bitcast.4), calls=%async_computation.2 | async-start | bytes 8388608
  12.3 18.9 %slice-start.2 = ((s8[11272192]{0:T(1024)(128)(4,1)}), s8[2883584]{0:T(1024)(128)(4,1)S(1)}, s32[]{:S(2)}) async-start(s8[11272192]{0:T(1024)(128)(4,1)} %bitcast.4), calls=%async_computation.3 | async-start | bytes 5767168
  12.3 18.9 %slice-start.4 = ((s8[11272192]{0:T(1024)(128)(4,1)}), s8[4194304]{0:T(1024)(128)(4,1)S(1)}, s32[]{:S(2)}) async-start(s8[11272192]{0:T(1024)(128)(4,1)} %bitcast.6), calls=%async_computation.5 | async-start | bytes 8388608
  12.3 18.9 %slice-start.5 = ((s8[11272192]{0:T(1024)(128)(4,1)}), s8[2883584]{0:T(1024)(128)(4,1)S(1)}, s32[]{:S(2)}) async-start(s8[11272192]{0:T(1024)(128)(4,1)} %bitcast.6), calls=%async_computation.6 | async-start | bytes 5767168
  12.4 18.9 %slice-start.7 = ((s8[11272192]{0:T(1024)(128)(4,1)}), s8[4194304]{0:T(1024)(128)(4,1)S(1)}, s32[]{:S(2)}) async-start(s8[11272192]{0:T(1024)(128)(4,1)} %bitcast.11), calls=%async_computation.8 | async-start | bytes 8388608
  12.4 18.9 %slice-start.8 = ((s8[11272192]{0:T(1024)(128)(4,1)}), s8[2883584]{0:T(1024)(128)(4,1)S(1)}, s32[]{:S(2)}) async-start(s8[11272192]{0:T(1024)(128)(4,1)} %bitcast.11), calls=%async_computation.9 | async-start | bytes 5767168
  26.7 4.5 %collective-permute-start.7 = (bf16[8,640]{1,0:T(8,128)(2,1)S(1)}, bf16[8,640]{1,0:T(8,128)(2,1)S(1)}, u32[]{:S(2)}, u32[]{:S(2)}) collective-permute-start(bf16[8,640]{1,0:T(8,128)(2,1)S(1)} %get-tuple-element.46.refs_0_), channel_id=1, source_target_pairs={{0,1},{1,0},{2,3},{3,2},{4,5},{5,4},{6,7},{7,6},{8,9},{9,8},{10,11... | collective-permute-start | bytes 30728 | tf_op jit(solution)/shard_map/ppermute | solution.py:501
  26.7 6.1 %collective-permute-start.6 = (bf16[8,640]{1,0:T(8,128)(2,1)S(1)}, bf16[8,640]{1,0:T(8,128)(2,1)S(1)}, u32[]{:S(2)}, u32[]{:S(2)}) collective-permute-start(bf16[8,640]{1,0:T(8,128)(2,1)S(1)} %get-tuple-element.46.refs_0_), channel_id=1, source_target_pairs={{0,6},{2,4},{4,2},{6,0},{1,7},{3,5},{5,3},{7,1},{8,14},{10,12},{12... | collective-permute-start | bytes 30728 | tf_op jit(solution)/shard_map/ppermute | solution.py:500
  27.5 5.4 %collective-permute-start.5 = (bf16[8,640]{1,0:T(8,128)(2,1)S(1)}, bf16[8,640]{1,0:T(8,128)(2,1)S(1)}, u32[]{:S(2)}, u32[]{:S(2)}) collective-permute-start(bf16[8,640]{1,0:T(8,128)(2,1)S(1)} %get-tuple-element.46.refs_0_), channel_id=1, source_target_pairs={{0,4},{2,6},{4,0},{6,2},{1,5},{3,7},{5,1},{7,3},{8,12},{10,14},{12... | collective-permute-start | bytes 30728 | tf_op jit(solution)/shard_map/ppermute | solution.py:500
  29.0 3.9 %collective-permute-start.4 = (bf16[8,640]{1,0:T(8,128)(2,1)S(1)}, bf16[8,640]{1,0:T(8,128)(2,1)S(1)}, u32[]{:S(2)}, u32[]{:S(2)}) collective-permute-start(bf16[8,640]{1,0:T(8,128)(2,1)S(1)} %get-tuple-element.46.refs_0_), channel_id=1, source_target_pairs={{0,2},{2,0},{4,6},{6,4},{1,3},{3,1},{5,7},{7,5},{8,10},{10,8},{12,... | collective-permute-start | bytes 30728 | tf_op jit(solution)/shard_map/ppermute | solution.py:500
  32.8 2.7 %collective-permute-start.8 = (bf16[8,640]{1,0:T(8,128)(2,1)S(1)}, bf16[8,640]{1,0:T(8,128)(2,1)S(1)}, u32[]{:S(2)}, u32[]{:S(2)}) collective-permute-start(bf16[8,640]{1,0:T(8,128)(2,1)S(1)} %collective-permute-done.4.refs_0_), channel_id=1, source_target_pairs={{0,1},{1,0},{2,3},{3,2},{4,5},{5,4},{6,7},{7,6},{8,9},{9,8},{10,11... | collective-permute-start | bytes 30728 | tf_op jit(solution)/shard_map/ppermute | solution.py:522
  32.9 2.7 %collective-permute-start.9 = (bf16[8,640]{1,0:T(8,128)(2,1)S(1)}, bf16[8,640]{1,0:T(8,128)(2,1)S(1)}, u32[]{:S(2)}, u32[]{:S(2)}) collective-permute-start(bf16[8,640]{1,0:T(8,128)(2,1)S(1)} %collective-permute-done.5.refs_1_), channel_id=1, source_target_pairs={{0,1},{1,0},{2,3},{3,2},{4,5},{5,4},{6,7},{7,6},{8,9},{9,8},{10,11... | collective-permute-start | bytes 30728 | tf_op jit(solution)/shard_map/ppermute | solution.py:522
  33.4 2.2 %collective-permute-start.10 = (bf16[8,640]{1,0:T(8,128)(2,1)S(1)}, bf16[8,640]{1,0:T(8,128)(2,1)S(1)}, u32[]{:S(2)}, u32[]{:S(2)}) collective-permute-start(bf16[8,640]{1,0:T(8,128)(2,1)S(1)} %collective-permute-done.6.refs_2_), channel_id=1, source_target_pairs={{0,1},{1,0},{2,3},{3,2},{4,5},{5,4},{6,7},{7,6},{8,9},{9,8},{10,11... | collective-permute-start | bytes 30728 | tf_op jit(solution)/shard_map/ppermute | solution.py:522
  38.5 1.3 %collective-permute-start.11 = (bf16[8,2048]{1,0:T(8,128)(2,1)S(1)}, bf16[8,2048]{1,0:T(8,128)(2,1)S(1)}, u32[]{:S(2)}, u32[]{:S(2)}) collective-permute-start(bf16[8,2048]{1,0:T(8,128)(2,1)S(1)} %get-tuple-element.67), channel_id=1, source_target_pairs={{0,1},{1,0},{2,3},{3,2},{4,5},{5,4},{6,7},{7,6},{8,9},{9,8},{10,11... | collective-permute-start | bytes 98312 | tf_op jit(solution)/shard_map/ppermute | solution.py:547
  39.9 5.5 %collective-permute-start.12 = (bf16[8,512]{1,0:T(8,128)(2,1)S(1)}, bf16[8,512]{1,0:T(8,128)(2,1)S(1)}, u32[]{:S(2)}, u32[]{:S(2)}) collective-permute-start(bf16[8,512]{1,0:T(8,128)(2,1)S(1)} %get-tuple-element.70), channel_id=1, source_target_pairs={{0,6},{2,4},{4,2},{6,0},{1,7},{3,5},{5,3},{7,1},{8,14},{10,12},{12... | collective-permute-start | bytes 24584 | tf_op jit(solution)/shard_map/ppermute | solution.py:569
  42.3 4.5 %collective-permute-start.13 = (bf16[8,512]{1,0:T(8,128)(2,1)S(1)}, bf16[8,512]{1,0:T(8,128)(2,1)S(1)}, u32[]{:S(2)}, u32[]{:S(2)}) collective-permute-start(bf16[8,512]{1,0:T(8,128)(2,1)S(1)} %get-tuple-element.71), channel_id=1, source_target_pairs={{0,4},{2,6},{4,0},{6,2},{1,5},{3,7},{5,1},{7,3},{8,12},{10,14},{12... | collective-permute-start | bytes 24584 | tf_op jit(solution)/shard_map/ppermute | solution.py:569
  43.4 3.7 %collective-permute-start.14 = (bf16[8,512]{1,0:T(8,128)(2,1)S(1)}, bf16[8,512]{1,0:T(8,128)(2,1)S(1)}, u32[]{:S(2)}, u32[]{:S(2)}) collective-permute-start(bf16[8,512]{1,0:T(8,128)(2,1)S(1)} %get-tuple-element.72), channel_id=1, source_target_pairs={{0,2},{2,0},{4,6},{6,4},{1,3},{3,1},{5,7},{7,5},{8,10},{10,8},{12,... | collective-permute-start | bytes 24584 | tf_op jit(solution)/shard_map/ppermute | solution.py:569
  (1 other events, 4.0 us)

commit v5 on v4

--- a/solution.py
+++ b/solution.py
@@ -288,18 +288,20 @@
         scale = lax.rsqrt(jnp.mean(attended * attended, axis=1, keepdims=True) + EPS)
         pieces.append(gate[:, vs] * (attended * scale * gain_ref[h : h + 1, :].astype(F32)))
     heads = jnp.concatenate(pieces, axis=1).astype(BF16)
-    for i in range(out_ref.shape[0]):
-        out_ref[i] = heads
-
-
-def output_kernel(n_tp, recv_ref, weight_ref, own_ref, gain_ref, after_ref, scaled_ref, rows_ref):
-    seq_dev, wide = recv_ref.shape[1], recv_ref.shape[2]
-    for i in range(recv_ref.shape[0]):
-        kv_at, tp_at = divmod(i, n_tp)
-        rows_ref[kv_at * seq_dev : (kv_at + 1) * seq_dev, tp_at * wide : (tp_at + 1) * wide] = recv_ref[
-            i
-        ].astype(F32)
-    projected = jnp.dot(rows_ref[...].astype(BF16), weight_ref[...], preferred_element_type=F32)
+    out_ref[...] = heads
+
+
+def output_kernel(n_kv, *refs):
+    near, far = refs[:n_kv], refs[n_kv : 2 * n_kv]
+    weight_ref, own_ref, gain_ref, after_ref, scaled_ref = refs[2 * n_kv :]
+    half = weight_ref.shape[0] // 2
+    tp = lax.axis_index("tp")
+    projected = 0.0
+    for parts, side in ((near, tp), (far, 1 - tp)):
+        rows = jnp.concatenate([part[...].astype(F32) for part in parts], axis=0).astype(BF16)
+        weight = weight_ref[pl.ds(pl.multiple_of(side * half, half), half), :]
+        projected = projected + jnp.dot(rows, weight, preferred_element_type=F32)
+    projected = by_partner(projected, near[0].shape[0], n_kv)
     after = (own_ref[...].astype(F32) + projected).astype(BF16)
     after_ref[...] = after
     after = after.astype(F32)
@@ -435,7 +437,6 @@
     seq_dev, heads_dev, key_dim, value_dim = state.shape
     width = mlp_gain.shape[0]
     n_kv, n_tp = lax.axis_size("kv"), lax.axis_size("tp")
-    members = n_kv * n_tp
     rows, columns = tokens.shape
     other = lax.ppermute(tokens, "tp", [(i, n_tp - 1 - i) for i in range(n_tp)])
     wide = heads_dev * (3 * key_dim + 2 * value_dim) + LANES
@@ -475,7 +476,7 @@
     )(lengths, own, in_vmem(state), in_vmem(cache_keys), in_vmem(cache_values), in_vmem(cache_rates), in_vmem(mlp_gain.reshape(-1, LANES)))
     send = call(
         lambda *refs: attend_kernel(width, refs[:n_kv], *refs[n_kv:]),
-        jax.ShapeDtypeStruct((members, seq_dev, heads_dev * value_dim), BF16),
+        jax.ShapeDtypeStruct((seq_dev, heads_dev * value_dim), BF16),
         [vmem_spec()] * (n_kv + 3),
         [pltpu.VMEM((seq_dev, heads_dev * value_dim), F32)],
         4 * MIB,
@@ -483,19 +484,22 @@
         state.size * 2,
         "attend",
     )(own, *parts[:0:-1], mixed, total, in_vmem(head_gain))
-    recv = lax.all_to_all(send, ("kv", "tp"), 0, 0, tiled=True)
+    swap = [(i, n_tp - 1 - i) for i in range(n_tp)]
+    near = [send] + [
+        lax.ppermute(send, "kv", [(i, i ^ step) for i in range(n_kv)]) for step in range(1, n_kv)
+    ]
+    across = [lax.ppermute(part, "tp", swap) for part in near]
     narrow = jax.ShapeDtypeStruct((rows, columns + LANES), BF16)
     after, scaled = call(
-        lambda *refs: output_kernel(n_tp, *refs),
+        lambda *refs: output_kernel(n_kv, *refs),
         (jax.ShapeDtypeStruct((rows, columns), BF16), narrow),
-        [vmem_spec()] * 4,
-        [pltpu.VMEM((rows, w_out.shape[0]), F32)],
-        2 * MIB,
+        [vmem_spec()] * (2 * n_kv + 3),
+        [],
+        6 * MIB,
         10**6,
         w_out.size * 2,
         "output",
-    )(recv, in_vmem(w_out), in_vmem(tokens), own_gain)
-    swap = [(i, n_tp - 1 - i) for i in range(n_tp)]
+    )(*near, *across, in_vmem(w_out), in_vmem(tokens), own_gain)
     far = n_kv - 1
     got = [lax.ppermute(scaled, "kv", [(i, i ^ step) for i in range(n_kv)]) for step in range(1, n_kv)]
     beside = lax.ppermute(scaled, "tp", swap)

time: 47.8 us -> 46.8 us (0.979)
  blocking collectives: 9.19 us -> 0 us
  starting transfers between devices: 16.1 us -> 21.3 us
  waiting for transfers between devices: 5.58 us -> 8.61 us
    all_to_all x1 -> x0, blocking collectives: 9.19 us -> none  [shards(): recv = lax.all_to_all(send, ('kv', 'tp'), 0, 0, tiled=True)]
    ppermute x0 -> x7, starting transfers between devices: none -> 4.96 us  [the longest x3 4.44 us: shards(): lax.ppermute(send, 'kv', [(i, i ^ step) for i in range(n_kv)])]
    ppermute x0 -> x7, waiting for transfers between devices: none -> 2.94 us  [the longest x3 2.12 us: shards(): lax.ppermute(send, 'kv', [(i, i ^ step) for i in range(n_kv)])]
  transfers between devices with their start and end apart: 15 -> 22, of which waited for: 5 -> 10; matrix products, arithmetic and copies ran while one was open for 0% -> 0% of each run, Pallas kernels for 14% -> 14%
where the time goes in v5:
time: 46.8 us; the launch traced here: 46.6 us
  starting transfers between devices  21.3 us (46%)
  Pallas kernels  16.4 us (35%)
  waiting for transfers between devices  8.61 us (18%)
    ppermute x3, starting transfers between devices, shards(): lax.ppermute(parts[step], 'kv', [(i, i ^ step) for i in range(n_kv)])  5.64 us
    pallas_call x1, Pallas kernels, shards(): call(lambda *refs: project_kernel(seq_dev, *refs), [jax.ShapeDtypeStruct(...  5 us
    ppermute x3, starting transfers between devices, shards(): lax.ppermute(merged[step], 'kv', [(i, i ^ step) for i in range(n_kv)])  4.45 us
    ppermute x3, starting transfers between devices, shards(): lax.ppermute(send, 'kv', [(i, i ^ step) for i in range(n_kv)])  4.44 us
    ppermute x3, starting transfers between devices, shards(): lax.ppermute(scaled, 'kv', [(i, i ^ step) for i in range(n_kv)])  4.39 us
    pallas_call x1, Pallas kernels, shards(): call(lambda *refs: third_kernel(cut, columns, far, width, *refs), [jax.Sh...  2.93 us
    ppermute x3, waiting for transfers between devices, shards(): lax.ppermute(merged[step], 'kv', [(i, i ^ step) for i in range(n_kv)])  2.39 us
    ppermute x3, waiting for transfers between devices, shards(): lax.ppermute(send, 'kv', [(i, i ^ step) for i in range(n_kv)])  2.12 us
  transfers between devices with their start and end apart: 22, of which 10 were waited for; matrix products, arithmetic and copies ran while one was open for 0% of the time, Pallas kernels for 14%

profile of v5, /device:TPU:0, one launch (start us, length us, event | category | flops | bytes accessed | tf_op | source)
XLA Modules:
  0.0 46.6 jit_solution(9868593889509334574)
XLA Ops:
  0.0 0.5 %collective-permute-start = (bf16[8,512]{1,0:T(8,128)(2,1)}, bf16[8,512]{1,0:T(8,128)(2,1)S(1)}, u32[]{:S(2)}, u32[]{:S(2)}) collective-permute-start(bf16[8,512]{1,0:T(8,128)(2,1)} %refs_9_.1), channel_id=1, source_target_pairs={{0,1},{1,0},{2,3},{3,2},{4,5},{5,4},{6,7},{7,6},{8,9},{9,8},{10,11... | collective-permute-start | bytes 24584 | tf_op jit(solution)/shard_map/ppermute | solution.py:441
  0.5 1.0 %collective-permute-done.refs_1_ = bf16[8,512]{1,0:T(8,128)(2,1)S(1)} collective-permute-done((bf16[8,512]{1,0:T(8,128)(2,1)}, bf16[8,512]{1,0:T(8,128)(2,1)S(1)}, u32[]{:S(2)}, u32[]{:S(2)}) %collective-permute-start) | collective-permute-done | bytes 8224 | tf_op jit(solution)/shard_map/ppermute | solution.py:441
  1.6 5.0 %project.1 = (f32[2,5504]{1,0:T(2,128)S(1)}, bf16[2,5504]{1,0:T(2,128)(2,1)S(1)}, bf16[2,5504]{1,0:T(2,128)(2,1)S(1)}, bf16[2,5504]{1,0:T(2,128)(2,1)S(1)}) custom-call(bf16[8,512]{1,0:T(8,128)(2,1)} %refs_9_.1, bf16[8,512]{1,0:T(8,128)(2,1)S(1)} %collective-permute-done.refs_1_, bf16[8,128]{1,0:T(8,128)(2,1)} %bitcast.17, bf16[1024,768]{1,0:T(8,128)(2,1)} %refs_3_.1, ...), custom_call_target="tpu_custom_call" | custom-call | flops 10000000000 | bytes 11010048 | tf_op jit(solution)/shard_map/project/pallas_call | solution.py:446
  6.6 5.0 %collective-permute-start.1 = (bf16[2,5504]{1,0:T(2,128)(2,1)S(1)}, bf16[2,5504]{1,0:T(2,128)(2,1)S(1)}, u32[]{:S(2)}, u32[]{:S(2)}) collective-permute-start(bf16[2,5504]{1,0:T(2,128)(2,1)S(1)} %get-tuple-element.40), channel_id=1, source_target_pairs={{0,6},{2,4},{4,2},{6,0},{1,7},{3,5},{5,3},{7,1},{8,14},{10,12},{12... | collective-permute-start | bytes 66056 | tf_op jit(solution)/shard_map/ppermute | solution.py:461
  11.6 0.6 %collective-permute-start.3 = (bf16[2,5504]{1,0:T(2,128)(2,1)S(1)}, bf16[2,5504]{1,0:T(2,128)(2,1)S(1)}, u32[]{:S(2)}, u32[]{:S(2)}) collective-permute-start(bf16[2,5504]{1,0:T(2,128)(2,1)S(1)} %get-tuple-element.42), channel_id=1, source_target_pairs={{0,2},{2,0},{4,6},{6,4},{1,3},{3,1},{5,7},{7,5},{8,10},{10,8},{12,... | collective-permute-start | bytes 66056 | tf_op jit(solution)/shard_map/ppermute | solution.py:461
  12.4 2.1 %gather.1 = (bf16[2,2,384,768]{3,2,1,0:T(8,128)(2,1)S(1)}, f32[2,768]{1,0:T(2,128)S(1)}, f32[1,512]{1,0:T(1,128)S(1)}) custom-call(s32[2]{0:T(128)S(1)} %copy-done.8, f32[2,5504]{1,0:T(2,128)S(1)} %get-tuple-element.39._.refs_0_, f32[2,2,384,768]{3,2,1,0:T(8,128)S(1)} %copy-done.3, bf16[2,2,64,384]{3,2,1,0:T(8,128)(2,1)S(1)} %copy-done.6, ...), custom_call_target="tpu_custom_call" | custom-call | flops 40000000000 | bytes 7864320 | tf_op jit(solution)/shard_map/gather/pallas_call | solution.py:463
  14.5 1.8 %collective-permute-done.2.refs_2_ = bf16[2,5504]{1,0:T(2,128)(2,1)S(1)} collective-permute-done((bf16[2,5504]{1,0:T(2,128)(2,1)S(1)}, bf16[2,5504]{1,0:T(2,128)(2,1)S(1)}, u32[]{:S(2)}, u32[]{:S(2)}) %collective-permute-start.2) | collective-permute-done | bytes 22048 | tf_op jit(solution)/shard_map/ppermute | solution.py:461
  16.3 0.6 %attend.1.refs_0_ = bf16[2,1536]{1,0:T(2,128)(2,1)S(1)} custom-call(f32[2,5504]{1,0:T(2,128)S(1)} %get-tuple-element.39._.refs_0_, bf16[2,5504]{1,0:T(2,128)(2,1)S(1)} %collective-permute-done.1.refs_1_, bf16[2,5504]{1,0:T(2,128)(2,1)S(1)} %collective-permute-done.2.refs_2_, bf16[2,5504]{1,0:T(2,128)(2,1)S(1)} %collective-permute-done.3.refs_3_, ...), custom_call_target="tpu_custom_call" | custom-call | flops 1000000 | bytes 2359296 | tf_op jit(solution)/shard_map/attend/pallas_call | solution.py:477
  16.9 2.0 %collective-permute-start.6 = (bf16[2,1536]{1,0:T(2,128)(2,1)S(1)}, bf16[2,1536]{1,0:T(2,128)(2,1)S(1)}, u32[]{:S(2)}, u32[]{:S(2)}) collective-permute-start(bf16[2,1536]{1,0:T(2,128)(2,1)S(1)} %attend.1.refs_0_), channel_id=1, source_target_pairs={{0,6},{2,4},{4,2},{6,0},{1,7},{3,5},{5,3},{7,1},{8,14},{10,12},{12... | collective-permute-start | bytes 18440 | tf_op jit(solution)/shard_map/ppermute | solution.py:489
  19.1 2.3 %collective-permute-start.4 = (bf16[2,1536]{1,0:T(2,128)(2,1)S(1)}, bf16[2,1536]{1,0:T(2,128)(2,1)S(1)}, u32[]{:S(2)}, u32[]{:S(2)}) collective-permute-start(bf16[2,1536]{1,0:T(2,128)(2,1)S(1)} %attend.1.refs_0_), channel_id=1, source_target_pairs={{0,2},{2,0},{4,6},{6,4},{1,3},{3,1},{5,7},{7,5},{8,10},{10,8},{12,... | collective-permute-start | bytes 18440 | tf_op jit(solution)/shard_map/ppermute | solution.py:489
  21.4 1.0 %collective-permute-done.6.refs_3_ = bf16[2,1536]{1,0:T(2,128)(2,1)S(1)} collective-permute-done((bf16[2,1536]{1,0:T(2,128)(2,1)S(1)}, bf16[2,1536]{1,0:T(2,128)(2,1)S(1)}, u32[]{:S(2)}, u32[]{:S(2)}) %collective-permute-start.6) | collective-permute-done | bytes 6176 | tf_op jit(solution)/shard_map/ppermute | solution.py:489
  22.4 1.1 %collective-permute-done.5.refs_2_ = bf16[2,1536]{1,0:T(2,128)(2,1)S(1)} collective-permute-done((bf16[2,1536]{1,0:T(2,128)(2,1)S(1)}, bf16[2,1536]{1,0:T(2,128)(2,1)S(1)}, u32[]{:S(2)}, u32[]{:S(2)}) %collective-permute-start.5) | collective-permute-done | bytes 6176 | tf_op jit(solution)/shard_map/ppermute | solution.py:489
  23.5 0.5 %collective-permute-start.8 = (bf16[2,1536]{1,0:T(2,128)(2,1)S(1)}, bf16[2,1536]{1,0:T(2,128)(2,1)S(1)}, u32[]{:S(2)}, u32[]{:S(2)}) collective-permute-start(bf16[2,1536]{1,0:T(2,128)(2,1)S(1)} %collective-permute-done.4.refs_1_), channel_id=1, source_target_pairs={{0,1},{1,0},{2,3},{3,2},{4,5},{5,4},{6,7},{7,6},{8,9},{9,8},{10,11... | collective-permute-start | bytes 18440 | tf_op jit(solution)/shard_map/ppermute | solution.py:491
  24.0 0.6 %collective-permute-done.9.refs_6_ = bf16[2,1536]{1,0:T(2,128)(2,1)S(1)} collective-permute-done((bf16[2,1536]{1,0:T(2,128)(2,1)S(1)}, bf16[2,1536]{1,0:T(2,128)(2,1)S(1)}, u32[]{:S(2)}, u32[]{:S(2)}) %collective-permute-start.9) | collective-permute-done | bytes 6176 | tf_op jit(solution)/shard_map/ppermute | solution.py:491
  24.8 0.6 %output.1 = (bf16[8,512]{1,0:T(8,128)(2,1)S(1)}, bf16[8,640]{1,0:T(8,128)(2,1)S(1)}) custom-call(bf16[2,1536]{1,0:T(2,128)(2,1)S(1)} %attend.1.refs_0_, bf16[2,1536]{1,0:T(2,128)(2,1)S(1)} %collective-permute-done.4.refs_1_, bf16[2,1536]{1,0:T(2,128)(2,1)S(1)} %collective-permute-done.5.refs_2_, bf16[2,1536]{1,0:T(2,128)(2,1)S(1)} %collective-permute-done.6.refs_3_, ...), custom_call_target="tpu_custom_call" | custom-call | flops 1000000 | bytes 3145728 | tf_op jit(solution)/shard_map/output/pallas_call | solution.py:493
  25.4 0.4 collective-permute-start.14
  25.8 1.8 %collective-permute-start.13 = (bf16[8,640]{1,0:T(8,128)(2,1)S(1)}, bf16[8,640]{1,0:T(8,128)(2,1)S(1)}, u32[]{:S(2)}, u32[]{:S(2)}) collective-permute-start(bf16[8,640]{1,0:T(8,128)(2,1)S(1)} %get-tuple-element.46.refs_0_), channel_id=1, source_target_pairs={{0,6},{2,4},{4,2},{6,0},{1,7},{3,5},{5,3},{7,1},{8,14},{10,12},{12... | collective-permute-start | bytes 30728 | tf_op jit(solution)/shard_map/ppermute | solution.py:504
  27.6 0.8 %collective-permute-start.12 = (bf16[8,640]{1,0:T(8,128)(2,1)S(1)}, bf16[8,640]{1,0:T(8,128)(2,1)S(1)}, u32[]{:S(2)}, u32[]{:S(2)}) collective-permute-start(bf16[8,640]{1,0:T(8,128)(2,1)S(1)} %get-tuple-element.46.refs_0_), channel_id=1, source_target_pairs={{0,4},{2,6},{4,0},{6,2},{1,5},{3,7},{5,1},{7,3},{8,12},{10,14},{12... | collective-permute-start | bytes 30728 | tf_op jit(solution)/shard_map/ppermute | solution.py:504
  28.4 1.8 %collective-permute-start.11 = (bf16[8,640]{1,0:T(8,128)(2,1)S(1)}, bf16[8,640]{1,0:T(8,128)(2,1)S(1)}, u32[]{:S(2)}, u32[]{:S(2)}) collective-permute-start(bf16[8,640]{1,0:T(8,128)(2,1)S(1)} %get-tuple-element.46.refs_0_), channel_id=1, source_target_pairs={{0,2},{2,0},{4,6},{6,4},{1,3},{3,1},{5,7},{7,5},{8,10},{10,8},{12,... | collective-permute-start | bytes 30728 | tf_op jit(solution)/shard_map/ppermute | solution.py:504
  30.3 1.5 %feed_first.1 = (f32[336,8]{1,0:T(8,128)S(1)}, f32[336,8]{1,0:T(8,128)S(1)}, f32[8,1040]{1,0:T(8,128)S(1)}, f32[8,1040]{1,0:T(8,128)S(1)}, f32[8,128]{1,0:T(8,128)S(1)}) custom-call(bf16[8,640]{1,0:T(8,128)(2,1)S(1)} %get-tuple-element.46.refs_0_, bf16[8,640]{1,0:T(8,128)(2,1)S(1)} %collective-permute-done.14.refs_1_, bf16[1376,4096]{1,0:T(8,128)(2,1)S(1)} %bitcast.8, ...), custom_call_target="tpu_custom_call" | custom-call | flops 1048576 | bytes 1048576 | tf_op jit(solution)/shard_map/feed_first/pallas_call | solution.py:515
  31.8 0.4 collective-permute-done.12.refs_1_
  32.2 0.5 %collective-permute-start.16 = (bf16[8,640]{1,0:T(8,128)(2,1)S(1)}, bf16[8,640]{1,0:T(8,128)(2,1)S(1)}, u32[]{:S(2)}, u32[]{:S(2)}) collective-permute-start(bf16[8,640]{1,0:T(8,128)(2,1)S(1)} %collective-permute-done.12.refs_1_), channel_id=1, source_target_pairs={{0,1},{1,0},{2,3},{3,2},{4,5},{5,4},{6,7},{7,6},{8,9},{9,8},{10,11... | collective-permute-start | bytes 30728 | tf_op jit(solution)/shard_map/ppermute | solution.py:526
  32.7 2.1 %feed_second.1 = (f32[336,8]{1,0:T(8,128)S(1)}, f32[336,8]{1,0:T(8,128)S(1)}, f32[8,1040]{1,0:T(8,128)S(1)}, f32[8,1040]{1,0:T(8,128)S(1)}, f32[8,128]{1,0:T(8,128)S(1)}) custom-call(bf16[8,640]{1,0:T(8,128)(2,1)S(1)} %collective-permute-done.11.refs_0_, bf16[8,640]{1,0:T(8,128)(2,1)S(1)} %collective-permute-done.12.refs_1_, ...), custom_call_target="tpu_custom_call" | custom-call | flops 1048576 | bytes 1048576 | tf_op jit(solution)/shard_map/feed_second/pallas_call | solution.py:527
  34.8 2.9 %feed_third.1 = (bf16[8,2048]{1,0:T(8,128)(2,1)S(1)}, bf16[336,8]{1,0:T(8,128)(2,1)S(1)}, bf16[8,1040]{1,0:T(8,128)(2,1)S(1)}) custom-call(bf16[8,640]{1,0:T(8,128)(2,1)S(1)} %collective-permute-done.15.refs_0_, bf16[8,640]{1,0:T(8,128)(2,1)S(1)} %collective-permute-done.16.refs_1_, bf16[8,640]{1,0:T(8,128)(2,1)S(1)} %collective-permute-done.17.refs_2_, ...), custom_call_target="tpu_custom_call" | custom-call | flops 1048576 | bytes 1048576 | tf_op jit(solution)/shard_map/feed_third/pallas_call | solution.py:537
  37.8 0.5 %collective-permute-start.18 = (bf16[8,2048]{1,0:T(8,128)(2,1)S(1)}, bf16[8,2048]{1,0:T(8,128)(2,1)S(1)}, u32[]{:S(2)}, u32[]{:S(2)}) collective-permute-start(bf16[8,2048]{1,0:T(8,128)(2,1)S(1)} %get-tuple-element.67), channel_id=1, source_target_pairs={{0,1},{1,0},{2,3},{3,2},{4,5},{5,4},{6,7},{7,6},{8,9},{9,8},{10,11... | collective-permute-start | bytes 98312 | tf_op jit(solution)/shard_map/ppermute | solution.py:551
  38.3 0.9 %feed_fourth.1.refs_0_ = f32[8,2048]{1,0:T(8,128)S(1)} custom-call(bf16[336,8]{1,0:T(8,128)(2,1)S(1)} %get-tuple-element.65.refs_0_, bf16[8,1040]{1,0:T(8,128)(2,1)S(1)} %get-tuple-element.66.refs_1_, bf16[1376,4096]{1,0:T(8,128)(2,1)S(1)} %bitcast.5), custom_call_target="tpu_custom_call" | custom-call | flops 1048576 | bytes 1048576 | tf_op jit(solution)/shard_map/feed_fourth/pallas_call | solution.py:552
  39.2 2.1 %collective-permute-start.19 = (bf16[8,512]{1,0:T(8,128)(2,1)S(1)}, bf16[8,512]{1,0:T(8,128)(2,1)S(1)}, u32[]{:S(2)}, u32[]{:S(2)}) collective-permute-start(bf16[8,512]{1,0:T(8,128)(2,1)S(1)} %get-tuple-element.70), channel_id=1, source_target_pairs={{0,6},{2,4},{4,2},{6,0},{1,7},{3,5},{5,3},{7,1},{8,14},{10,12},{12... | collective-permute-start | bytes 24584 | tf_op jit(solution)/shard_map/ppermute | solution.py:573
  41.3 1.1 %collective-permute-start.20 = (bf16[8,512]{1,0:T(8,128)(2,1)S(1)}, bf16[8,512]{1,0:T(8,128)(2,1)S(1)}, u32[]{:S(2)}, u32[]{:S(2)}) collective-permute-start(bf16[8,512]{1,0:T(8,128)(2,1)S(1)} %get-tuple-element.71), channel_id=1, source_target_pairs={{0,4},{2,6},{4,0},{6,2},{1,5},{3,7},{5,1},{7,3},{8,12},{10,14},{12... | collective-permute-start | bytes 24584 | tf_op jit(solution)/shard_map/ppermute | solution.py:573
  42.4 1.3 %collective-permute-start.21 = (bf16[8,512]{1,0:T(8,128)(2,1)S(1)}, bf16[8,512]{1,0:T(8,128)(2,1)S(1)}, u32[]{:S(2)}, u32[]{:S(2)}) collective-permute-start(bf16[8,512]{1,0:T(8,128)(2,1)S(1)} %get-tuple-element.72), channel_id=1, source_target_pairs={{0,2},{2,0},{4,6},{6,4},{1,3},{3,1},{5,7},{7,5},{8,10},{10,8},{12,... | collective-permute-start | bytes 24584 | tf_op jit(solution)/shard_map/ppermute | solution.py:573
  43.7 1.1 %collective-permute-done.19.refs_1_ = bf16[8,512]{1,0:T(8,128)(2,1)S(1)} collective-permute-done((bf16[8,512]{1,0:T(8,128)(2,1)S(1)}, bf16[8,512]{1,0:T(8,128)(2,1)S(1)}, u32[]{:S(2)}, u32[]{:S(2)}) %collective-permute-start.19) | collective-permute-done | bytes 8224 | tf_op jit(solution)/shard_map/ppermute | solution.py:573
  44.7 1.1 %collective-permute-done.20.refs_2_ = bf16[8,512]{1,0:T(8,128)(2,1)S(1)} collective-permute-done((bf16[8,512]{1,0:T(8,128)(2,1)S(1)}, bf16[8,512]{1,0:T(8,128)(2,1)S(1)}, u32[]{:S(2)}, u32[]{:S(2)}) %collective-permute-start.20) | collective-permute-done | bytes 8224 | tf_op jit(solution)/shard_map/ppermute | solution.py:573
  46.0 0.6 %finish.1 = bf16[8,512]{1,0:T(8,128)(2,1)} custom-call(f32[8,512]{1,0:T(8,128)S(1)} %get-tuple-element.69.refs_0_, bf16[8,512]{1,0:T(8,128)(2,1)S(1)} %collective-permute-done.19.refs_1_, bf16[8,512]{1,0:T(8,128)(2,1)S(1)} %collective-permute-done.20.refs_2_, bf16[8,512]{1,0:T(8,128)(2,1)S(1)} %collective-permute-done.21.refs_3_), custom_call_target="tpu_custom_call" | custom-call | flops 16384 | bytes 32768 | tf_op jit(solution)/shard_map/finish/pallas_call | solution.py:575
  (61 shorter events, 0.7 us)
Async XLA Ops:
  0.0 1.5 %collective-permute-start = (bf16[8,512]{1,0:T(8,128)(2,1)}, bf16[8,512]{1,0:T(8,128)(2,1)S(1)}, u32[]{:S(2)}, u32[]{:S(2)}) collective-permute-start(bf16[8,512]{1,0:T(8,128)(2,1)} %refs_9_.1), channel_id=1, source_target_pairs={{0,1},{1,0},{2,3},{3,2},{4,5},{5,4},{6,7},{7,6},{8,9},{9,8},{10,11... | collective-permute-start | bytes 24584 | tf_op jit(solution)/shard_map/ppermute | solution.py:441
  6.6 7.9 %collective-permute-start.1 = (bf16[2,5504]{1,0:T(2,128)(2,1)S(1)}, bf16[2,5504]{1,0:T(2,128)(2,1)S(1)}, u32[]{:S(2)}, u32[]{:S(2)}) collective-permute-start(bf16[2,5504]{1,0:T(2,128)(2,1)S(1)} %get-tuple-element.40), channel_id=1, source_target_pairs={{0,6},{2,4},{4,2},{6,0},{1,7},{3,5},{5,3},{7,1},{8,14},{10,12},{12... | collective-permute-start | bytes 66056 | tf_op jit(solution)/shard_map/ppermute | solution.py:461
  11.6 4.7 %collective-permute-start.2 = (bf16[2,5504]{1,0:T(2,128)(2,1)S(1)}, bf16[2,5504]{1,0:T(2,128)(2,1)S(1)}, u32[]{:S(2)}, u32[]{:S(2)}) collective-permute-start(bf16[2,5504]{1,0:T(2,128)(2,1)S(1)} %get-tuple-element.41), channel_id=1, source_target_pairs={{0,4},{2,6},{4,0},{6,2},{1,5},{3,7},{5,1},{7,3},{8,12},{10,14},{12... | collective-permute-start | bytes 66056 | tf_op jit(solution)/shard_map/ppermute | solution.py:461
  11.6 4.7 %collective-permute-start.3 = (bf16[2,5504]{1,0:T(2,128)(2,1)S(1)}, bf16[2,5504]{1,0:T(2,128)(2,1)S(1)}, u32[]{:S(2)}, u32[]{:S(2)}) collective-permute-start(bf16[2,5504]{1,0:T(2,128)(2,1)S(1)} %get-tuple-element.42), channel_id=1, source_target_pairs={{0,2},{2,0},{4,6},{6,4},{1,3},{3,1},{5,7},{7,5},{8,10},{10,8},{12,... | collective-permute-start | bytes 66056 | tf_op jit(solution)/shard_map/ppermute | solution.py:461
  12.2 18.0 %slice-start = ((s8[11272192]{0:T(1024)(128)(4,1)}), s8[4194304]{0:T(1024)(128)(4,1)S(1)}, s32[]{:S(2)}) async-start(s8[11272192]{0:T(1024)(128)(4,1)} %bitcast.4), calls=%async_computation | async-start | bytes 8388608
  12.2 18.0 %slice-start.3 = ((s8[11272192]{0:T(1024)(128)(4,1)}), s8[4194304]{0:T(1024)(128)(4,1)S(1)}, s32[]{:S(2)}) async-start(s8[11272192]{0:T(1024)(128)(4,1)} %bitcast.6), calls=%async_computation.3 | async-start | bytes 8388608
  12.2 18.0 %slice-start.6 = ((s8[11272192]{0:T(1024)(128)(4,1)}), s8[4194304]{0:T(1024)(128)(4,1)S(1)}, s32[]{:S(2)}) async-start(s8[11272192]{0:T(1024)(128)(4,1)} %bitcast.11), calls=%async_computation.6 | async-start | bytes 8388608
  12.3 12.5 %copy-start = (bf16[3072,512]{1,0:T(8,128)(2,1)S(1)}, bf16[3072,512]{1,0:T(8,128)(2,1)}, u32[]{:S(2)}) copy-start(bf16[3072,512]{1,0:T(8,128)(2,1)} %refs_8_.1) | copy-start | bytes 9437188
  12.3 17.9 %slice-start.1 = ((s8[11272192]{0:T(1024)(128)(4,1)}), s8[4194304]{0:T(1024)(128)(4,1)S(1)}, s32[]{:S(2)}) async-start(s8[11272192]{0:T(1024)(128)(4,1)} %bitcast.4), calls=%async_computation.1 | async-start | bytes 8388608
  12.3 17.9 %slice-start.2 = ((s8[11272192]{0:T(1024)(128)(4,1)}), s8[2883584]{0:T(1024)(128)(4,1)S(1)}, s32[]{:S(2)}) async-start(s8[11272192]{0:T(1024)(128)(4,1)} %bitcast.4), calls=%async_computation.2 | async-start | bytes 5767168
  12.3 17.9 %slice-start.4 = ((s8[11272192]{0:T(1024)(128)(4,1)}), s8[4194304]{0:T(1024)(128)(4,1)S(1)}, s32[]{:S(2)}) async-start(s8[11272192]{0:T(1024)(128)(4,1)} %bitcast.6), calls=%async_computation.4 | async-start | bytes 8388608
  12.3 17.9 %slice-start.5 = ((s8[11272192]{0:T(1024)(128)(4,1)}), s8[2883584]{0:T(1024)(128)(4,1)S(1)}, s32[]{:S(2)}) async-start(s8[11272192]{0:T(1024)(128)(4,1)} %bitcast.6), calls=%async_computation.5 | async-start | bytes 5767168
  12.4 17.9 %slice-start.7 = ((s8[11272192]{0:T(1024)(128)(4,1)}), s8[4194304]{0:T(1024)(128)(4,1)S(1)}, s32[]{:S(2)}) async-start(s8[11272192]{0:T(1024)(128)(4,1)} %bitcast.11), calls=%async_computation.7 | async-start | bytes 8388608
  12.4 17.9 %slice-start.8 = ((s8[11272192]{0:T(1024)(128)(4,1)}), s8[2883584]{0:T(1024)(128)(4,1)S(1)}, s32[]{:S(2)}) async-start(s8[11272192]{0:T(1024)(128)(4,1)} %bitcast.11), calls=%async_computation.8 | async-start | bytes 5767168
  16.9 5.5 %collective-permute-start.6 = (bf16[2,1536]{1,0:T(2,128)(2,1)S(1)}, bf16[2,1536]{1,0:T(2,128)(2,1)S(1)}, u32[]{:S(2)}, u32[]{:S(2)}) collective-permute-start(bf16[2,1536]{1,0:T(2,128)(2,1)S(1)} %attend.1.refs_0_), channel_id=1, source_target_pairs={{0,6},{2,4},{4,2},{6,0},{1,7},{3,5},{5,3},{7,1},{8,14},{10,12},{12... | collective-permute-start | bytes 18440 | tf_op jit(solution)/shard_map/ppermute | solution.py:489
  18.9 4.5 %collective-permute-start.5 = (bf16[2,1536]{1,0:T(2,128)(2,1)S(1)}, bf16[2,1536]{1,0:T(2,128)(2,1)S(1)}, u32[]{:S(2)}, u32[]{:S(2)}) collective-permute-start(bf16[2,1536]{1,0:T(2,128)(2,1)S(1)} %attend.1.refs_0_), channel_id=1, source_target_pairs={{0,4},{2,6},{4,0},{6,2},{1,5},{3,7},{5,1},{7,3},{8,12},{10,14},{12... | collective-permute-start | bytes 18440 | tf_op jit(solution)/shard_map/ppermute | solution.py:489
  19.1 4.4 %collective-permute-start.4 = (bf16[2,1536]{1,0:T(2,128)(2,1)S(1)}, bf16[2,1536]{1,0:T(2,128)(2,1)S(1)}, u32[]{:S(2)}, u32[]{:S(2)}) collective-permute-start(bf16[2,1536]{1,0:T(2,128)(2,1)S(1)} %attend.1.refs_0_), channel_id=1, source_target_pairs={{0,2},{2,0},{4,6},{6,4},{1,3},{3,1},{5,7},{7,5},{8,10},{10,8},{12,... | collective-permute-start | bytes 18440 | tf_op jit(solution)/shard_map/ppermute | solution.py:489
  21.3 2.6 %collective-permute-start.7 = (bf16[2,1536]{1,0:T(2,128)(2,1)S(1)}, bf16[2,1536]{1,0:T(2,128)(2,1)S(1)}, u32[]{:S(2)}, u32[]{:S(2)}) collective-permute-start(bf16[2,1536]{1,0:T(2,128)(2,1)S(1)} %attend.1.refs_0_), channel_id=1, source_target_pairs={{0,1},{1,0},{2,3},{3,2},{4,5},{5,4},{6,7},{7,6},{8,9},{9,8},{10,11... | collective-permute-start | bytes 18440 | tf_op jit(solution)/shard_map/ppermute | solution.py:491
  22.4 1.6 %collective-permute-start.10 = (bf16[2,1536]{1,0:T(2,128)(2,1)S(1)}, bf16[2,1536]{1,0:T(2,128)(2,1)S(1)}, u32[]{:S(2)}, u32[]{:S(2)}) collective-permute-start(bf16[2,1536]{1,0:T(2,128)(2,1)S(1)} %collective-permute-done.6.refs_3_), channel_id=1, source_target_pairs={{0,1},{1,0},{2,3},{3,2},{4,5},{5,4},{6,7},{7,6},{8,9},{9,8},{10,11... | collective-permute-start | bytes 18440 | tf_op jit(solution)/shard_map/ppermute | solution.py:491
  23.5 1.2 %collective-permute-start.9 = (bf16[2,1536]{1,0:T(2,128)(2,1)S(1)}, bf16[2,1536]{1,0:T(2,128)(2,1)S(1)}, u32[]{:S(2)}, u32[]{:S(2)}) collective-permute-start(bf16[2,1536]{1,0:T(2,128)(2,1)S(1)} %collective-permute-done.5.refs_2_), channel_id=1, source_target_pairs={{0,1},{1,0},{2,3},{3,2},{4,5},{5,4},{6,7},{7,6},{8,9},{9,8},{10,11... | collective-permute-start | bytes 18440 | tf_op jit(solution)/shard_map/ppermute | solution.py:491
  23.5 1.3 %collective-permute-start.8 = (bf16[2,1536]{1,0:T(2,128)(2,1)S(1)}, bf16[2,1536]{1,0:T(2,128)(2,1)S(1)}, u32[]{:S(2)}, u32[]{:S(2)}) collective-permute-start(bf16[2,1536]{1,0:T(2,128)(2,1)S(1)} %collective-permute-done.4.refs_1_), channel_id=1, source_target_pairs={{0,1},{1,0},{2,3},{3,2},{4,5},{5,4},{6,7},{7,6},{8,9},{9,8},{10,11... | collective-permute-start | bytes 18440 | tf_op jit(solution)/shard_map/ppermute | solution.py:491
  25.4 4.7 %collective-permute-start.14 = (bf16[8,640]{1,0:T(8,128)(2,1)S(1)}, bf16[8,640]{1,0:T(8,128)(2,1)S(1)}, u32[]{:S(2)}, u32[]{:S(2)}) collective-permute-start(bf16[8,640]{1,0:T(8,128)(2,1)S(1)} %get-tuple-element.46.refs_0_), channel_id=1, source_target_pairs={{0,1},{1,0},{2,3},{3,2},{4,5},{5,4},{6,7},{7,6},{8,9},{9,8},{10,11... | collective-permute-start | bytes 30728 | tf_op jit(solution)/shard_map/ppermute | solution.py:505
  25.8 6.0 %collective-permute-start.13 = (bf16[8,640]{1,0:T(8,128)(2,1)S(1)}, bf16[8,640]{1,0:T(8,128)(2,1)S(1)}, u32[]{:S(2)}, u32[]{:S(2)}) collective-permute-start(bf16[8,640]{1,0:T(8,128)(2,1)S(1)} %get-tuple-element.46.refs_0_), channel_id=1, source_target_pairs={{0,6},{2,4},{4,2},{6,0},{1,7},{3,5},{5,3},{7,1},{8,14},{10,12},{12... | collective-permute-start | bytes 30728 | tf_op jit(solution)/shard_map/ppermute | solution.py:504
  27.6 4.6 %collective-permute-start.12 = (bf16[8,640]{1,0:T(8,128)(2,1)S(1)}, bf16[8,640]{1,0:T(8,128)(2,1)S(1)}, u32[]{:S(2)}, u32[]{:S(2)}) collective-permute-start(bf16[8,640]{1,0:T(8,128)(2,1)S(1)} %get-tuple-element.46.refs_0_), channel_id=1, source_target_pairs={{0,4},{2,6},{4,0},{6,2},{1,5},{3,7},{5,1},{7,3},{8,12},{10,14},{12... | collective-permute-start | bytes 30728 | tf_op jit(solution)/shard_map/ppermute | solution.py:504
  28.4 3.8 %collective-permute-start.11 = (bf16[8,640]{1,0:T(8,128)(2,1)S(1)}, bf16[8,640]{1,0:T(8,128)(2,1)S(1)}, u32[]{:S(2)}, u32[]{:S(2)}) collective-permute-start(bf16[8,640]{1,0:T(8,128)(2,1)S(1)} %get-tuple-element.46.refs_0_), channel_id=1, source_target_pairs={{0,2},{2,0},{4,6},{6,4},{1,3},{3,1},{5,7},{7,5},{8,10},{10,8},{12,... | collective-permute-start | bytes 30728 | tf_op jit(solution)/shard_map/ppermute | solution.py:504
  32.2 2.6 %collective-permute-start.15 = (bf16[8,640]{1,0:T(8,128)(2,1)S(1)}, bf16[8,640]{1,0:T(8,128)(2,1)S(1)}, u32[]{:S(2)}, u32[]{:S(2)}) collective-permute-start(bf16[8,640]{1,0:T(8,128)(2,1)S(1)} %collective-permute-done.11.refs_0_), channel_id=1, source_target_pairs={{0,1},{1,0},{2,3},{3,2},{4,5},{5,4},{6,7},{7,6},{8,9},{9,8},{10,11... | collective-permute-start | bytes 30728 | tf_op jit(solution)/shard_map/ppermute | solution.py:526
  32.2 2.6 %collective-permute-start.16 = (bf16[8,640]{1,0:T(8,128)(2,1)S(1)}, bf16[8,640]{1,0:T(8,128)(2,1)S(1)}, u32[]{:S(2)}, u32[]{:S(2)}) collective-permute-start(bf16[8,640]{1,0:T(8,128)(2,1)S(1)} %collective-permute-done.12.refs_1_), channel_id=1, source_target_pairs={{0,1},{1,0},{2,3},{3,2},{4,5},{5,4},{6,7},{7,6},{8,9},{9,8},{10,11... | collective-permute-start | bytes 30728 | tf_op jit(solution)/shard_map/ppermute | solution.py:526
  32.7 2.1 %collective-permute-start.17 = (bf16[8,640]{1,0:T(8,128)(2,1)S(1)}, bf16[8,640]{1,0:T(8,128)(2,1)S(1)}, u32[]{:S(2)}, u32[]{:S(2)}) collective-permute-start(bf16[8,640]{1,0:T(8,128)(2,1)S(1)} %collective-permute-done.13.refs_2_), channel_id=1, source_target_pairs={{0,1},{1,0},{2,3},{3,2},{4,5},{5,4},{6,7},{7,6},{8,9},{9,8},{10,11... | collective-permute-start | bytes 30728 | tf_op jit(solution)/shard_map/ppermute | solution.py:526
  37.8 1.4 %collective-permute-start.18 = (bf16[8,2048]{1,0:T(8,128)(2,1)S(1)}, bf16[8,2048]{1,0:T(8,128)(2,1)S(1)}, u32[]{:S(2)}, u32[]{:S(2)}) collective-permute-start(bf16[8,2048]{1,0:T(8,128)(2,1)S(1)} %get-tuple-element.67), channel_id=1, source_target_pairs={{0,1},{1,0},{2,3},{3,2},{4,5},{5,4},{6,7},{7,6},{8,9},{9,8},{10,11... | collective-permute-start | bytes 98312 | tf_op jit(solution)/shard_map/ppermute | solution.py:551
  39.2 5.5 %collective-permute-start.19 = (bf16[8,512]{1,0:T(8,128)(2,1)S(1)}, bf16[8,512]{1,0:T(8,128)(2,1)S(1)}, u32[]{:S(2)}, u32[]{:S(2)}) collective-permute-start(bf16[8,512]{1,0:T(8,128)(2,1)S(1)} %get-tuple-element.70), channel_id=1, source_target_pairs={{0,6},{2,4},{4,2},{6,0},{1,7},{3,5},{5,3},{7,1},{8,14},{10,12},{12... | collective-permute-start | bytes 24584 | tf_op jit(solution)/shard_map/ppermute | solution.py:573
  41.3 4.6 %collective-permute-start.20 = (bf16[8,512]{1,0:T(8,128)(2,1)S(1)}, bf16[8,512]{1,0:T(8,128)(2,1)S(1)}, u32[]{:S(2)}, u32[]{:S(2)}) collective-permute-start(bf16[8,512]{1,0:T(8,128)(2,1)S(1)} %get-tuple-element.71), channel_id=1, source_target_pairs={{0,4},{2,6},{4,0},{6,2},{1,5},{3,7},{5,1},{7,3},{8,12},{10,14},{12... | collective-permute-start | bytes 24584 | tf_op jit(solution)/shard_map/ppermute | solution.py:573
  42.4 3.7 %collective-permute-start.21 = (bf16[8,512]{1,0:T(8,128)(2,1)S(1)}, bf16[8,512]{1,0:T(8,128)(2,1)S(1)}, u32[]{:S(2)}, u32[]{:S(2)}) collective-permute-start(bf16[8,512]{1,0:T(8,128)(2,1)S(1)} %get-tuple-element.72), channel_id=1, source_target_pairs={{0,2},{2,0},{4,6},{6,4},{1,3},{3,1},{5,7},{7,5},{8,10},{10,8},{12,... | collective-permute-start | bytes 24584 | tf_op jit(solution)/shard_map/ppermute | solution.py:573
  (8 other events, 80.7 us)

commit v6 on v5

--- a/solution.py
+++ b/solution.py
@@ -182,35 +182,61 @@
     return block
 
 
-def project_kernel(
-    seq_dev, own_hbm, other_ref, gain_hbm, wq, wk, wd, wv, wg, *rest
-):
-    out_refs, (own_ref, gain_ref, bq, bk, bd, bv, bg, acc, sems) = rest[:-9], rest[-9:]
-    pairs = ((own_hbm, own_ref), (gain_hbm, gain_ref), (wq, bq), (wk, bk), (wd, bd), (wv, bv), (wg, bg))
-    copies = [pltpu.make_async_copy(src, dst, sems.at[i]) for i, (src, dst) in enumerate(pairs)]
+def scale_half(half, gain, seq_dev, n_kv):
+    ordered = by_partner(half.astype(F32), seq_dev, n_kv)
+    squares = jnp.sum(ordered * ordered, axis=1, keepdims=True)
+    return (ordered * gain).astype(BF16), jnp.broadcast_to(squares, (half.shape[0], LANES))
+
+
+def half_gain(gain_ref, own):
+    gain = spread(gain_ref)
+    half = gain.shape[1] // 2
+    low = (lax.axis_index("tp") == 0) == own
+    return jnp.where(low, gain[:, :half], gain[:, half:])
+
+
+def prepare_kernel(seq_dev, n_kv, own_hbm, gain_hbm, scaled_ref, squares_ref, own_ref, gain_ref, sems):
+    copies = [
+        pltpu.make_async_copy(own_hbm, own_ref, sems.at[0]),
+        pltpu.make_async_copy(gain_hbm, gain_ref, sems.at[1]),
+    ]
     for copy in copies:
         copy.start()
-    copies[0].wait()
-    copies[1].wait()
-    own = own_ref[...].astype(F32)
-    other = other_ref[...].astype(F32)
+    for copy in copies:
+        copy.wait()
+    scaled_ref[...], squares_ref[...] = scale_half(own_ref[...], half_gain(gain_ref, True), seq_dev, n_kv)
+
+
+def values_kernel(seq_dev, n_kv, scaled_ref, squares_ref, other_ref, gain_ref, wv, wg, sums_ref, block_ref, total_ref):
+    scaled, squares = scale_half(other_ref[...], half_gain(gain_ref, False), seq_dev, n_kv)
+    total_ref[...] = squares_ref[...] + squares
+    own = scaled_ref[...].astype(F32)
+    scaled = scaled.astype(F32)
     first = lax.axis_index("tp") == 0
-    low = jnp.where(first, own, other)
-    high = jnp.where(first, other, own)
-    block = by_partner(jnp.concatenate([low, high], axis=1), seq_dev, len(out_refs))
-    total = jnp.sum(block * block, axis=1, keepdims=True)
-    scaled = (block * spread(gain_ref)).astype(BF16)
+    block = jnp.concatenate([jnp.where(first, own, scaled), jnp.where(first, scaled, own)], axis=1).astype(BF16)
+    block_ref[...] = block
+    cut = wv.shape[1]
+    sums_ref[:, :cut] = jnp.dot(block, wv[...], preferred_element_type=F32)
+    sums_ref[:, cut:] = jnp.dot(block, wg[...], preferred_element_type=F32)
+
+
+def keys_kernel(seq_dev, block_ref, total_ref, sums_ref, wq, wk, wd, *rest):
+    out_refs, acc = rest[:-1], rest[-1]
+    block = block_ref[...]
     at = 0
-    for copy, (_, buf) in zip(copies[2:], pairs[2:]):
-        copy.wait()
-        acc[:, at : at + buf.shape[1]] = jnp.dot(scaled, buf[...], preferred_element_type=F32)
-        at += buf.shape[1]
-    lane = lax.broadcasted_iota(jnp.int32, (block.shape[0], LANES), 1)
+    for weight in (wq, wk, wd):
+        acc[:, at : at + weight.shape[1]] = jnp.dot(block, weight[...], preferred_element_type=F32)
+        at += weight.shape[1]
+    total = total_ref[...]
+    lane = lax.broadcasted_iota(jnp.int32, total.shape, 1)
     upper = total.astype(BF16).astype(F32)
     lower = total - upper
-    acc[:, at : at + LANES] = jnp.where(lane == 0, upper, jnp.where(lane == 1, lower, 0.0))
+    squares = jnp.where(lane == 0, upper, jnp.where(lane == 1, lower, 0.0))
     for step, out_ref in enumerate(out_refs):
-        out_ref[...] = acc[step * seq_dev : (step + 1) * seq_dev, :].astype(out_ref.dtype)
+        take = slice(step * seq_dev, (step + 1) * seq_dev)
+        out_ref[:, :at] = acc[take, :].astype(out_ref.dtype)
+        out_ref[:, at : at + sums_ref.shape[1]] = sums_ref[take, :].astype(out_ref.dtype)
+        out_ref[:, at + sums_ref.shape[1] :] = squares[take, :].astype(out_ref.dtype)
 
 
 def split_rows(row):
@@ -441,20 +467,46 @@
     other = lax.ppermute(tokens, "tp", [(i, n_tp - 1 - i) for i in range(n_tp)])
     wide = heads_dev * (3 * key_dim + 2 * value_dim) + LANES
     anywhere = pl.BlockSpec(memory_space=pl.ANY)
-    weights = (w_query, w_key, w_decay, w_value, w_gate)
-    moved = sum(w.size for w in weights) * 2
+    gain_rows = attn_gain.reshape(-1, LANES)
+    scaled, squares = call(
+        lambda *refs: prepare_kernel(seq_dev, n_kv, *refs),
+        [jax.ShapeDtypeStruct(tokens.shape, BF16), jax.ShapeDtypeStruct((rows, LANES), F32)],
+        [anywhere] * 2,
+        [
+            pltpu.VMEM(tokens.shape, BF16),
+            pltpu.VMEM(gain_rows.shape, BF16),
+            pltpu.SemaphoreType.DMA((2,)),
+        ],
+        MIB,
+        10**10,
+        tokens.size * 2,
+        "prepare",
+    )(in_hbm(tokens), in_hbm(gain_rows))
+    late = 2 * heads_dev * value_dim
+    sums, block, squares = call(
+        lambda *refs: values_kernel(seq_dev, n_kv, *refs),
+        [
+            jax.ShapeDtypeStruct((rows, late), F32),
+            jax.ShapeDtypeStruct((rows, n_tp * columns), BF16),
+            jax.ShapeDtypeStruct((rows, LANES), F32),
+        ],
+        [vmem_spec()] * 6,
+        [],
+        4 * MIB,
+        10**6,
+        MIB,
+        "values",
+    )(scaled, squares, other, in_vmem(gain_rows), in_vmem(w_value), in_vmem(w_gate))
     parts = call(
-        lambda *refs: project_kernel(seq_dev, *refs),
+        lambda *refs: keys_kernel(seq_dev, *refs),
         [jax.ShapeDtypeStruct((seq_dev, wide), F32 if step == 0 else BF16) for step in range(n_kv)],
-        [anywhere, vmem_spec()] + [anywhere] * 6,
-        [pltpu.VMEM(tokens.shape, BF16), pltpu.VMEM((attn_gain.size // LANES, LANES), BF16)]
-        + [pltpu.VMEM(w.shape, BF16) for w in weights]
-        + [pltpu.VMEM((rows, wide), F32), pltpu.SemaphoreType.DMA((7,))],
-        16 * MIB,
+        [vmem_spec()] * 6,
+        [pltpu.VMEM((rows, wide - LANES - late), F32)],
+        4 * MIB,
         10**10,
-        moved,
-        "project",
-    )(in_hbm(tokens), other, in_hbm(attn_gain.reshape(-1, LANES)), *(in_hbm(w) for w in weights))
+        MIB,
+        "keys",
+    )(block, squares, sums, in_vmem(w_query), in_vmem(w_key), in_vmem(w_decay))
     parts = list(parts)
     own = parts[0]
     for step in range(1, n_kv):

time: 46.8 us -> 45.7 us (0.976)
  local copies, waits for them, and re-layouts: 0.08 us -> 2.64 us
  Pallas kernels: 16.4 us -> 14 us
  waiting for transfers between devices: 8.61 us -> 7.62 us
    unnamed x36 -> x50, local copies, waits for them, and re-layouts: 0.08 us -> 2.64 us
    pallas_call x1 -> x3, Pallas kernels: 5 us -> 2.62 us  [the longest x1 0.96 us: shards(): call(lambda *refs: prepare_kernel(seq_dev, n_kv, *refs), [jax.ShapeDtypeS...]
    ppermute x1, waiting for transfers between devices: 1.04 us -> 0.05 us  [shards(): other = lax.ppermute(tokens, 'tp', [(i, n_tp - 1 - i) for i in range(n_tp)])]
  transfers between devices with their start and end apart: 22 -> 22, of which waited for: 10 -> 9; matrix products, arithmetic and copies ran while one was open for 0% -> 0% of each run, Pallas kernels for 14% -> 17%
where the time goes in v6:
time: 45.7 us; the launch traced here: 45.5 us
  starting transfers between devices  20.9 us (46%)
  Pallas kernels  14 us (31%)
  waiting for transfers between devices  7.62 us (17%)
  local copies, waits for them, and re-layouts  2.64 us (6%)
    ppermute x3, starting transfers between devices, shards(): lax.ppermute(parts[step], 'kv', [(i, i ^ step) for i in range(n_kv)])  5.3 us
    ppermute x3, starting transfers between devices, shards(): lax.ppermute(merged[step], 'kv', [(i, i ^ step) for i in range(n_kv)])  4.45 us
    ppermute x3, starting transfers between devices, shards(): lax.ppermute(send, 'kv', [(i, i ^ step) for i in range(n_kv)])  4.44 us
    ppermute x3, starting transfers between devices, shards(): lax.ppermute(scaled, 'kv', [(i, i ^ step) for i in range(n_kv)])  4.39 us
    pallas_call x1, Pallas kernels, shards(): call(lambda *refs: third_kernel(cut, columns, far, width, *refs), [jax.Sh...  2.93 us
    unnamed x50, local copies, waits for them, and re-layouts  2.64 us
    ppermute x3, waiting for transfers between devices, shards(): lax.ppermute(merged[step], 'kv', [(i, i ^ step) for i in range(n_kv)])  2.41 us
    ppermute x3, waiting for transfers between devices, shards(): lax.ppermute(send, 'kv', [(i, i ^ step) for i in range(n_kv)])  2.14 us
  transfers between devices with their start and end apart: 22, of which 9 were waited for; matrix products, arithmetic and copies ran while one was open for 0% of the time, Pallas kernels for 17%

profile of v6, /device:TPU:0, one launch (start us, length us, event | category | flops | bytes accessed | tf_op | source)
XLA Modules:
  0.0 45.5 jit_solution(8135833395146005528)
XLA Ops:
  0.5 1.0 %prepare.1 = (bf16[8,512]{1,0:T(8,128)(2,1)S(1)}, f32[8,128]{1,0:T(8,128)S(1)}) custom-call(bf16[8,512]{1,0:T(8,128)(2,1)} %refs_9_.1, bf16[8,128]{1,0:T(8,128)(2,1)} %bitcast.16), custom_call_target="tpu_custom_call" | custom-call | flops 10000000000 | bytes 8192 | tf_op jit(solution)/shard_map/prepare/pallas_call | solution.py:471
  1.5 0.9 %copy-done = bf16[1024,1536]{1,0:T(8,128)(2,1)S(1)} copy-done((bf16[1024,1536]{1,0:T(8,128)(2,1)S(1)}, bf16[1024,1536]{1,0:T(8,128)(2,1)}, u32[]{:S(2)}) %copy-start) | copy-done | bytes 3145752
  2.4 1.0 %copy-done.1 = bf16[1024,1536]{1,0:T(8,128)(2,1)S(1)} copy-done((bf16[1024,1536]{1,0:T(8,128)(2,1)S(1)}, bf16[1024,1536]{1,0:T(8,128)(2,1)}, u32[]{:S(2)}) %copy-start.1) | copy-done | bytes 3145752
  3.4 0.9 %values.1 = (f32[8,3072]{1,0:T(8,128)S(1)}, bf16[8,1024]{1,0:T(8,128)(2,1)S(1)}, f32[8,128]{1,0:T(8,128)S(1)}) custom-call(bf16[8,512]{1,0:T(8,128)(2,1)S(1)} %get-tuple-element.44.refs_0_, f32[8,128]{1,0:T(8,128)S(1)} %get-tuple-element.45.refs_1_, bf16[8,512]{1,0:T(8,128)(2,1)S(1)} %collective-permute-done.refs_2_, bf16[8,128]{1,0:T(8,128)(2,1)S(1)} %bitcast.17, ...), custom_call_target="tpu_custom_call" | custom-call | flops 1000000 | bytes 1048576 | tf_op jit(solution)/shard_map/values/pallas_call | solution.py:486
  4.3 0.7 %copy-done.6 = bf16[1024,768]{1,0:T(8,128)(2,1)S(1)} copy-done((bf16[1024,768]{1,0:T(8,128)(2,1)S(1)}, bf16[1024,768]{1,0:T(8,128)(2,1)}, u32[]{:S(2)}) %copy-start.6) | copy-done | bytes 1572888
  5.0 0.7 %keys.1 = (f32[2,5504]{1,0:T(2,128)S(1)}, bf16[2,5504]{1,0:T(2,128)(2,1)S(1)}, bf16[2,5504]{1,0:T(2,128)(2,1)S(1)}, bf16[2,5504]{1,0:T(2,128)(2,1)S(1)}) custom-call(bf16[8,1024]{1,0:T(8,128)(2,1)S(1)} %get-tuple-element.46.refs_0_, f32[8,128]{1,0:T(8,128)S(1)} %get-tuple-element.47.refs_1_, f32[8,3072]{1,0:T(8,128)S(1)} %get-tuple-element.48.refs_2_, ...), custom_call_target="tpu_custom_call" | custom-call | flops 10000000000 | bytes 1048576 | tf_op jit(solution)/shard_map/keys/pallas_call | solution.py:500
  5.8 4.7 %collective-permute-start.1 = (bf16[2,5504]{1,0:T(2,128)(2,1)S(1)}, bf16[2,5504]{1,0:T(2,128)(2,1)S(1)}, u32[]{:S(2)}, u32[]{:S(2)}) collective-permute-start(bf16[2,5504]{1,0:T(2,128)(2,1)S(1)} %get-tuple-element.50), channel_id=1, source_target_pairs={{0,6},{2,4},{4,2},{6,0},{1,7},{3,5},{5,3},{7,1},{8,14},{10,12},{12... | collective-permute-start | bytes 66056 | tf_op jit(solution)/shard_map/ppermute | solution.py:513
  10.4 0.6 %collective-permute-start.3 = (bf16[2,5504]{1,0:T(2,128)(2,1)S(1)}, bf16[2,5504]{1,0:T(2,128)(2,1)S(1)}, u32[]{:S(2)}, u32[]{:S(2)}) collective-permute-start(bf16[2,5504]{1,0:T(2,128)(2,1)S(1)} %get-tuple-element.52), channel_id=1, source_target_pairs={{0,2},{2,0},{4,6},{6,4},{1,3},{3,1},{5,7},{7,5},{8,10},{10,8},{12,... | collective-permute-start | bytes 66056 | tf_op jit(solution)/shard_map/ppermute | solution.py:513
  11.3 2.1 %gather.1 = (bf16[2,2,384,768]{3,2,1,0:T(8,128)(2,1)S(1)}, f32[2,768]{1,0:T(2,128)S(1)}, f32[1,512]{1,0:T(1,128)S(1)}) custom-call(s32[2]{0:T(128)S(1)} %copy-done.13, f32[2,5504]{1,0:T(2,128)S(1)} %get-tuple-element.49._.refs_0_, f32[2,2,384,768]{3,2,1,0:T(8,128)S(1)} %bitcast.19, bf16[2,2,64,384]{3,2,1,0:T(8,128)(2,1)S(1)} %copy-done.11, ...), custom_call_target="tpu_custom_call" | custom-call | flops 40000000000 | bytes 7864320 | tf_op jit(solution)/shard_map/gather/pallas_call | solution.py:515
  13.4 1.8 %collective-permute-done.2.refs_2_ = bf16[2,5504]{1,0:T(2,128)(2,1)S(1)} collective-permute-done((bf16[2,5504]{1,0:T(2,128)(2,1)S(1)}, bf16[2,5504]{1,0:T(2,128)(2,1)S(1)}, u32[]{:S(2)}, u32[]{:S(2)}) %collective-permute-start.2) | collective-permute-done | bytes 22048 | tf_op jit(solution)/shard_map/ppermute | solution.py:513
  15.1 0.6 %attend.1.refs_0_ = bf16[2,1536]{1,0:T(2,128)(2,1)S(1)} custom-call(f32[2,5504]{1,0:T(2,128)S(1)} %get-tuple-element.49._.refs_0_, bf16[2,5504]{1,0:T(2,128)(2,1)S(1)} %collective-permute-done.1.refs_1_, bf16[2,5504]{1,0:T(2,128)(2,1)S(1)} %collective-permute-done.2.refs_2_, bf16[2,5504]{1,0:T(2,128)(2,1)S(1)} %collective-permute-done.3.refs_3_, ...), custom_call_target="tpu_custom_call" | custom-call | flops 1000000 | bytes 2359296 | tf_op jit(solution)/shard_map/attend/pallas_call | solution.py:529
  15.8 2.0 %collective-permute-start.6 = (bf16[2,1536]{1,0:T(2,128)(2,1)S(1)}, bf16[2,1536]{1,0:T(2,128)(2,1)S(1)}, u32[]{:S(2)}, u32[]{:S(2)}) collective-permute-start(bf16[2,1536]{1,0:T(2,128)(2,1)S(1)} %attend.1.refs_0_), channel_id=1, source_target_pairs={{0,6},{2,4},{4,2},{6,0},{1,7},{3,5},{5,3},{7,1},{8,14},{10,12},{12... | collective-permute-start | bytes 18440 | tf_op jit(solution)/shard_map/ppermute | solution.py:541
  17.9 2.3 %collective-permute-start.4 = (bf16[2,1536]{1,0:T(2,128)(2,1)S(1)}, bf16[2,1536]{1,0:T(2,128)(2,1)S(1)}, u32[]{:S(2)}, u32[]{:S(2)}) collective-permute-start(bf16[2,1536]{1,0:T(2,128)(2,1)S(1)} %attend.1.refs_0_), channel_id=1, source_target_pairs={{0,2},{2,0},{4,6},{6,4},{1,3},{3,1},{5,7},{7,5},{8,10},{10,8},{12,... | collective-permute-start | bytes 18440 | tf_op jit(solution)/shard_map/ppermute | solution.py:541
  20.2 1.0 %collective-permute-done.6.refs_3_ = bf16[2,1536]{1,0:T(2,128)(2,1)S(1)} collective-permute-done((bf16[2,1536]{1,0:T(2,128)(2,1)S(1)}, bf16[2,1536]{1,0:T(2,128)(2,1)S(1)}, u32[]{:S(2)}, u32[]{:S(2)}) %collective-permute-start.6) | collective-permute-done | bytes 6176 | tf_op jit(solution)/shard_map/ppermute | solution.py:541
  21.3 1.1 %collective-permute-done.5.refs_2_ = bf16[2,1536]{1,0:T(2,128)(2,1)S(1)} collective-permute-done((bf16[2,1536]{1,0:T(2,128)(2,1)S(1)}, bf16[2,1536]{1,0:T(2,128)(2,1)S(1)}, u32[]{:S(2)}, u32[]{:S(2)}) %collective-permute-start.5) | collective-permute-done | bytes 6176 | tf_op jit(solution)/shard_map/ppermute | solution.py:541
  22.4 0.5 %collective-permute-start.8 = (bf16[2,1536]{1,0:T(2,128)(2,1)S(1)}, bf16[2,1536]{1,0:T(2,128)(2,1)S(1)}, u32[]{:S(2)}, u32[]{:S(2)}) collective-permute-start(bf16[2,1536]{1,0:T(2,128)(2,1)S(1)} %collective-permute-done.4.refs_1_), channel_id=1, source_target_pairs={{0,1},{1,0},{2,3},{3,2},{4,5},{5,4},{6,7},{7,6},{8,9},{9,8},{10,11... | collective-permute-start | bytes 18440 | tf_op jit(solution)/shard_map/ppermute | solution.py:543
  22.9 0.6 %collective-permute-done.9.refs_6_ = bf16[2,1536]{1,0:T(2,128)(2,1)S(1)} collective-permute-done((bf16[2,1536]{1,0:T(2,128)(2,1)S(1)}, bf16[2,1536]{1,0:T(2,128)(2,1)S(1)}, u32[]{:S(2)}, u32[]{:S(2)}) %collective-permute-start.9) | collective-permute-done | bytes 6176 | tf_op jit(solution)/shard_map/ppermute | solution.py:543
  23.7 0.6 %output.1 = (bf16[8,512]{1,0:T(8,128)(2,1)S(1)}, bf16[8,640]{1,0:T(8,128)(2,1)S(1)}) custom-call(bf16[2,1536]{1,0:T(2,128)(2,1)S(1)} %attend.1.refs_0_, bf16[2,1536]{1,0:T(2,128)(2,1)S(1)} %collective-permute-done.4.refs_1_, bf16[2,1536]{1,0:T(2,128)(2,1)S(1)} %collective-permute-done.5.refs_2_, bf16[2,1536]{1,0:T(2,128)(2,1)S(1)} %collective-permute-done.6.refs_3_, ...), custom_call_target="tpu_custom_call" | custom-call | flops 1000000 | bytes 3145728 | tf_op jit(solution)/shard_map/output/pallas_call | solution.py:545
  24.7 1.8 %collective-permute-start.13 = (bf16[8,640]{1,0:T(8,128)(2,1)S(1)}, bf16[8,640]{1,0:T(8,128)(2,1)S(1)}, u32[]{:S(2)}, u32[]{:S(2)}) collective-permute-start(bf16[8,640]{1,0:T(8,128)(2,1)S(1)} %get-tuple-element.56.refs_0_), channel_id=1, source_target_pairs={{0,6},{2,4},{4,2},{6,0},{1,7},{3,5},{5,3},{7,1},{8,14},{10,12},{12... | collective-permute-start | bytes 30728 | tf_op jit(solution)/shard_map/ppermute | solution.py:556
  26.5 0.8 %collective-permute-start.12 = (bf16[8,640]{1,0:T(8,128)(2,1)S(1)}, bf16[8,640]{1,0:T(8,128)(2,1)S(1)}, u32[]{:S(2)}, u32[]{:S(2)}) collective-permute-start(bf16[8,640]{1,0:T(8,128)(2,1)S(1)} %get-tuple-element.56.refs_0_), channel_id=1, source_target_pairs={{0,4},{2,6},{4,0},{6,2},{1,5},{3,7},{5,1},{7,3},{8,12},{10,14},{12... | collective-permute-start | bytes 30728 | tf_op jit(solution)/shard_map/ppermute | solution.py:556
  27.3 1.8 %collective-permute-start.11 = (bf16[8,640]{1,0:T(8,128)(2,1)S(1)}, bf16[8,640]{1,0:T(8,128)(2,1)S(1)}, u32[]{:S(2)}, u32[]{:S(2)}) collective-permute-start(bf16[8,640]{1,0:T(8,128)(2,1)S(1)} %get-tuple-element.56.refs_0_), channel_id=1, source_target_pairs={{0,2},{2,0},{4,6},{6,4},{1,3},{3,1},{5,7},{7,5},{8,10},{10,8},{12,... | collective-permute-start | bytes 30728 | tf_op jit(solution)/shard_map/ppermute | solution.py:556
  29.2 1.5 %feed_first.1 = (f32[336,8]{1,0:T(8,128)S(1)}, f32[336,8]{1,0:T(8,128)S(1)}, f32[8,1040]{1,0:T(8,128)S(1)}, f32[8,1040]{1,0:T(8,128)S(1)}, f32[8,128]{1,0:T(8,128)S(1)}) custom-call(bf16[8,640]{1,0:T(8,128)(2,1)S(1)} %get-tuple-element.56.refs_0_, bf16[8,640]{1,0:T(8,128)(2,1)S(1)} %collective-permute-done.14.refs_1_, bf16[1376,4096]{1,0:T(8,128)(2,1)S(1)} %bitcast.8, ...), custom_call_target="tpu_custom_call" | custom-call | flops 1048576 | bytes 1048576 | tf_op jit(solution)/shard_map/feed_first/pallas_call | solution.py:567
  31.1 0.5 %collective-permute-start.16 = (bf16[8,640]{1,0:T(8,128)(2,1)S(1)}, bf16[8,640]{1,0:T(8,128)(2,1)S(1)}, u32[]{:S(2)}, u32[]{:S(2)}) collective-permute-start(bf16[8,640]{1,0:T(8,128)(2,1)S(1)} %collective-permute-done.12.refs_1_), channel_id=1, source_target_pairs={{0,1},{1,0},{2,3},{3,2},{4,5},{5,4},{6,7},{7,6},{8,9},{9,8},{10,11... | collective-permute-start | bytes 30728 | tf_op jit(solution)/shard_map/ppermute | solution.py:578
  31.6 2.1 %feed_second.1 = (f32[336,8]{1,0:T(8,128)S(1)}, f32[336,8]{1,0:T(8,128)S(1)}, f32[8,1040]{1,0:T(8,128)S(1)}, f32[8,1040]{1,0:T(8,128)S(1)}, f32[8,128]{1,0:T(8,128)S(1)}) custom-call(bf16[8,640]{1,0:T(8,128)(2,1)S(1)} %collective-permute-done.11.refs_0_, bf16[8,640]{1,0:T(8,128)(2,1)S(1)} %collective-permute-done.12.refs_1_, ...), custom_call_target="tpu_custom_call" | custom-call | flops 1048576 | bytes 1048576 | tf_op jit(solution)/shard_map/feed_second/pallas_call | solution.py:579
  33.7 2.9 %feed_third.1 = (bf16[8,2048]{1,0:T(8,128)(2,1)S(1)}, bf16[336,8]{1,0:T(8,128)(2,1)S(1)}, bf16[8,1040]{1,0:T(8,128)(2,1)S(1)}) custom-call(bf16[8,640]{1,0:T(8,128)(2,1)S(1)} %collective-permute-done.15.refs_0_, bf16[8,640]{1,0:T(8,128)(2,1)S(1)} %collective-permute-done.16.refs_1_, bf16[8,640]{1,0:T(8,128)(2,1)S(1)} %collective-permute-done.17.refs_2_, ...), custom_call_target="tpu_custom_call" | custom-call | flops 1048576 | bytes 1048576 | tf_op jit(solution)/shard_map/feed_third/pallas_call | solution.py:589
  37.1 0.9 %feed_fourth.1.refs_0_ = f32[8,2048]{1,0:T(8,128)S(1)} custom-call(bf16[336,8]{1,0:T(8,128)(2,1)S(1)} %get-tuple-element.75.refs_0_, bf16[8,1040]{1,0:T(8,128)(2,1)S(1)} %get-tuple-element.76.refs_1_, bf16[1376,4096]{1,0:T(8,128)(2,1)S(1)} %bitcast.5), custom_call_target="tpu_custom_call" | custom-call | flops 1048576 | bytes 1048576 | tf_op jit(solution)/shard_map/feed_fourth/pallas_call | solution.py:604
  38.0 2.1 %collective-permute-start.19 = (bf16[8,512]{1,0:T(8,128)(2,1)S(1)}, bf16[8,512]{1,0:T(8,128)(2,1)S(1)}, u32[]{:S(2)}, u32[]{:S(2)}) collective-permute-start(bf16[8,512]{1,0:T(8,128)(2,1)S(1)} %get-tuple-element.80), channel_id=1, source_target_pairs={{0,6},{2,4},{4,2},{6,0},{1,7},{3,5},{5,3},{7,1},{8,14},{10,12},{12... | collective-permute-start | bytes 24584 | tf_op jit(solution)/shard_map/ppermute | solution.py:625
  40.1 1.1 %collective-permute-start.20 = (bf16[8,512]{1,0:T(8,128)(2,1)S(1)}, bf16[8,512]{1,0:T(8,128)(2,1)S(1)}, u32[]{:S(2)}, u32[]{:S(2)}) collective-permute-start(bf16[8,512]{1,0:T(8,128)(2,1)S(1)} %get-tuple-element.81), channel_id=1, source_target_pairs={{0,4},{2,6},{4,0},{6,2},{1,5},{3,7},{5,1},{7,3},{8,12},{10,14},{12... | collective-permute-start | bytes 24584 | tf_op jit(solution)/shard_map/ppermute | solution.py:625
  41.3 1.2 %collective-permute-start.21 = (bf16[8,512]{1,0:T(8,128)(2,1)S(1)}, bf16[8,512]{1,0:T(8,128)(2,1)S(1)}, u32[]{:S(2)}, u32[]{:S(2)}) collective-permute-start(bf16[8,512]{1,0:T(8,128)(2,1)S(1)} %get-tuple-element.82), channel_id=1, source_target_pairs={{0,2},{2,0},{4,6},{6,4},{1,3},{3,1},{5,7},{7,5},{8,10},{10,8},{12,... | collective-permute-start | bytes 24584 | tf_op jit(solution)/shard_map/ppermute | solution.py:625
  42.5 1.1 %collective-permute-done.19.refs_1_ = bf16[8,512]{1,0:T(8,128)(2,1)S(1)} collective-permute-done((bf16[8,512]{1,0:T(8,128)(2,1)S(1)}, bf16[8,512]{1,0:T(8,128)(2,1)S(1)}, u32[]{:S(2)}, u32[]{:S(2)}) %collective-permute-start.19) | collective-permute-done | bytes 8224 | tf_op jit(solution)/shard_map/ppermute | solution.py:625
  43.6 1.1 %collective-permute-done.20.refs_2_ = bf16[8,512]{1,0:T(8,128)(2,1)S(1)} collective-permute-done((bf16[8,512]{1,0:T(8,128)(2,1)S(1)}, bf16[8,512]{1,0:T(8,128)(2,1)S(1)}, u32[]{:S(2)}, u32[]{:S(2)}) %collective-permute-start.20) | collective-permute-done | bytes 8224 | tf_op jit(solution)/shard_map/ppermute | solution.py:625
  44.9 0.6 %finish.1 = bf16[8,512]{1,0:T(8,128)(2,1)} custom-call(f32[8,512]{1,0:T(8,128)S(1)} %get-tuple-element.79.refs_0_, bf16[8,512]{1,0:T(8,128)(2,1)S(1)} %collective-permute-done.19.refs_1_, bf16[8,512]{1,0:T(8,128)(2,1)S(1)} %collective-permute-done.20.refs_2_, bf16[8,512]{1,0:T(8,128)(2,1)S(1)} %collective-permute-done.21.refs_3_), custom_call_target="tpu_custom_call" | custom-call | flops 16384 | bytes 32768 | tf_op jit(solution)/shard_map/finish/pallas_call | solution.py:627
  (78 shorter events, 2.4 us)
Async XLA Ops:
  0.0 1.5 %collective-permute-start = (bf16[8,512]{1,0:T(8,128)(2,1)}, bf16[8,512]{1,0:T(8,128)(2,1)S(1)}, u32[]{:S(2)}, u32[]{:S(2)}) collective-permute-start(bf16[8,512]{1,0:T(8,128)(2,1)} %refs_9_.1), channel_id=1, source_target_pairs={{0,1},{1,0},{2,3},{3,2},{4,5},{5,4},{6,7},{7,6},{8,9},{9,8},{10,11... | collective-permute-start | bytes 24584 | tf_op jit(solution)/shard_map/ppermute | solution.py:467
  5.8 7.6 %collective-permute-start.1 = (bf16[2,5504]{1,0:T(2,128)(2,1)S(1)}, bf16[2,5504]{1,0:T(2,128)(2,1)S(1)}, u32[]{:S(2)}, u32[]{:S(2)}) collective-permute-start(bf16[2,5504]{1,0:T(2,128)(2,1)S(1)} %get-tuple-element.50), channel_id=1, source_target_pairs={{0,6},{2,4},{4,2},{6,0},{1,7},{3,5},{5,3},{7,1},{8,14},{10,12},{12... | collective-permute-start | bytes 66056 | tf_op jit(solution)/shard_map/ppermute | solution.py:513
  10.4 4.7 %collective-permute-start.2 = (bf16[2,5504]{1,0:T(2,128)(2,1)S(1)}, bf16[2,5504]{1,0:T(2,128)(2,1)S(1)}, u32[]{:S(2)}, u32[]{:S(2)}) collective-permute-start(bf16[2,5504]{1,0:T(2,128)(2,1)S(1)} %get-tuple-element.51), channel_id=1, source_target_pairs={{0,4},{2,6},{4,0},{6,2},{1,5},{3,7},{5,1},{7,3},{8,12},{10,14},{12... | collective-permute-start | bytes 66056 | tf_op jit(solution)/shard_map/ppermute | solution.py:513
  10.4 4.7 %collective-permute-start.3 = (bf16[2,5504]{1,0:T(2,128)(2,1)S(1)}, bf16[2,5504]{1,0:T(2,128)(2,1)S(1)}, u32[]{:S(2)}, u32[]{:S(2)}) collective-permute-start(bf16[2,5504]{1,0:T(2,128)(2,1)S(1)} %get-tuple-element.52), channel_id=1, source_target_pairs={{0,2},{2,0},{4,6},{6,4},{1,3},{3,1},{5,7},{7,5},{8,10},{10,8},{12,... | collective-permute-start | bytes 66056 | tf_op jit(solution)/shard_map/ppermute | solution.py:513
  11.1 18.0 %slice-start = ((s8[11272192]{0:T(1024)(128)(4,1)}), s8[4194304]{0:T(1024)(128)(4,1)S(1)}, s32[]{:S(2)}) async-start(s8[11272192]{0:T(1024)(128)(4,1)} %bitcast.4), calls=%async_computation | async-start | bytes 8388608
  11.1 18.0 %slice-start.3 = ((s8[11272192]{0:T(1024)(128)(4,1)}), s8[4194304]{0:T(1024)(128)(4,1)S(1)}, s32[]{:S(2)}) async-start(s8[11272192]{0:T(1024)(128)(4,1)} %bitcast.6), calls=%async_computation.3 | async-start | bytes 8388608
  11.1 18.0 %slice-start.6 = ((s8[11272192]{0:T(1024)(128)(4,1)}), s8[4194304]{0:T(1024)(128)(4,1)S(1)}, s32[]{:S(2)}) async-start(s8[11272192]{0:T(1024)(128)(4,1)} %bitcast.11), calls=%async_computation.6 | async-start | bytes 8388608
  11.2 12.5 %copy-start.2 = (bf16[3072,512]{1,0:T(8,128)(2,1)S(1)}, bf16[3072,512]{1,0:T(8,128)(2,1)}, u32[]{:S(2)}) copy-start(bf16[3072,512]{1,0:T(8,128)(2,1)} %refs_8_.1) | copy-start | bytes 9437188
  11.2 17.9 %slice-start.1 = ((s8[11272192]{0:T(1024)(128)(4,1)}), s8[4194304]{0:T(1024)(128)(4,1)S(1)}, s32[]{:S(2)}) async-start(s8[11272192]{0:T(1024)(128)(4,1)} %bitcast.4), calls=%async_computation.1 | async-start | bytes 8388608
  11.2 17.9 %slice-start.2 = ((s8[11272192]{0:T(1024)(128)(4,1)}), s8[2883584]{0:T(1024)(128)(4,1)S(1)}, s32[]{:S(2)}) async-start(s8[11272192]{0:T(1024)(128)(4,1)} %bitcast.4), calls=%async_computation.2 | async-start | bytes 5767168
  11.2 17.9 %slice-start.4 = ((s8[11272192]{0:T(1024)(128)(4,1)}), s8[4194304]{0:T(1024)(128)(4,1)S(1)}, s32[]{:S(2)}) async-start(s8[11272192]{0:T(1024)(128)(4,1)} %bitcast.6), calls=%async_computation.4 | async-start | bytes 8388608
  11.2 17.9 %slice-start.5 = ((s8[11272192]{0:T(1024)(128)(4,1)}), s8[2883584]{0:T(1024)(128)(4,1)S(1)}, s32[]{:S(2)}) async-start(s8[11272192]{0:T(1024)(128)(4,1)} %bitcast.6), calls=%async_computation.5 | async-start | bytes 5767168
  11.2 17.9 %slice-start.7 = ((s8[11272192]{0:T(1024)(128)(4,1)}), s8[4194304]{0:T(1024)(128)(4,1)S(1)}, s32[]{:S(2)}) async-start(s8[11272192]{0:T(1024)(128)(4,1)} %bitcast.11), calls=%async_computation.7 | async-start | bytes 8388608
  11.3 17.9 %slice-start.8 = ((s8[11272192]{0:T(1024)(128)(4,1)}), s8[2883584]{0:T(1024)(128)(4,1)S(1)}, s32[]{:S(2)}) async-start(s8[11272192]{0:T(1024)(128)(4,1)} %bitcast.11), calls=%async_computation.8 | async-start | bytes 5767168
  15.8 5.5 %collective-permute-start.6 = (bf16[2,1536]{1,0:T(2,128)(2,1)S(1)}, bf16[2,1536]{1,0:T(2,128)(2,1)S(1)}, u32[]{:S(2)}, u32[]{:S(2)}) collective-permute-start(bf16[2,1536]{1,0:T(2,128)(2,1)S(1)} %attend.1.refs_0_), channel_id=1, source_target_pairs={{0,6},{2,4},{4,2},{6,0},{1,7},{3,5},{5,3},{7,1},{8,14},{10,12},{12... | collective-permute-start | bytes 18440 | tf_op jit(solution)/shard_map/ppermute | solution.py:541
  17.8 4.5 %collective-permute-start.5 = (bf16[2,1536]{1,0:T(2,128)(2,1)S(1)}, bf16[2,1536]{1,0:T(2,128)(2,1)S(1)}, u32[]{:S(2)}, u32[]{:S(2)}) collective-permute-start(bf16[2,1536]{1,0:T(2,128)(2,1)S(1)} %attend.1.refs_0_), channel_id=1, source_target_pairs={{0,4},{2,6},{4,0},{6,2},{1,5},{3,7},{5,1},{7,3},{8,12},{10,14},{12... | collective-permute-start | bytes 18440 | tf_op jit(solution)/shard_map/ppermute | solution.py:541
  17.9 4.4 %collective-permute-start.4 = (bf16[2,1536]{1,0:T(2,128)(2,1)S(1)}, bf16[2,1536]{1,0:T(2,128)(2,1)S(1)}, u32[]{:S(2)}, u32[]{:S(2)}) collective-permute-start(bf16[2,1536]{1,0:T(2,128)(2,1)S(1)} %attend.1.refs_0_), channel_id=1, source_target_pairs={{0,2},{2,0},{4,6},{6,4},{1,3},{3,1},{5,7},{7,5},{8,10},{10,8},{12,... | collective-permute-start | bytes 18440 | tf_op jit(solution)/shard_map/ppermute | solution.py:541
  20.2 2.7 %collective-permute-start.7 = (bf16[2,1536]{1,0:T(2,128)(2,1)S(1)}, bf16[2,1536]{1,0:T(2,128)(2,1)S(1)}, u32[]{:S(2)}, u32[]{:S(2)}) collective-permute-start(bf16[2,1536]{1,0:T(2,128)(2,1)S(1)} %attend.1.refs_0_), channel_id=1, source_target_pairs={{0,1},{1,0},{2,3},{3,2},{4,5},{5,4},{6,7},{7,6},{8,9},{9,8},{10,11... | collective-permute-start | bytes 18440 | tf_op jit(solution)/shard_map/ppermute | solution.py:543
  21.3 1.6 %collective-permute-start.10 = (bf16[2,1536]{1,0:T(2,128)(2,1)S(1)}, bf16[2,1536]{1,0:T(2,128)(2,1)S(1)}, u32[]{:S(2)}, u32[]{:S(2)}) collective-permute-start(bf16[2,1536]{1,0:T(2,128)(2,1)S(1)} %collective-permute-done.6.refs_3_), channel_id=1, source_target_pairs={{0,1},{1,0},{2,3},{3,2},{4,5},{5,4},{6,7},{7,6},{8,9},{9,8},{10,11... | collective-permute-start | bytes 18440 | tf_op jit(solution)/shard_map/ppermute | solution.py:543
  22.4 1.2 %collective-permute-start.9 = (bf16[2,1536]{1,0:T(2,128)(2,1)S(1)}, bf16[2,1536]{1,0:T(2,128)(2,1)S(1)}, u32[]{:S(2)}, u32[]{:S(2)}) collective-permute-start(bf16[2,1536]{1,0:T(2,128)(2,1)S(1)} %collective-permute-done.5.refs_2_), channel_id=1, source_target_pairs={{0,1},{1,0},{2,3},{3,2},{4,5},{5,4},{6,7},{7,6},{8,9},{9,8},{10,11... | collective-permute-start | bytes 18440 | tf_op jit(solution)/shard_map/ppermute | solution.py:543
  22.4 1.3 %collective-permute-start.8 = (bf16[2,1536]{1,0:T(2,128)(2,1)S(1)}, bf16[2,1536]{1,0:T(2,128)(2,1)S(1)}, u32[]{:S(2)}, u32[]{:S(2)}) collective-permute-start(bf16[2,1536]{1,0:T(2,128)(2,1)S(1)} %collective-permute-done.4.refs_1_), channel_id=1, source_target_pairs={{0,1},{1,0},{2,3},{3,2},{4,5},{5,4},{6,7},{7,6},{8,9},{9,8},{10,11... | collective-permute-start | bytes 18440 | tf_op jit(solution)/shard_map/ppermute | solution.py:543
  24.3 4.7 %collective-permute-start.14 = (bf16[8,640]{1,0:T(8,128)(2,1)S(1)}, bf16[8,640]{1,0:T(8,128)(2,1)S(1)}, u32[]{:S(2)}, u32[]{:S(2)}) collective-permute-start(bf16[8,640]{1,0:T(8,128)(2,1)S(1)} %get-tuple-element.56.refs_0_), channel_id=1, source_target_pairs={{0,1},{1,0},{2,3},{3,2},{4,5},{5,4},{6,7},{7,6},{8,9},{9,8},{10,11... | collective-permute-start | bytes 30728 | tf_op jit(solution)/shard_map/ppermute | solution.py:557
  24.7 6.0 %collective-permute-start.13 = (bf16[8,640]{1,0:T(8,128)(2,1)S(1)}, bf16[8,640]{1,0:T(8,128)(2,1)S(1)}, u32[]{:S(2)}, u32[]{:S(2)}) collective-permute-start(bf16[8,640]{1,0:T(8,128)(2,1)S(1)} %get-tuple-element.56.refs_0_), channel_id=1, source_target_pairs={{0,6},{2,4},{4,2},{6,0},{1,7},{3,5},{5,3},{7,1},{8,14},{10,12},{12... | collective-permute-start | bytes 30728 | tf_op jit(solution)/shard_map/ppermute | solution.py:556
  26.5 4.6 %collective-permute-start.12 = (bf16[8,640]{1,0:T(8,128)(2,1)S(1)}, bf16[8,640]{1,0:T(8,128)(2,1)S(1)}, u32[]{:S(2)}, u32[]{:S(2)}) collective-permute-start(bf16[8,640]{1,0:T(8,128)(2,1)S(1)} %get-tuple-element.56.refs_0_), channel_id=1, source_target_pairs={{0,4},{2,6},{4,0},{6,2},{1,5},{3,7},{5,1},{7,3},{8,12},{10,14},{12... | collective-permute-start | bytes 30728 | tf_op jit(solution)/shard_map/ppermute | solution.py:556
  27.3 3.8 %collective-permute-start.11 = (bf16[8,640]{1,0:T(8,128)(2,1)S(1)}, bf16[8,640]{1,0:T(8,128)(2,1)S(1)}, u32[]{:S(2)}, u32[]{:S(2)}) collective-permute-start(bf16[8,640]{1,0:T(8,128)(2,1)S(1)} %get-tuple-element.56.refs_0_), channel_id=1, source_target_pairs={{0,2},{2,0},{4,6},{6,4},{1,3},{3,1},{5,7},{7,5},{8,10},{10,8},{12,... | collective-permute-start | bytes 30728 | tf_op jit(solution)/shard_map/ppermute | solution.py:556
  31.1 2.6 %collective-permute-start.15 = (bf16[8,640]{1,0:T(8,128)(2,1)S(1)}, bf16[8,640]{1,0:T(8,128)(2,1)S(1)}, u32[]{:S(2)}, u32[]{:S(2)}) collective-permute-start(bf16[8,640]{1,0:T(8,128)(2,1)S(1)} %collective-permute-done.11.refs_0_), channel_id=1, source_target_pairs={{0,1},{1,0},{2,3},{3,2},{4,5},{5,4},{6,7},{7,6},{8,9},{9,8},{10,11... | collective-permute-start | bytes 30728 | tf_op jit(solution)/shard_map/ppermute | solution.py:578
  31.1 2.6 %collective-permute-start.16 = (bf16[8,640]{1,0:T(8,128)(2,1)S(1)}, bf16[8,640]{1,0:T(8,128)(2,1)S(1)}, u32[]{:S(2)}, u32[]{:S(2)}) collective-permute-start(bf16[8,640]{1,0:T(8,128)(2,1)S(1)} %collective-permute-done.12.refs_1_), channel_id=1, source_target_pairs={{0,1},{1,0},{2,3},{3,2},{4,5},{5,4},{6,7},{7,6},{8,9},{9,8},{10,11... | collective-permute-start | bytes 30728 | tf_op jit(solution)/shard_map/ppermute | solution.py:578
  31.6 2.1 %collective-permute-start.17 = (bf16[8,640]{1,0:T(8,128)(2,1)S(1)}, bf16[8,640]{1,0:T(8,128)(2,1)S(1)}, u32[]{:S(2)}, u32[]{:S(2)}) collective-permute-start(bf16[8,640]{1,0:T(8,128)(2,1)S(1)} %collective-permute-done.13.refs_2_), channel_id=1, source_target_pairs={{0,1},{1,0},{2,3},{3,2},{4,5},{5,4},{6,7},{7,6},{8,9},{9,8},{10,11... | collective-permute-start | bytes 30728 | tf_op jit(solution)/shard_map/ppermute | solution.py:578
  36.6 1.4 %collective-permute-start.18 = (bf16[8,2048]{1,0:T(8,128)(2,1)S(1)}, bf16[8,2048]{1,0:T(8,128)(2,1)S(1)}, u32[]{:S(2)}, u32[]{:S(2)}) collective-permute-start(bf16[8,2048]{1,0:T(8,128)(2,1)S(1)} %get-tuple-element.77), channel_id=1, source_target_pairs={{0,1},{1,0},{2,3},{3,2},{4,5},{5,4},{6,7},{7,6},{8,9},{9,8},{10,11... | collective-permute-start | bytes 98312 | tf_op jit(solution)/shard_map/ppermute | solution.py:603
  38.0 5.5 %collective-permute-start.19 = (bf16[8,512]{1,0:T(8,128)(2,1)S(1)}, bf16[8,512]{1,0:T(8,128)(2,1)S(1)}, u32[]{:S(2)}, u32[]{:S(2)}) collective-permute-start(bf16[8,512]{1,0:T(8,128)(2,1)S(1)} %get-tuple-element.80), channel_id=1, source_target_pairs={{0,6},{2,4},{4,2},{6,0},{1,7},{3,5},{5,3},{7,1},{8,14},{10,12},{12... | collective-permute-start | bytes 24584 | tf_op jit(solution)/shard_map/ppermute | solution.py:625
  40.1 4.6 %collective-permute-start.20 = (bf16[8,512]{1,0:T(8,128)(2,1)S(1)}, bf16[8,512]{1,0:T(8,128)(2,1)S(1)}, u32[]{:S(2)}, u32[]{:S(2)}) collective-permute-start(bf16[8,512]{1,0:T(8,128)(2,1)S(1)} %get-tuple-element.81), channel_id=1, source_target_pairs={{0,4},{2,6},{4,0},{6,2},{1,5},{3,7},{5,1},{7,3},{8,12},{10,14},{12... | collective-permute-start | bytes 24584 | tf_op jit(solution)/shard_map/ppermute | solution.py:625
  41.3 3.7 %collective-permute-start.21 = (bf16[8,512]{1,0:T(8,128)(2,1)S(1)}, bf16[8,512]{1,0:T(8,128)(2,1)S(1)}, u32[]{:S(2)}, u32[]{:S(2)}) collective-permute-start(bf16[8,512]{1,0:T(8,128)(2,1)S(1)} %get-tuple-element.82), channel_id=1, source_target_pairs={{0,2},{2,0},{4,6},{6,4},{1,3},{3,1},{5,7},{7,5},{8,10},{10,8},{12,... | collective-permute-start | bytes 24584 | tf_op jit(solution)/shard_map/ppermute | solution.py:625
  (15 other events, 77.8 us)
